TPU v7x, 256 devices: a whole 4x4x8 slice. The times are simulated.
256 devices in a mesh: ep: 64 (over z, y, core), tp: 4 (over x).
Axes of the slice: x: 4, y: 4, z: 8, core: 2. Of those that a mesh axis runs over, the one named last changes fastest.
Arguments:
- mixer_input: bfloat16 [32768, 2048], P('ep'), may hold values from -6 to 6
- mixer_gain: bfloat16 [2048], replicated, may hold values from 0.099609375 to 1.8984375
- pool_in: bfloat16 [2048, 1024], P(None, 'tp'), may hold values from -0.125 to 0.125
- pool_map: bfloat16 [4, 256, 256], P('tp'), may hold values from -0.375 to 0.375
- pool_scale: bfloat16 [1024], P('tp'), may hold values from 0.099609375 to 1.8984375
- pool_out: bfloat16 [1024, 2048], P('tp'), may hold values from -0.1875 to 0.1875
- expert_input: bfloat16 [24576, 2048], P('ep'), may hold values from -6 to 6
- expert_gain: bfloat16 [2048], replicated, may hold values from 0.099609375 to 1.8984375
- group_router: bfloat16 [2048, 4], replicated, may hold values from -0.125 to 0.125
- expert_router: bfloat16 [2048, 64], replicated, may hold values from -0.125 to 0.125
- routes: int32 [24576, 2], P('ep'), may hold values from 0 to 63, all different within a row; in each aligned block of 96 rows (0 to 95, 96 to 191, ...) at most 6 rows name the same one
- gate_weight: bfloat16 [64, 2048, 1024], P('ep', None, 'tp'), may hold values from -0.125 to 0.125
- up_weight: bfloat16 [64, 2048, 1024], P('ep', None, 'tp'), may hold values from -0.125 to 0.125
- down_weight: bfloat16 [64, 1024, 2048], P('ep', 'tp'), may hold values from -0.1875 to 0.1875
Outputs:
- mixer_output: bfloat16 [32768, 2048], P(('ep', 'tp'))
- expert_output: bfloat16 [24576, 2048], P(('ep', 'tp'))
Inputs may be any that keep to these rules, and one draw needn't show every extreme that they name: `routes`: each row names two different experts. In each aligned block of 96 rows no expert is named more than 6 times, a bound that some block reaches.
All inputs are finite; a program needn't handle non-finite values.
Results may differ from a plain program's by a relative error of at most 0.01.
Values may be sent and summed in bfloat16 or wider, within the bound.
No kernel may reach another device: no remote copies, remote signals or barrier semaphores. Data moves between devices by JAX's collectives and lax.ppermute only.
A program may use at most 64 MiB of HBM per device.

v0:
```python
import jax
import jax.numpy as jnp
from jax import lax
from jax.sharding import PartitionSpec as P

RIM = 15


EPS = 1e-06


def passed_along(value, axis, steps):
    count = lax.axis_size(axis)
    leading, last = (max(0, -steps), min(count, count - steps))
    return lax.ppermute(value, axis, [(source, source + steps) for source in range(leading, last)])


def norm_rows(values, gain):
    floats = values.astype(jnp.float32)
    scale = lax.rsqrt(jnp.mean(floats * floats, axis=-1, keepdims=True) + EPS)
    return (floats * scale * gain.astype(jnp.float32)).astype(jnp.bfloat16)


def route_weights(rows, group_router, expert_router, route_rows):
    group_logits = jnp.dot(rows, group_router, preferred_element_type=jnp.float32)
    expert_logits = jnp.dot(rows, expert_router, preferred_element_type=jnp.float32)
    groups = group_logits.shape[1]
    experts = expert_logits.shape[1]
    member = (
        jnp.arange(experts, dtype=jnp.int32)[:, None] // (experts // groups)
        == jnp.arange(groups, dtype=jnp.int32)[None, :]
    ).astype(jnp.float32)
    group_exp = jnp.exp(group_logits)
    group_prob = group_exp / jnp.sum(group_exp, axis=1, keepdims=True)
    expert_exp = jnp.exp(expert_logits)
    within = jnp.dot(expert_exp, member, precision=lax.Precision.HIGHEST)
    prob = expert_exp * jnp.dot(group_prob / within, member.T, precision=lax.Precision.HIGHEST)
    chosen = (route_rows[:, :, None] == jnp.arange(experts, dtype=jnp.int32)[None, None, :]).astype(
        jnp.float32
    )
    picked = jnp.sum(chosen * prob[:, None, :], axis=2)
    return picked / jnp.sum(picked, axis=1, keepdims=True)


def mixer_half(mixer_input, mixer_gain, pool_in, pool_map, pool_scale, pool_out):
    normed = norm_rows(mixer_input, mixer_gain)
    pooled_in = jnp.dot(normed, pool_in, preferred_element_type=jnp.float32).astype(jnp.bfloat16)
    local_rows = pooled_in.shape[0]
    groups_here = pool_map.shape[0]
    channels = pool_map.shape[1]
    border = passed_along(pooled_in[local_rows - RIM :], "ep", 1)
    padded = jnp.concatenate([border, pooled_in], axis=0).astype(jnp.float32)
    padded = padded.reshape(local_rows + RIM, groups_here, channels)
    leading = lax.axis_index("tp") * groups_here
    windows = jnp.left_shift(jnp.int32(2), leading + jnp.arange(groups_here, dtype=jnp.int32))
    window_sum = jnp.zeros((local_rows, groups_here, channels), jnp.float32)
    for offset in range(RIM + 1):
        active = (offset < windows).astype(jnp.float32)
        window_sum = (
            window_sum + padded[RIM - offset : RIM - offset + local_rows] * active[None, :, None]
        )
    position = lax.axis_index("ep") * local_rows + jnp.arange(local_rows, dtype=jnp.int32)
    counts_here = jnp.minimum(position[:, None] + 1, windows[None, :]).astype(jnp.float32)
    pooled = (window_sum / counts_here[:, :, None] - padded[RIM:]).astype(jnp.bfloat16)
    mapped = jnp.einsum("tgc,gce->tge", pooled, pool_map, preferred_element_type=jnp.float32)
    mixed_rows = (
        mapped.reshape(local_rows, groups_here * channels) * pool_scale.astype(jnp.float32)
    ).astype(jnp.bfloat16)
    return lax.psum_scatter(
        jnp.dot(mixed_rows, pool_out, preferred_element_type=jnp.float32).astype(jnp.bfloat16),
        "tp",
        scatter_dimension=0,
        tiled=True,
    )


def slot_positions(route_rows, blocks, experts):
    flat = route_rows.reshape(blocks, -1)
    onehot = (flat[:, :, None] == jnp.arange(experts, dtype=jnp.int32)[None, None, :]).astype(
        jnp.int32
    )
    before = jnp.cumsum(onehot, axis=1) - onehot
    return (jnp.sum(before * onehot, axis=2), flat)


def dispatch_rows(normed, route_rows, blocks, slots_each, experts):
    block_len = normed.shape[0] // blocks
    positions, flat = slot_positions(route_rows, blocks, experts)
    block_index = jnp.arange(blocks, dtype=jnp.int32)[:, None]
    slot_index = block_index * slots_each + positions
    token_index = block_index * block_len + jnp.arange(2 * block_len, dtype=jnp.int32)[None, :] // 2
    table = jnp.full((blocks * slots_each, experts), -1, jnp.int32)
    table = table.at[slot_index.reshape(-1), flat.reshape(-1)].set(token_index.reshape(-1))
    fetched = normed[jnp.maximum(table, 0)]
    return jnp.where((table >= 0)[:, :, None], fetched, jnp.zeros_like(fetched))


def expert_half(
    expert_input,
    expert_gain,
    group_router,
    expert_router,
    routes,
    gate_weight,
    up_weight,
    down_weight,
):
    normed = norm_rows(expert_input, expert_gain)
    tp_count = lax.axis_size("tp")
    tp_place = lax.axis_index("tp")
    experts = expert_router.shape[1]
    block_len = normed.shape[0] // tp_count
    slots_each = 4 * block_len // experts
    own_rows = lax.dynamic_slice_in_dim(normed, tp_place * block_len, block_len, 0)
    own_routes = lax.dynamic_slice_in_dim(routes, tp_place * block_len, block_len, 0)
    sending = dispatch_rows(own_rows, own_routes, 1, slots_each, experts)
    arrived = lax.all_to_all(sending, "ep", split_axis=1, concat_axis=1, tiled=True)
    received = lax.all_gather(arrived, "tp", axis=0, tiled=True)
    held = gate_weight.shape[0]
    model = received.shape[2]
    down_whole = lax.all_gather(down_weight, "tp", axis=1, tiled=True)
    all_slots = received.reshape(received.shape[0], -1, held, model)
    gate = jnp.einsum("csed,edh->cseh", all_slots, gate_weight, preferred_element_type=jnp.float32)
    upward = jnp.einsum("csed,edh->cseh", all_slots, up_weight, preferred_element_type=jnp.float32)
    hidden = (jax.nn.silu(gate) * upward).astype(jnp.bfloat16)
    swapped = lax.all_to_all(hidden, "tp", split_axis=0, concat_axis=3, tiled=True)
    hid_part = hidden.shape[3]
    total = jnp.zeros((swapped.shape[0], swapped.shape[1], held, model), jnp.float32)
    for part in range(tp_count):
        partial_value = jnp.einsum(
            "cseh,ehd->csed",
            swapped[:, :, :, part * hid_part : (part + 1) * hid_part],
            down_whole[:, part * hid_part : (part + 1) * hid_part],
            preferred_element_type=jnp.float32,
        ).astype(jnp.bfloat16)
        partial_value = lax.optimization_barrier(partial_value)
        total = total + partial_value.astype(jnp.float32)
    summed = total.astype(jnp.bfloat16).reshape(slots_each, -1, model)
    returned = lax.all_to_all(summed, "ep", split_axis=1, concat_axis=1, tiled=True)
    positions, flat = slot_positions(own_routes, 1, experts)
    lookup = positions[0] * experts + flat[0]
    picked = (
        returned.reshape(slots_each * experts, model)[lookup]
        .astype(jnp.float32)
        .reshape(block_len, 2, model)
    )
    weights = route_weights(own_rows, group_router, expert_router, own_routes)
    return jnp.sum(picked * weights[:, :, None], axis=1).astype(jnp.bfloat16)


def on_device(
    mixer_input,
    mixer_gain,
    pool_in,
    pool_map,
    pool_scale,
    pool_out,
    expert_input,
    expert_gain,
    group_router,
    expert_router,
    routes,
    gate_weight,
    up_weight,
    down_weight,
):
    mixer_output = mixer_half(mixer_input, mixer_gain, pool_in, pool_map, pool_scale, pool_out)
    expert_output = expert_half(
        expert_input,
        expert_gain,
        group_router,
        expert_router,
        routes,
        gate_weight,
        up_weight,
        down_weight,
    )
    return (mixer_output, expert_output)


def solution(mesh):
    return jax.shard_map(
        on_device,
        mesh=mesh,
        in_specs=(
            P("ep", None),
            P(),
            P(None, "tp"),
            P("tp", None, None),
            P("tp"),
            P("tp", None),
            P("ep", None),
            P(),
            P(),
            P(),
            P("ep", None),
            P("ep", None, "tp"),
            P("ep", None, "tp"),
            P("ep", "tp", None),
        ),
        out_specs=(P(("ep", "tp"), None), P(("ep", "tp"), None)),
        check_vma=False,
    )
```

profile of v0, /device:TPU:8, one launch (start us, length us, event | category | flops | bytes accessed | tf_op | source)
XLA Modules:
  0.0 302.8 jit_solution(5306408200580199578)
XLA Ops:
  9.5 1.8 multiply_reduce_fusion
  11.3 2.0 convert_element_type.227
  13.9 9.3 %scatter_fusion = s32[6,64]{1,0:T(8,128)S(1)} fusion(s32[6,64]{1,0:T(8,128)S(1)} %broadcast_in_dim.11, s32[192]{0:T(256)S(1)} %bitcast.129, s32[192]{0:T(256)S(1)} %and_select_fusion.1), kind=kCustom, calls=%fused_computation.2 | custom fusion | bytes 3840 | tf_op jit(solution)/shard_map/scatter | solution.py:93
  24.8 2.5 gather_fusion
  28.2 63.1 %all_to_all.28 = bf16[6,64,2048]{2,0,1:T(8,128)(2,1)S(1)} all-to-all(bf16[6,64,2048]{2,0,1:T(8,128)(2,1)S(1)} %copy_select_fusion), channel_id=1, replica_groups=mesh['ep'=64,'tp'=4] {'ep'}, dimensions={1} | all-to-all | bytes 3145728 | tf_op jit(solution)/shard_map/all_to_all | solution.py:117
  91.4 2.0 copy.48
  97.1 1.9 collective-permute-start
  99.1 58.8 %all-gather.3.cloned.1.call-done = bf16[24,64,2048]{2,1,0:T(8,128)(2,1)} async-done(((bf16[6,64,2048]{2,1,0:T(8,128)(2,1)}), bf16[24,64,2048]{2,1,0:T(8,128)(2,1)}) %all-gather.3.cloned.1.call-update) | async-done | bytes 6291472 | tf_op jit(solution)/shard_map/all_gather | solution.py:118
  157.9 5.1 %fusion.23 = f32[24,64,256]{2,1,0:T(8,128)S(1)} fusion(bf16[24,64,2048]{2,1,0:T(8,128)(2,1)} %all-gather.3.cloned.1.call-done, bf16[1,2048,256]{2,1,0:T(8,128)(2,1)} %param.25), kind=kOutput, calls=%fused_computation.46 | convolution fusion | flops 1610612736 | bytes 8912896 | tf_op jit(solution)/shard_map/csed,edh->cseh/dot_general | solution.py:123
  163.1 3.0 fusion.16
  166.1 3.8 %all-to-all-start.1 = ((bf16[24,64,1,256]{3,1,2,0:T(8,128)(2,1)}), bf16[24,64,1,256]{3,1,2,0:T(8,128)(2,1)S(1)}, u32[]{:S(2)}, u32[]{:S(2)}) async-start(bf16[24,64,1,256]{3,1,2,0:T(8,128)(2,1)} %fusion.16), calls=%async_computation.2 | async-start | bytes 1572864 | tf_op jit(solution)/shard_map/all_to_all | solution.py:126
  170.0 3.3 %convolution_convert_fusion = bf16[512,2048]{1,0:T(8,128)(2,1)} fusion(bf16[256,2048]{1,0:T(8,128)(2,1)S(1)} %copy-done, f32[256]{0:T(256)S(1)} %convert_element_type.223, f32[527,256]{1,0:T(8,128)S(1)} %maximum_convert_fusion, f32[512]{0:T(512)S(1)} %minimum_convert_fusion, f32[]{:T(128)S(6)} %convert_element_type.220, f32[]{:T(128)S(6)} %convert_element_type.219, ...), kind=kOutput, calls=%fused_computation.10 | convolution fusion | flops 609746944 | bytes 11668544 | tf_op jit(solution)/shard_map/dot_general | solution.py:70
  173.4 14.8 %all-to-all-done.1 = bf16[24,64,1,256]{3,1,2,0:T(8,128)(2,1)S(1)} async-done(((bf16[24,64,1,256]{3,1,2,0:T(8,128)(2,1)}), bf16[24,64,1,256]{3,1,2,0:T(8,128)(2,1)S(1)}, u32[]{:S(2)}, u32[]{:S(2)}) %all-to-all-start.1) | async-done | bytes 786464 | tf_op jit(solution)/shard_map/all_to_all | solution.py:126
  189.4 26.5 %all-gather.5.cloned.1.call-done = bf16[1,1024,2048]{2,1,0:T(8,128)(2,1)} async-done(((bf16[1,256,2048]{2,1,0:T(8,128)(2,1)}), bf16[1,1024,2048]{2,1,0:T(8,128)(2,1)}) %all-gather.5.cloned.1.call-update) | async-done | bytes 4194320 | tf_op jit(solution)/shard_map/all_gather | solution.py:121
  215.8 2.0 fusion.3
  217.8 1.8 fusion.4
  220.8 1.4 fusion.11
  222.2 2.2 copy.51
  224.4 10.9 %all-to-all-start.2 = ((bf16[6,64,2048]{2,0,1:T(8,128)(2,1)}), bf16[6,64,2048]{2,0,1:T(8,128)(2,1)}, u32[]{:S(2)}, u32[]{:S(2)}) async-start(bf16[6,64,2048]{2,0,1:T(8,128)(2,1)} %copy.51), calls=%async_computation.3 | async-start | bytes 4194304 | tf_op jit(solution)/shard_map/all_to_all | solution.py:139
  236.5 49.9 %all-to-all-done.2 = bf16[6,64,2048]{2,0,1:T(8,128)(2,1)} async-done(((bf16[6,64,2048]{2,0,1:T(8,128)(2,1)}), bf16[6,64,2048]{2,0,1:T(8,128)(2,1)}, u32[]{:S(2)}, u32[]{:S(2)}) %all-to-all-start.2) | async-done | bytes 1572896 | tf_op jit(solution)/shard_map/all_to_all | solution.py:139
  286.4 2.5 copy.52
  288.9 2.1 gather_fusion.1
  290.9 2.1 reshape.556
  293.1 3.1 %multiply_reduce_fusion.1 = bf16[96,2048]{1,0:T(8,128)(2,1)} fusion(f32[96,2,2048]{2,1,0:T(2,128)S(1)} %reshape.556, f32[96,2]{1,0:T(8,128)S(1)} %copy.53), kind=kLoop, calls=%fused_computation.31 | loop fusion | flops 589824 | bytes 1966848 | tf_op jit(solution)/shard_map/reduce_sum | solution.py:148
  (88 shorter events, 12.7 us)
Async XLA Ops:
  7.2 162.9 %copy-start = (bf16[256,2048]{1,0:T(8,128)(2,1)S(1)}, bf16[256,2048]{1,0:T(8,128)(2,1)}, u32[]{:S(2)}) copy-start(bf16[256,2048]{1,0:T(8,128)(2,1)} %param.19) | copy-start | bytes 3145732
  7.2 4.2 %copy-start.1 = (bf16[384,2048]{1,0:T(8,128)(2,1)S(1)}, bf16[384,2048]{1,0:T(8,128)(2,1)}, u32[]{:S(2)}) copy-start(bf16[384,2048]{1,0:T(8,128)(2,1)} %param.20) | copy-start | bytes 4718596
  7.2 150.7 %all-gather.3.cloned.1.call-start = ((), (), s32[]{:S(2)}) async-start(), calls=%async_computation.5 | async-start | bytes 7864320 | tf_op jit(solution)/shard_map/all_gather | solution.py:118
  13.4 10.0 %copy-start.8 = (bf16[2048]{0:T(1024)(128)(2,1)S(1)}, bf16[2048]{0:T(1024)(128)(2,1)}, u32[]{:S(2)}) copy-start(bf16[2048]{0:T(1024)(128)(2,1)} %param.21) | copy-start | bytes 12292
  93.4 0.8 copy-start.9
  93.4 1.6 copy-start.3
  93.4 122.4 %all-gather.5.cloned.1.call-start = ((), (), s32[]{:S(2)}) async-start(), calls=%async_computation.6 | async-start | bytes 5242880 | tf_op jit(solution)/shard_map/all_gather | solution.py:121
  94.2 1.4 copy-start.11
  95.6 3.5 %copy-start.14 = (bf16[256]{0:T(256)(128)(2,1)S(1)}, bf16[256]{0:T(256)(128)(2,1)}, u32[]{:S(2)}) copy-start(bf16[256]{0:T(256)(128)(2,1)} %param.18) | copy-start | bytes 1540
  96.4 0.7 copy-start.4
  97.1 72.9 %collective-permute-start = (bf16[15,256]{1,0:T(8,128)(2,1)S(1)}, bf16[15,256]{1,0:T(8,128)(2,1)S(1)}, u32[]{:S(2)}, u32[]{:S(2)}) collective-permute-start(bf16[15,256]{1,0:T(8,128)(2,1)S(1)} %slice.135), channel_id=1, source_target_pairs={{0,4},{4,8},{8,12},{12,16},{16,20},{20,24},{24,28},{28,32},{32,36}... | collective-permute-start | bytes 23048 | tf_op jit(solution)/shard_map/ppermute | solution.py:15
  157.9 5.1 %copy-start.10 = (bf16[24,64,2048]{2,1,0:T(8,128)(2,1)S(1)}, bf16[24,64,2048]{2,1,0:T(8,128)(2,1)}, u32[]{:S(2)}) copy-start(bf16[24,64,2048]{2,1,0:T(8,128)(2,1)} %all-gather.3.cloned.1.call-done) | copy-start | bytes 18874372
  157.9 5.1 %copy-start.12 = (bf16[1,2048,256]{2,1,0:T(8,128)(2,1)S(1)}, bf16[1,2048,256]{2,1,0:T(8,128)(2,1)}, u32[]{:S(2)}) copy-start(bf16[1,2048,256]{2,1,0:T(8,128)(2,1)} %param.26) | copy-start | bytes 3145732
  163.1 6.9 %copy-start.5 = (bf16[512,256]{1,0:T(8,128)(2,1)S(1)}, bf16[512,256]{1,0:T(8,128)(2,1)}, u32[]{:S(2)}) copy-start(bf16[512,256]{1,0:T(8,128)(2,1)} %copy-done.4) | copy-start | bytes 786436
  166.1 4.0 %copy-start.13 = (bf16[1,256,256]{2,1,0:T(8,128)(2,1)S(1)}, bf16[1,256,256]{2,1,0:T(8,128)(2,1)}, u32[]{:S(2)}) copy-start(bf16[1,256,256]{2,1,0:T(8,128)(2,1)} %param.17) | copy-start | bytes 393220
  166.1 22.1 %all-to-all-start.1 = ((bf16[24,64,1,256]{3,1,2,0:T(8,128)(2,1)}), bf16[24,64,1,256]{3,1,2,0:T(8,128)(2,1)S(1)}, u32[]{:S(2)}, u32[]{:S(2)}) async-start(bf16[24,64,1,256]{3,1,2,0:T(8,128)(2,1)} %fusion.16), calls=%async_computation.2 | async-start | bytes 1572864 | tf_op jit(solution)/shard_map/all_to_all | solution.py:126
  169.9 126.4 %reduce-scatter.2.cloned.1.call-start = ((), (), s32[]{:S(2)}) async-start(), calls=%async_computation.4 | async-start | bytes 2621440 | tf_op jit(solution)/shard_map/reduce_scatter | solution.py:69
  215.8 3.8 %copy-start.2 = (bf16[1,1024,2048]{2,1,0:T(8,128)(2,1)S(1)}, bf16[1,1024,2048]{2,1,0:T(8,128)(2,1)}, u32[]{:S(2)}) copy-start(bf16[1,1024,2048]{2,1,0:T(8,128)(2,1)} %all-gather.5.cloned.1.call-done) | copy-start | bytes 12582916
  224.4 10.9 %copy-start.7 = (bf16[2048,4]{0,1:T(4,128)(2,1)S(1)}, bf16[2048,4]{0,1:T(4,128)(2,1)}, u32[]{:S(2)}) copy-start(bf16[2048,4]{0,1:T(4,128)(2,1)} %param.22) | copy-start | bytes 49156
  224.4 11.2 %copy-start.6 = (bf16[2048,64]{0,1:T(8,128)(2,1)S(1)}, bf16[2048,64]{0,1:T(8,128)(2,1)}, u32[]{:S(2)}) copy-start(bf16[2048,64]{0,1:T(8,128)(2,1)} %param.23) | copy-start | bytes 786436
  224.4 62.0 %all-to-all-start.2 = ((bf16[6,64,2048]{2,0,1:T(8,128)(2,1)}), bf16[6,64,2048]{2,0,1:T(8,128)(2,1)}, u32[]{:S(2)}, u32[]{:S(2)}) async-start(bf16[6,64,2048]{2,0,1:T(8,128)(2,1)} %copy.51), calls=%async_computation.3 | async-start | bytes 4194304 | tf_op jit(solution)/shard_map/all_to_all | solution.py:139
Sparse Core Ops, SparseCore 0:
  93.5 64.3 all-gather.2
  159.7 56.0 all-gather.4
  219.0 31.9 reduce-scatter.1
where the time goes:
time: 303 us
  waiting for transfers between devices  151 us (50%)
  blocking collectives  63.1 us (21%)
  local copies, waits for them, and re-layouts  27.7 us (9%)
  matrix products  18 us (6%)
  starting transfers between devices  16.7 us (6%)
  between operations  14.2 us (5%)
  other arithmetic  12.1 us (4%)
    all_to_all x1, blocking collectives, expert_half(): lax.all_to_all(sending, 'ep', split_axis=1, concat_axis=1, tiled=True)  63.1 us
    all_gather x1, waiting for transfers between devices, expert_half(): received = lax.all_gather(arrived, 'tp', axis=0, tiled=True)  58.8 us
    all_to_all x1, waiting for transfers between devices, expert_half(): lax.all_to_all(summed, 'ep', split_axis=1, concat_axis=1, tiled=True)  49.9 us
    all_gather x1, waiting for transfers between devices, expert_half(): down_whole = lax.all_gather(down_weight, 'tp', axis=1, tiled=True)  26.5 us
    all_to_all x1, waiting for transfers between devices, expert_half(): lax.all_to_all(hidden, 'tp', split_axis=0, concat_axis=3, tiled=True)  14.8 us
    all_to_all x1, starting transfers between devices, expert_half(): lax.all_to_all(summed, 'ep', split_axis=1, concat_axis=1, tiled=True)  10.9 us
    scatter x1, local copies, waits for them, and re-layouts, dispatch_rows(): table.at[slot_index.reshape(-1), flat.reshape(-1)]  9.28 us
  transfers between devices with their start and end apart: 6, of which 4 were waited for; matrix products, arithmetic and copies ran while one was open for 11% of the time, Pallas kernels for 0%

commit v1 on v0

v1 whole, which is shorter than its diff:
```python
import jax
import jax.numpy as jnp
from jax import lax
from jax.experimental import pallas as pl
from jax.sharding import PartitionSpec as P


RIM = 15
EPS = 1e-06
CHUNKS = 1
WIDTHS = (1024, 1024)


def passed_along(value, axis, steps):
    count = lax.axis_size(axis)
    leading, last = (max(0, -steps), min(count, count - steps))
    return lax.ppermute(value, axis, [(source, source + steps) for source in range(leading, last)])


def swapped(value, mask):
    count = lax.axis_size("tp")
    return lax.ppermute(value, "tp", [(source, source ^ mask) for source in range(count)])


def norm_rows(values, gain):
    floats = values.astype(jnp.float32)
    scale = lax.rsqrt(jnp.mean(floats * floats, axis=-1, keepdims=True) + EPS)
    return (floats * scale * gain.astype(jnp.float32)).astype(jnp.bfloat16)


def mixer_partial(mixer_input, mixer_gain, pool_in, pool_map, pool_scale, pool_out):
    normed = norm_rows(mixer_input, mixer_gain)
    pooled_in = jnp.dot(normed, pool_in, preferred_element_type=jnp.float32).astype(jnp.bfloat16)
    local_rows = pooled_in.shape[0]
    groups_here = pool_map.shape[0]
    channels = pool_map.shape[1]
    border = passed_along(pooled_in[local_rows - RIM :], "ep", 1)
    padded = jnp.concatenate([border, pooled_in], axis=0).astype(jnp.float32)
    padded = padded.reshape(local_rows + RIM, groups_here, channels)
    leading = lax.axis_index("tp") * groups_here
    windows = jnp.left_shift(jnp.int32(2), leading + jnp.arange(groups_here, dtype=jnp.int32))
    window_sum = jnp.zeros((local_rows, groups_here, channels), jnp.float32)
    for offset in range(RIM + 1):
        active = (offset < windows).astype(jnp.float32)
        window_sum = (
            window_sum + padded[RIM - offset : RIM - offset + local_rows] * active[None, :, None]
        )
    position = lax.axis_index("ep") * local_rows + jnp.arange(local_rows, dtype=jnp.int32)
    counts_here = jnp.minimum(position[:, None] + 1, windows[None, :]).astype(jnp.float32)
    pooled = (window_sum / counts_here[:, :, None] - padded[RIM:]).astype(jnp.bfloat16)
    mapped = jnp.einsum("tgc,gce->tge", pooled, pool_map, preferred_element_type=jnp.float32)
    mixed_rows = (
        mapped.reshape(local_rows, groups_here * channels) * pool_scale.astype(jnp.float32)
    ).astype(jnp.bfloat16)
    return jnp.dot(mixed_rows, pool_out, preferred_element_type=jnp.float32).astype(jnp.bfloat16)


def mixer_reduce(partial_rows):
    count = lax.axis_size("tp")
    place = lax.axis_index("tp")
    rows = partial_rows.shape[0] // count

    def piece(k):
        return lax.dynamic_slice_in_dim(partial_rows, (place ^ k) * rows, rows, 0)

    total = piece(0).astype(jnp.float32)
    for k in range(1, count):
        total = total + swapped(piece(k), k).astype(jnp.float32)
    return total.astype(jnp.bfloat16)


def dispatch_kernel(x_ref, gain_ref, routes_ref, *outs):
    normed_ref, pick_ref = outs[0], outs[1]
    payloads = outs[2:]
    tokens = x_ref.shape[0]
    floats = x_ref[...].astype(jnp.float32)
    scale = lax.rsqrt(jnp.mean(floats * floats, axis=-1, keepdims=True) + EPS)
    normed = (floats * scale * gain_ref[...].astype(jnp.float32)).astype(jnp.bfloat16)
    normed_ref[...] = normed
    routes = routes_ref[...]
    slots = pick_ref.shape[2]
    experts = 64
    each = slots // experts
    expert = lax.broadcasted_iota(jnp.int32, (tokens, experts), 1)
    first = routes[:, 0:1] == expert
    second = routes[:, 1:2] == expert
    named = jnp.where(first | second, 1.0, 0.0)
    earlier = lax.broadcasted_iota(jnp.int32, (tokens, tokens), 1) < lax.broadcasted_iota(
        jnp.int32, (tokens, tokens), 0
    )
    before = jnp.dot(
        jnp.where(earlier, 1.0, 0.0).astype(jnp.bfloat16),
        named.astype(jnp.bfloat16),
        preferred_element_type=jnp.float32,
    )
    spread = lax.broadcasted_iota(jnp.int32, (experts, slots), 1) // each == lax.broadcasted_iota(
        jnp.int32, (experts, slots), 0
    )
    spread = jnp.where(spread, 1.0, 0.0).astype(jnp.bfloat16)
    within = (lax.broadcasted_iota(jnp.int32, (tokens, slots), 1) % each).astype(jnp.float32)
    chosen = []
    for mask in (first, second):
        place = jnp.where(mask, before, -1.0).astype(jnp.bfloat16)
        spread_place = jnp.dot(place, spread, preferred_element_type=jnp.float32)
        chosen.append(jnp.where(spread_place == within, 1.0, 0.0))
    pick_ref[0] = chosen[0].astype(jnp.bfloat16)
    pick_ref[1] = chosen[1].astype(jnp.bfloat16)
    either = (chosen[0] + chosen[1]).astype(jnp.bfloat16)
    for index, out in enumerate(payloads):
        width = out.shape[1]
        out[...] = lax.dot_general(
            either,
            normed[:, index * width : (index + 1) * width],
            (((0,), (0,)), ((), ())),
            preferred_element_type=jnp.float32,
        ).astype(jnp.bfloat16)


def dispatch(x, gain, routes, experts, slots_each):
    tokens, model = x.shape
    slots = experts * slots_each
    return pl.pallas_call(
        dispatch_kernel,
        out_shape=[
            jax.ShapeDtypeStruct((tokens, model), jnp.bfloat16),
            jax.ShapeDtypeStruct((2, tokens, slots), jnp.bfloat16),
        ]
        + [jax.ShapeDtypeStruct((slots, model // CHUNKS), jnp.bfloat16)] * CHUNKS,
        name="dispatch",
    )(x, gain.reshape(1, model), routes)


def route_weights(rows, group_router, expert_router, route_rows):
    group_logits = jnp.dot(rows, group_router, preferred_element_type=jnp.float32)
    expert_logits = jnp.dot(rows, expert_router, preferred_element_type=jnp.float32)
    groups = group_logits.shape[1]
    experts = expert_logits.shape[1]
    member = (
        jnp.arange(experts, dtype=jnp.int32)[:, None] // (experts // groups)
        == jnp.arange(groups, dtype=jnp.int32)[None, :]
    ).astype(jnp.float32)
    group_exp = jnp.exp(group_logits)
    group_prob = group_exp / jnp.sum(group_exp, axis=1, keepdims=True)
    expert_exp = jnp.exp(expert_logits)
    within = jnp.dot(expert_exp, member, precision=lax.Precision.HIGHEST)
    prob = expert_exp * jnp.dot(group_prob / within, member.T, precision=lax.Precision.HIGHEST)
    chosen = (route_rows[:, :, None] == jnp.arange(experts, dtype=jnp.int32)[None, None, :]).astype(
        jnp.float32
    )
    picked = jnp.sum(chosen * prob[:, None, :], axis=2)
    return picked / jnp.sum(picked, axis=1, keepdims=True)


def combine_kernel(returned_ref, pick_ref, weight_ref, *refs):
    out_ref = refs[-1]
    returned = returned_ref[...]
    weight = weight_ref[...]
    total = jnp.dot(pick_ref[0], returned, preferred_element_type=jnp.float32) * weight[:, 0:1]
    total = total + jnp.dot(pick_ref[1], returned, preferred_element_type=jnp.float32) * weight[:, 1:2]
    out_ref[...] = total.astype(jnp.bfloat16)


def combine(returned, pick, weight, index, so_far):
    width = returned.shape[1]
    tokens = pick.shape[1]
    whole = [
        pl.BlockSpec(array.shape, lambda i, n=array.ndim: (0,) * n)
        for array in (returned, pick, weight)
    ]
    extra = [] if so_far is None else [so_far]
    return pl.pallas_call(
        combine_kernel,
        grid=(1,),
        in_specs=whole + [pl.BlockSpec(memory_space=pl.ANY)] * len(extra),
        out_specs=pl.BlockSpec((tokens, width), lambda i: (0, index)),
        out_shape=jax.ShapeDtypeStruct((tokens, sum(WIDTHS)), jnp.bfloat16),
        input_output_aliases={3: 0} if extra else {},
        name="combine",
    )(returned, pick, weight, *extra)


def hidden_kernel(rows_ref, *refs):
    gate_refs, up_refs, out_ref = refs[: len(refs) // 2], refs[len(refs) // 2 : -1], refs[-1]

    def product(parts):
        total, start = None, 0
        for part in parts:
            depth = part.shape[0]
            piece = jnp.dot(
                rows_ref[:, start : start + depth], part[...], preferred_element_type=jnp.float32
            )
            start += depth
            total = piece if total is None else total + piece
        return total

    gate = product(gate_refs)
    out_ref[...] = (gate / (1.0 + jnp.exp(-gate)) * product(up_refs)).astype(jnp.bfloat16)


def hidden_of(rows, gate_parts, up_parts):
    units = gate_parts[0].shape[1]
    return pl.pallas_call(
        hidden_kernel,
        out_shape=jax.ShapeDtypeStruct((rows.shape[0], units), jnp.bfloat16),
        cost_estimate=pl.CostEstimate(
            flops=4 * rows.shape[0] * rows.shape[1] * units, bytes_accessed=4 << 20, transcendentals=0
        ),
        name="hidden",
    )(rows, *gate_parts, *up_parts)


def down_kernel(hidden_refs, down_refs, base_ref, out_ref):
    total = None if base_ref is None else base_ref[...]
    index, start = 0, 0
    for part in down_refs:
        depth = part.shape[0]
        piece = jnp.dot(
            hidden_refs[index][:, start : start + depth],
            part[...],
            preferred_element_type=jnp.float32,
        )
        total = piece if total is None else total + piece
        start += depth
        if start == hidden_refs[index].shape[1]:
            index, start = index + 1, 0
    out_ref[...] = total.astype(out_ref.dtype)


def down_of(hidden, parts, base, dtype):
    rows, width = hidden[0].shape[0], parts[0].shape[1]
    depth = sum(part.shape[0] for part in parts)
    bases = [] if base is None else [base]

    def kernel(*refs):
        refs = list(refs)
        hidden_refs, rest = refs[: len(hidden)], refs[len(hidden) :]
        down_refs, rest = rest[: len(parts)], rest[len(parts) :]
        down_kernel(hidden_refs, down_refs, rest[0] if bases else None, rest[-1])

    return pl.pallas_call(
        kernel,
        out_shape=jax.ShapeDtypeStruct((rows, width), dtype),
        cost_estimate=pl.CostEstimate(
            flops=2 * rows * depth * width, bytes_accessed=4 << 20, transcendentals=0
        ),
        name="down",
    )(*hidden, *parts, *bases)


def exchange(rows, experts):
    slots, width = rows.shape
    each = slots // experts
    moved = lax.all_to_all(
        rows.reshape(experts, each // 2, 2, width), "ep", split_axis=0, concat_axis=0, tiled=True
    )
    return moved.reshape(slots, width)


def layer(
    mixer_input,
    mixer_gain,
    pool_in,
    pool_map,
    pool_scale,
    pool_out,
    expert_input,
    expert_gain,
    group_router,
    expert_router,
    routes,
    gate_weight,
    up_weight,
    down_weight,
):
    tp_count = lax.axis_size("tp")
    tp_place = lax.axis_index("tp")
    experts = expert_router.shape[1]
    block_len = expert_input.shape[0] // tp_count
    slots_each = 4 * block_len // experts

    def near(own):
        return [swapped(own, 1), swapped(own, 3)]

    gates = [gate_weight[0]] + near(gate_weight[0])
    ups = [up_weight[0]] + near(up_weight[0])
    gates.append(swapped(gates[2], 1))
    ups.append(swapped(ups[1], 3))
    downs, start = [], 0
    for width in WIDTHS:
        own = down_weight[0][:, start : start + width]
        start += width
        half = own.shape[0] // 2
        near_a, near_b = near(own)
        far_a = swapped(near_b[:half], 1)
        far_b = swapped(near_a[half:], 3)
        downs.append([own, near_a, near_b, far_a, far_b])

    own_input = lax.dynamic_slice_in_dim(expert_input, tp_place * block_len, block_len, 0)
    own_routes = lax.dynamic_slice_in_dim(routes, tp_place * block_len, block_len, 0)
    normed, pick, payload = dispatch(own_input, expert_gain, own_routes, experts, slots_each)
    rows = exchange(payload, experts)

    partial_rows = mixer_partial(mixer_input, mixer_gain, pool_in, pool_map, pool_scale, pool_out)
    mixer_output = mixer_reduce(partial_rows)
    weight = route_weights(normed, group_router, expert_router, own_routes)

    hidden = []
    for gate_w, up_w in zip(gates, ups):
        hidden.append(hidden_of(rows, [gate_w], [up_w]))
    expert_output = None
    for index, parts in enumerate(downs):
        most = down_of(hidden[:3], parts[:3], None, jnp.float32)
        result = down_of(hidden[3:], parts[3:], most, jnp.bfloat16)
        returned = exchange(result, experts)
        expert_output = combine(returned, pick, weight, index, expert_output)
    return (mixer_output, expert_output)


def solution(mesh):
    return jax.shard_map(
        layer,
        mesh=mesh,
        in_specs=(
            P("ep", None),
            P(),
            P(None, "tp"),
            P("tp", None, None),
            P("tp"),
            P("tp", None),
            P("ep", None),
            P(),
            P(),
            P(),
            P("ep", None),
            P("ep", None, "tp"),
            P("ep", None, "tp"),
            P("ep", "tp", None),
        ),
        out_specs=(P(("ep", "tp"), None), P(("ep", "tp"), None)),
        check_vma=False,
    )
```

time: 303 us -> 240 us (0.79)
  blocking collectives: 63.1 us -> 0 us
  waiting for transfers between devices: 151 us -> 97.6 us
  starting transfers between devices: 16.7 us -> 55.4 us
  Pallas kernels: 0 us -> 35.9 us
  between operations: 14.2 us -> 0.87 us
  other arithmetic: 12.1 us -> 6.1 us
  matrix products: 18 us -> 12.8 us
    ppermute x0 -> x17, waiting for transfers between devices: none -> 97.6 us  [swapped(): lax.ppermute(value, 'tp', [(source, source ^ mask) for source in range(co...]
    all_gather x2 -> x0, waiting for transfers between devices: 85.3 us -> none  [the longest x1 58.8 us: expert_half(): received = lax.all_gather(arrived, 'tp', axis=0, tiled=True)]
    all_to_all x2 -> x3, waiting for transfers between devices: 64.7 us -> 0.01 us  [exchange(): lax.all_to_all(rows.reshape(experts, each // 2, 2, width), 'ep', split_ax...]
    all_to_all x1 -> x0, blocking collectives: 63.1 us -> none  [expert_half(): lax.all_to_all(sending, 'ep', split_axis=1, concat_axis=1, tiled=True)]
    pallas_call x0 -> x11, Pallas kernels: none -> 35.9 us  [the longest x4 14.8 us: hidden_of(): pl.pallas_call(hidden_kernel, out_shape=jax.ShapeDtypeStruct((rows.shape[...]
    ppermute x0 -> x17, starting transfers between devices: none -> 19.7 us  [swapped(): lax.ppermute(value, 'tp', [(source, source ^ mask) for source in range(co...]
    all_to_all x2 -> x3, starting transfers between devices: 14.7 us -> 33.7 us  [exchange(): lax.all_to_all(rows.reshape(experts, each // 2, 2, width), 'ep', split_ax...]
    reshape x2 -> x7, local copies, waits for them, and re-layouts: 2.22 us -> 15.2 us  [the longest x3 9.47 us: exchange(): rows.reshape(experts, each // 2, 2, width)]
  transfers between devices with their start and end apart: 6 -> 21, of which waited for: 4 -> 7; matrix products, arithmetic and copies ran while one was open for 11% -> 16% of each run, Pallas kernels for 0% -> 13%
where the time goes in v1:
time: 240 us; the launch traced here: 238 us
  waiting for transfers between devices  97.6 us (41%)
  starting transfers between devices  55.4 us (23%)
  Pallas kernels  35.9 us (15%)
  local copies, waits for them, and re-layouts  29.6 us (12%)
  matrix products  12.8 us (5%)
  other arithmetic  6.1 us (3%)
    ppermute x17, waiting for transfers between devices, swapped(): lax.ppermute(value, 'tp', [(source, source ^ mask) for source in range(co...  97.6 us
    all_to_all x3, starting transfers between devices, exchange(): lax.all_to_all(rows.reshape(experts, each // 2, 2, width), 'ep', split_ax...  33.7 us
    ppermute x17, starting transfers between devices, swapped(): lax.ppermute(value, 'tp', [(source, source ^ mask) for source in range(co...  19.7 us
    pallas_call x4, Pallas kernels, hidden_of(): pl.pallas_call(hidden_kernel, out_shape=jax.ShapeDtypeStruct((rows.shape[...  14.8 us
    pallas_call x4, Pallas kernels, down_of(): pl.pallas_call(kernel, out_shape=jax.ShapeDtypeStruct((rows, width), dtyp...  13.3 us
    reshape x3, local copies, waits for them, and re-layouts, exchange(): rows.reshape(experts, each // 2, 2, width)  9.47 us
    dot_general x1, matrix products, mixer_partial(): jnp.dot(mixed_rows, pool_out, preferred_element_type=jnp.float32)  8.27 us
  transfers between devices with their start and end apart: 21, of which 7 were waited for; matrix products, arithmetic and copies ran while one was open for 16% of the time, Pallas kernels for 13%

profile of v1, /device:TPU:8, one launch (start us, length us, event | category | flops | bytes accessed | tf_op | source)
XLA Modules:
  0.0 238.2 jit_solution(18138393223982951158)
XLA Ops:
  4.3 3.2 %dispatch.1 = (bf16[96,2048]{1,0:T(8,128)(2,1)}, bf16[2,96,384]{2,1,0:T(8,128)(2,1)}, bf16[384,2048]{1,0:T(8,128)(2,1)}) custom-call(bf16[96,2048]{1,0:T(8,128)(2,1)} %constant_dynamic-slice_fusion.1.x_ref, bf16[1,2048]{1,0:T(2,128)(2,1)} %reshape.266.gain_ref, s32[96,2]{1,0:T(8,128)} %copy.22.routes_ref), custom_call_target="tpu_custom_call" | custom-call | tf_op jit(solution)/shard_map/dispatch/pallas_call | solution.py:122
  7.5 3.7 %reshape.267 = bf16[64,3,2,2048]{3,2,1,0:T(2,128)(2,1)} reshape(bf16[384,2048]{1,0:T(8,128)(2,1)} %get-tuple-element.5) | data formatting | bytes 3145728 | tf_op jit(solution)/shard_map/reshape | solution.py:254
  11.2 12.1 %all-to-all-start = ((bf16[64,3,2,2048]{3,2,1,0:T(2,128)(2,1)}), bf16[64,3,2,2048]{3,2,1,0:T(2,128)(2,1)S(1)}, u32[]{:S(2)}, u32[]{:S(2)}) async-start(bf16[64,3,2,2048]{3,2,1,0:T(2,128)(2,1)} %reshape.267), calls=%async_computation | async-start | bytes 3145728 | tf_op jit(solution)/shard_map/all_to_all | solution.py:253
  23.3 2.8 %collective-permute-start.4 = (bf16[2048,256]{1,0:T(8,128)(2,1)}, bf16[2048,256]{1,0:T(8,128)(2,1)}, u32[]{:S(2)}, u32[]{:S(2)}) collective-permute-start(bf16[2048,256]{1,0:T(8,128)(2,1)} %bitcast.16), channel_id=1, source_target_pairs={{0,3},{1,2},{2,1},{3,0},{4,7},{5,6},{6,5},{7,4},{8,11},{9,10},{10,... | collective-permute-start | bytes 3145736 | tf_op jit(solution)/shard_map/ppermute | solution.py:22
  32.9 18.1 %collective-permute-done.4.refs_0_ = bf16[2048,256]{1,0:T(8,128)(2,1)} collective-permute-done((bf16[2048,256]{1,0:T(8,128)(2,1)}, bf16[2048,256]{1,0:T(8,128)(2,1)}, u32[]{:S(2)}, u32[]{:S(2)}) %collective-permute-start.4) | collective-permute-done | bytes 1048608 | tf_op jit(solution)/shard_map/ppermute | solution.py:22
  53.7 8.4 %collective-permute-done.14.refs_5_ = bf16[256,1024]{1,0:T(8,128)(2,1)S(1)} collective-permute-done((bf16[256,1024]{1,0:T(8,128)(2,1)S(1)}, bf16[256,1024]{1,0:T(8,128)(2,1)S(1)}, u32[]{:S(2)}, u32[]{:S(2)}) %collective-permute-start.14) | collective-permute-done | bytes 524320 | tf_op jit(solution)/shard_map/ppermute | solution.py:22
  63.6 43.9 %collective-permute-done.16.refs_4_ = bf16[256,1024]{1,0:T(8,128)(2,1)S(1)} collective-permute-done((bf16[256,1024]{1,0:T(8,128)(2,1)S(1)}, bf16[256,1024]{1,0:T(8,128)(2,1)S(1)}, u32[]{:S(2)}, u32[]{:S(2)}) %collective-permute-start.16) | collective-permute-done | bytes 524320 | tf_op jit(solution)/shard_map/ppermute | solution.py:22
  110.9 3.7 %hidden.5.refs_0_ = bf16[384,256]{1,0:T(8,128)(2,1)} custom-call(bf16[384,2048]{1,0:T(8,128)(2,1)} %reshape.268.rows_ref, bf16[2048,256]{1,0:T(8,128)(2,1)} %bitcast.18, bf16[2048,256]{1,0:T(8,128)(2,1)} %bitcast.21), custom_call_target="tpu_custom_call" | custom-call | flops 805306368 | bytes 4194304 | tf_op jit(solution)/shard_map/hidden/pallas_call | solution.py:202
  115.4 3.7 %hidden.6.refs_1_ = bf16[384,256]{1,0:T(8,128)(2,1)} custom-call(bf16[384,2048]{1,0:T(8,128)(2,1)} %reshape.268.rows_ref, bf16[2048,256]{1,0:T(8,128)(2,1)} %collective-permute-done.12.refs_0_, bf16[2048,256]{1,0:T(8,128)(2,1)} %collective-permute-done.6.refs_1_), custom_call_target="tpu_custom_call" | custom-call | flops 805306368 | bytes 4194304 | tf_op jit(solution)/shard_map/hidden/pallas_call | solution.py:202
  121.7 3.7 %hidden.7.refs_2_ = bf16[384,256]{1,0:T(8,128)(2,1)} custom-call(bf16[384,2048]{1,0:T(8,128)(2,1)} %reshape.268.rows_ref, bf16[2048,256]{1,0:T(8,128)(2,1)} %collective-permute-done.4.refs_0_, bf16[2048,256]{1,0:T(8,128)(2,1)} %collective-permute-done.13.refs_1_), custom_call_target="tpu_custom_call" | custom-call | flops 805306368 | bytes 4194304 | tf_op jit(solution)/shard_map/hidden/pallas_call | solution.py:202
  125.4 3.5 %down.6.refs_3_ = f32[384,1024]{1,0:T(8,128)} custom-call(bf16[384,256]{1,0:T(8,128)(2,1)} %hidden.5.refs_0_, bf16[384,256]{1,0:T(8,128)(2,1)} %hidden.6.refs_1_, bf16[384,256]{1,0:T(8,128)(2,1)} %hidden.7.refs_2_, bf16[256,1024]{1,0:T(8,128)(2,1)} %copy-done.3, bf16[256,1024]{1,0:T(8,128)(2,1)} %copy-done.6, bf16[256,1024]{1,0:T(8,128)(2,1)} %copy-done.5), custom_call_target="tpu_custom_call" | custom-call | flops 603979776 | bytes 4194304 | tf_op jit(solution)/shard_map/down/pallas_call | solution.py:240
  128.9 3.7 %hidden.4.refs_0_ = bf16[384,256]{1,0:T(8,128)(2,1)} custom-call(bf16[384,2048]{1,0:T(8,128)(2,1)} %reshape.268.rows_ref, bf16[2048,256]{1,0:T(8,128)(2,1)} %collective-permute-done.5.refs_0_, bf16[2048,256]{1,0:T(8,128)(2,1)} %collective-permute-done.7.refs_1_), custom_call_target="tpu_custom_call" | custom-call | flops 805306368 | bytes 4194304 | tf_op jit(solution)/shard_map/hidden/pallas_call | solution.py:202
  134.1 3.1 %down.7 = bf16[384,1024]{1,0:T(8,128)(2,1)} custom-call(bf16[384,256]{1,0:T(8,128)(2,1)} %hidden.4.refs_0_, bf16[128,1024]{1,0:T(8,128)(2,1)} %copy-done.9, bf16[128,1024]{1,0:T(8,128)(2,1)} %copy-done.10, f32[384,1024]{1,0:T(8,128)} %down.6.refs_3_), custom_call_target="tpu_custom_call" | custom-call | flops 201326592 | bytes 4194304 | tf_op jit(solution)/shard_map/down/pallas_call | solution.py:240
  137.2 2.9 %reshape.271 = bf16[64,3,2,1024]{3,2,1,0:T(2,128)(2,1)} reshape(bf16[384,1024]{1,0:T(8,128)(2,1)} %down.7) | data formatting | bytes 1572864 | tf_op jit(solution)/shard_map/reshape | solution.py:254
  140.0 10.3 %all-to-all-start.2 = ((bf16[64,3,2,1024]{3,2,1,0:T(2,128)(2,1)}), bf16[64,3,2,1024]{3,2,1,0:T(2,128)(2,1)S(1)}, u32[]{:S(2)}, u32[]{:S(2)}) async-start(bf16[64,3,2,1024]{3,2,1,0:T(2,128)(2,1)} %reshape.271), calls=%async_computation.2 | async-start | bytes 1572864 | tf_op jit(solution)/shard_map/all_to_all | solution.py:253
  150.4 2.7 %fusion.7 = bf16[512,256]{1,0:T(8,128)(2,1)S(1)} fusion(bf16[2048,256]{1,0:T(8,128)(2,1)} %param.16, bf16[512,2048]{1,0:T(8,128)(2,1)} %param.14, f32[2048]{0:T(1024)S(1)} %convert_element_type.119, f32[512]{0:T(512)S(1)} %add_rsqrt_fusion), kind=kOutput, calls=%fused_computation.10 | convolution fusion | flops 541196288 | bytes 3418112 | tf_op jit(solution)/shard_map/dot_general | solution.py:33
  165.0 3.5 %down.4.refs_3_ = f32[384,1024]{1,0:T(8,128)} custom-call(bf16[384,256]{1,0:T(8,128)(2,1)} %hidden.5.refs_0_, bf16[384,256]{1,0:T(8,128)(2,1)} %hidden.6.refs_1_, bf16[384,256]{1,0:T(8,128)(2,1)} %hidden.7.refs_2_, bf16[256,1024]{1,0:T(8,128)(2,1)} %get-tuple-element.14.refs_3_, bf16[256,1024]{1,0:T(8,128)(2,1)} %collective-permute-done.10.refs_4_, ...), custom_call_target="tpu_custom_call" | custom-call | flops 603979776 | bytes 4194304 | tf_op jit(solution)/shard_map/down/pallas_call | solution.py:240
  168.5 3.8 %collective-permute-done.11.refs_2_ = bf16[128,1024]{1,0:T(8,128)(2,1)S(1)} collective-permute-done((bf16[128,1024]{1,0:T(8,128)(2,1)S(1)}, bf16[128,1024]{1,0:T(8,128)(2,1)S(1)}, u32[]{:S(2)}, u32[]{:S(2)}) %collective-permute-start.11) | collective-permute-done | bytes 262176 | tf_op jit(solution)/shard_map/ppermute | solution.py:22
  173.1 3.1 %down.5 = bf16[384,1024]{1,0:T(8,128)(2,1)} custom-call(bf16[384,256]{1,0:T(8,128)(2,1)} %hidden.4.refs_0_, bf16[128,1024]{1,0:T(8,128)(2,1)} %copy-done.7, bf16[128,1024]{1,0:T(8,128)(2,1)} %copy-done.8, f32[384,1024]{1,0:T(8,128)} %down.4.refs_3_), custom_call_target="tpu_custom_call" | custom-call | flops 201326592 | bytes 4194304 | tf_op jit(solution)/shard_map/down/pallas_call | solution.py:240
  176.2 2.9 %reshape.269 = bf16[64,3,2,1024]{3,2,1,0:T(2,128)(2,1)} reshape(bf16[384,1024]{1,0:T(8,128)(2,1)} %down.5) | data formatting | bytes 1572864 | tf_op jit(solution)/shard_map/reshape | solution.py:254
  179.1 11.3 %all-to-all-start.1 = ((bf16[64,3,2,1024]{3,2,1,0:T(2,128)(2,1)}), bf16[64,3,2,1024]{3,2,1,0:T(2,128)(2,1)S(1)}, u32[]{:S(2)}, u32[]{:S(2)}) async-start(bf16[64,3,2,1024]{3,2,1,0:T(2,128)(2,1)} %reshape.269), calls=%async_computation.1 | async-start | bytes 1572864 | tf_op jit(solution)/shard_map/all_to_all | solution.py:253
  190.4 8.3 %convolution_convert_fusion = bf16[512,2048]{1,0:T(8,128)(2,1)} fusion(bf16[256,2048]{1,0:T(8,128)(2,1)} %param.19, f32[256]{0:T(256)S(1)} %convert_element_type.141, f32[527,256]{1,0:T(8,128)} %maximum_convert_fusion, f32[512]{0:T(512)S(1)} %minimum_convert_fusion, f32[]{:T(128)S(6)} %convert_element_type.138, f32[]{:T(128)S(6)} %convert_element_type.137, ...), kind=kOutput, calls=%fused_computation.5 | convolution fusion | flops 609746944 | bytes 11668544 | tf_op jit(solution)/shard_map/dot_general | solution.py:55
  201.9 3.4 %collective-permute-start.2 = (bf16[128,2048]{1,0:T(8,128)(2,1)}, bf16[128,2048]{1,0:T(8,128)(2,1)}, u32[]{:S(2)}, u32[]{:S(2)}) collective-permute-start(bf16[128,2048]{1,0:T(8,128)(2,1)} %get-tuple-element.12), channel_id=1, source_target_pairs={{0,2},{1,3},{2,0},{3,1},{4,6},{5,7},{6,4},{7,5},{8,10},{9,11},{10,... | collective-permute-start | bytes 1572872 | tf_op jit(solution)/shard_map/ppermute | solution.py:22
  206.4 21.5 %collective-permute-done.3 = bf16[128,2048]{1,0:T(8,128)(2,1)} collective-permute-done((bf16[128,2048]{1,0:T(8,128)(2,1)}, bf16[128,2048]{1,0:T(8,128)(2,1)}, u32[]{:S(2)}, u32[]{:S(2)}) %collective-permute-start.3) | collective-permute-done | bytes 524320 | tf_op jit(solution)/shard_map/ppermute | solution.py:22
  (101 shorter events, 50.2 us)
Async XLA Ops:
  11.2 97.8 %all-to-all-start = ((bf16[64,3,2,2048]{3,2,1,0:T(2,128)(2,1)}), bf16[64,3,2,2048]{3,2,1,0:T(2,128)(2,1)S(1)}, u32[]{:S(2)}, u32[]{:S(2)}) async-start(bf16[64,3,2,2048]{3,2,1,0:T(2,128)(2,1)} %reshape.267), calls=%async_computation | async-start | bytes 3145728 | tf_op jit(solution)/shard_map/all_to_all | solution.py:253
  23.3 39.1 %copy-start.1 = (bf16[512,2048]{1,0:T(8,128)(2,1)S(1)}, bf16[512,2048]{1,0:T(8,128)(2,1)}, u32[]{:S(2)}) copy-start(bf16[512,2048]{1,0:T(8,128)(2,1)} %param.14) | copy-start | bytes 6291460
  23.3 27.6 %collective-permute-start.4 = (bf16[2048,256]{1,0:T(8,128)(2,1)}, bf16[2048,256]{1,0:T(8,128)(2,1)}, u32[]{:S(2)}, u32[]{:S(2)}) collective-permute-start(bf16[2048,256]{1,0:T(8,128)(2,1)} %bitcast.16), channel_id=1, source_target_pairs={{0,3},{1,2},{2,1},{3,0},{4,7},{5,6},{6,5},{7,4},{8,11},{9,10},{10,... | collective-permute-start | bytes 3145736 | tf_op jit(solution)/shard_map/ppermute | solution.py:22
  26.2 26.3 %collective-permute-start.6 = (bf16[2048,256]{1,0:T(8,128)(2,1)}, bf16[2048,256]{1,0:T(8,128)(2,1)}, u32[]{:S(2)}, u32[]{:S(2)}) collective-permute-start(bf16[2048,256]{1,0:T(8,128)(2,1)} %bitcast.19), channel_id=1, source_target_pairs={{0,1},{1,0},{2,3},{3,2},{4,5},{5,4},{6,7},{7,6},{8,9},{9,8},{10,11... | collective-permute-start | bytes 3145736 | tf_op jit(solution)/shard_map/ppermute | solution.py:22
  28.5 79.3 %copy-start.3 = (bf16[256,1024]{1,0:T(8,128)(2,1)}, bf16[256,1024]{1,0:T(8,128)(2,1)S(1)}, u32[]{:S(2)}) copy-start(bf16[256,1024]{1,0:T(8,128)(2,1)S(1)} %get-tuple-element.13.refs_3_) | copy-start | bytes 1572868
  28.5 33.6 %collective-permute-start.14 = (bf16[256,1024]{1,0:T(8,128)(2,1)S(1)}, bf16[256,1024]{1,0:T(8,128)(2,1)S(1)}, u32[]{:S(2)}, u32[]{:S(2)}) collective-permute-start(bf16[256,1024]{1,0:T(8,128)(2,1)S(1)} %get-tuple-element.13.refs_3_), channel_id=1, source_target_pairs={{0,3},{1,2},{2,1},{3,0},{4,7},{5,6},{6,5},{7,4},{8,11},{9,10},{10,... | collective-permute-start | bytes 1572872 | tf_op jit(solution)/shard_map/ppermute | solution.py:22
  29.6 85.1 %collective-permute-start.12 = (bf16[2048,256]{1,0:T(8,128)(2,1)}, bf16[2048,256]{1,0:T(8,128)(2,1)}, u32[]{:S(2)}, u32[]{:S(2)}) collective-permute-start(bf16[2048,256]{1,0:T(8,128)(2,1)} %bitcast.17), channel_id=1, source_target_pairs={{0,1},{1,0},{2,3},{3,2},{4,5},{5,4},{6,7},{7,6},{8,9},{9,8},{10,11... | collective-permute-start | bytes 3145736 | tf_op jit(solution)/shard_map/ppermute | solution.py:22
  30.3 88.8 %collective-permute-start.13 = (bf16[2048,256]{1,0:T(8,128)(2,1)}, bf16[2048,256]{1,0:T(8,128)(2,1)}, u32[]{:S(2)}, u32[]{:S(2)}) collective-permute-start(bf16[2048,256]{1,0:T(8,128)(2,1)} %bitcast.20), channel_id=1, source_target_pairs={{0,3},{1,2},{2,1},{3,0},{4,7},{5,6},{6,5},{7,4},{8,11},{9,10},{10,... | collective-permute-start | bytes 3145736 | tf_op jit(solution)/shard_map/ppermute | solution.py:22
  51.0 77.9 %collective-permute-start.5 = (bf16[2048,256]{1,0:T(8,128)(2,1)}, bf16[2048,256]{1,0:T(8,128)(2,1)}, u32[]{:S(2)}, u32[]{:S(2)}) collective-permute-start(bf16[2048,256]{1,0:T(8,128)(2,1)} %collective-permute-done.4.refs_0_), channel_id=1, source_target_pairs={{0,1},{1,0},{2,3},{3,2},{4,5},{5,4},{6,7},{7,6},{8,9},{9,8},{10,11... | collective-permute-start | bytes 3145736 | tf_op jit(solution)/shard_map/ppermute | solution.py:22
  52.5 76.4 %collective-permute-start.7 = (bf16[2048,256]{1,0:T(8,128)(2,1)}, bf16[2048,256]{1,0:T(8,128)(2,1)}, u32[]{:S(2)}, u32[]{:S(2)}) collective-permute-start(bf16[2048,256]{1,0:T(8,128)(2,1)} %collective-permute-done.6.refs_1_), channel_id=1, source_target_pairs={{0,3},{1,2},{2,1},{3,0},{4,7},{5,6},{6,5},{7,4},{8,11},{9,10},{10,... | collective-permute-start | bytes 3145736 | tf_op jit(solution)/shard_map/ppermute | solution.py:22
  62.1 45.6 %copy-start.5 = (bf16[256,1024]{1,0:T(8,128)(2,1)}, bf16[256,1024]{1,0:T(8,128)(2,1)S(1)}, u32[]{:S(2)}) copy-start(bf16[256,1024]{1,0:T(8,128)(2,1)S(1)} %collective-permute-done.14.refs_5_) | copy-start | bytes 1572868
  62.1 45.4 %collective-permute-start.16 = (bf16[256,1024]{1,0:T(8,128)(2,1)S(1)}, bf16[256,1024]{1,0:T(8,128)(2,1)S(1)}, u32[]{:S(2)}, u32[]{:S(2)}) collective-permute-start(bf16[256,1024]{1,0:T(8,128)(2,1)S(1)} %get-tuple-element.13.refs_3_), channel_id=1, source_target_pairs={{0,1},{1,0},{2,3},{3,2},{4,5},{5,4},{6,7},{7,6},{8,9},{9,8},{10,11... | collective-permute-start | bytes 1572872 | tf_op jit(solution)/shard_map/ppermute | solution.py:22
  107.5 25.2 %collective-permute-start.15 = (bf16[128,1024]{1,0:T(8,128)(2,1)}, bf16[128,1024]{1,0:T(8,128)(2,1)S(1)}, u32[]{:S(2)}, u32[]{:S(2)}) collective-permute-start(bf16[128,1024]{1,0:T(8,128)(2,1)} %slice.130), channel_id=1, source_target_pairs={{0,1},{1,0},{2,3},{3,2},{4,5},{5,4},{6,7},{7,6},{8,9},{9,8},{10,11... | collective-permute-start | bytes 786440 | tf_op jit(solution)/shard_map/ppermute | solution.py:22
  114.7 18.0 %collective-permute-start.17 = (bf16[128,1024]{1,0:T(8,128)(2,1)S(1)}, bf16[128,1024]{1,0:T(8,128)(2,1)S(1)}, u32[]{:S(2)}, u32[]{:S(2)}) collective-permute-start(bf16[128,1024]{1,0:T(8,128)(2,1)S(1)} %copy-done.11), channel_id=1, source_target_pairs={{0,3},{1,2},{2,1},{3,0},{4,7},{5,6},{6,5},{7,4},{8,11},{9,10},{10,... | collective-permute-start | bytes 786440 | tf_op jit(solution)/shard_map/ppermute | solution.py:22
  119.1 38.4 %collective-permute-start.8 = (bf16[256,1024]{1,0:T(8,128)(2,1)S(1)}, bf16[256,1024]{1,0:T(8,128)(2,1)}, u32[]{:S(2)}, u32[]{:S(2)}) collective-permute-start(bf16[256,1024]{1,0:T(8,128)(2,1)S(1)} %copy-done.2), channel_id=1, source_target_pairs={{0,3},{1,2},{2,1},{3,0},{4,7},{5,6},{6,5},{7,4},{8,11},{9,10},{10,... | collective-permute-start | bytes 1572872 | tf_op jit(solution)/shard_map/ppermute | solution.py:22
  128.9 32.2 %collective-permute-start.10 = (bf16[256,1024]{1,0:T(8,128)(2,1)S(1)}, bf16[256,1024]{1,0:T(8,128)(2,1)}, u32[]{:S(2)}, u32[]{:S(2)}) collective-permute-start(bf16[256,1024]{1,0:T(8,128)(2,1)S(1)} %copy-done.2), channel_id=1, source_target_pairs={{0,1},{1,0},{2,3},{3,2},{4,5},{5,4},{6,7},{7,6},{8,9},{9,8},{10,11... | collective-permute-start | bytes 1572872 | tf_op jit(solution)/shard_map/ppermute | solution.py:22
  140.0 39.1 %all-to-all-start.2 = ((bf16[64,3,2,1024]{3,2,1,0:T(2,128)(2,1)}), bf16[64,3,2,1024]{3,2,1,0:T(2,128)(2,1)S(1)}, u32[]{:S(2)}, u32[]{:S(2)}) async-start(bf16[64,3,2,1024]{3,2,1,0:T(2,128)(2,1)} %reshape.271), calls=%async_computation.2 | async-start | bytes 1572864 | tf_op jit(solution)/shard_map/all_to_all | solution.py:253
  153.7 9.8 %collective-permute-start = (bf16[15,256]{1,0:T(8,128)(2,1)}, bf16[15,256]{1,0:T(8,128)(2,1)}, u32[]{:S(2)}, u32[]{:S(2)}) collective-permute-start(bf16[15,256]{1,0:T(8,128)(2,1)} %slice.109), channel_id=1, source_target_pairs={{0,4},{4,8},{8,12},{12,16},{16,20},{20,24},{24,28},{28,32},{32,36}... | collective-permute-start | bytes 23048 | tf_op jit(solution)/shard_map/ppermute | solution.py:17
  159.2 9.4 %collective-permute-start.9 = (bf16[128,1024]{1,0:T(8,128)(2,1)}, bf16[128,1024]{1,0:T(8,128)(2,1)S(1)}, u32[]{:S(2)}, u32[]{:S(2)}) collective-permute-start(bf16[128,1024]{1,0:T(8,128)(2,1)} %slice.127), channel_id=1, source_target_pairs={{0,1},{1,0},{2,3},{3,2},{4,5},{5,4},{6,7},{7,6},{8,9},{9,8},{10,11... | collective-permute-start | bytes 786440 | tf_op jit(solution)/shard_map/ppermute | solution.py:22
  162.1 10.3 %collective-permute-start.11 = (bf16[128,1024]{1,0:T(8,128)(2,1)S(1)}, bf16[128,1024]{1,0:T(8,128)(2,1)S(1)}, u32[]{:S(2)}, u32[]{:S(2)}) collective-permute-start(bf16[128,1024]{1,0:T(8,128)(2,1)S(1)} %slice.128), channel_id=1, source_target_pairs={{0,3},{1,2},{2,1},{3,0},{4,7},{5,6},{6,5},{7,4},{8,11},{9,10},{10,... | collective-permute-start | bytes 786440 | tf_op jit(solution)/shard_map/ppermute | solution.py:22
  179.1 55.6 %all-to-all-start.1 = ((bf16[64,3,2,1024]{3,2,1,0:T(2,128)(2,1)}), bf16[64,3,2,1024]{3,2,1,0:T(2,128)(2,1)S(1)}, u32[]{:S(2)}, u32[]{:S(2)}) async-start(bf16[64,3,2,1024]{3,2,1,0:T(2,128)(2,1)} %reshape.269), calls=%async_computation.1 | async-start | bytes 1572864 | tf_op jit(solution)/shard_map/all_to_all | solution.py:253
  201.2 26.7 %collective-permute-start.3 = (bf16[128,2048]{1,0:T(8,128)(2,1)}, bf16[128,2048]{1,0:T(8,128)(2,1)}, u32[]{:S(2)}, u32[]{:S(2)}) collective-permute-start(bf16[128,2048]{1,0:T(8,128)(2,1)} %get-tuple-element.11), channel_id=1, source_target_pairs={{0,3},{1,2},{2,1},{3,0},{4,7},{5,6},{6,5},{7,4},{8,11},{9,10},{10,... | collective-permute-start | bytes 1572872 | tf_op jit(solution)/shard_map/ppermute | solution.py:22
  201.9 26.0 %collective-permute-start.2 = (bf16[128,2048]{1,0:T(8,128)(2,1)}, bf16[128,2048]{1,0:T(8,128)(2,1)}, u32[]{:S(2)}, u32[]{:S(2)}) collective-permute-start(bf16[128,2048]{1,0:T(8,128)(2,1)} %get-tuple-element.12), channel_id=1, source_target_pairs={{0,2},{1,3},{2,0},{3,1},{4,6},{5,7},{6,4},{7,5},{8,10},{9,11},{10,... | collective-permute-start | bytes 1572872 | tf_op jit(solution)/shard_map/ppermute | solution.py:22
  205.3 23.3 %collective-permute-start.1 = (bf16[128,2048]{1,0:T(8,128)(2,1)}, bf16[128,2048]{1,0:T(8,128)(2,1)}, u32[]{:S(2)}, u32[]{:S(2)}) collective-permute-start(bf16[128,2048]{1,0:T(8,128)(2,1)} %get-tuple-element.10), channel_id=1, source_target_pairs={{0,1},{1,0},{2,3},{3,2},{4,5},{5,4},{6,7},{7,6},{8,9},{9,8},{10,11... | collective-permute-start | bytes 1572872 | tf_op jit(solution)/shard_map/ppermute | solution.py:22
  (16 other events, 81.1 us)

commit v2 on v1

--- a/solution.py
+++ b/solution.py
@@ -2,13 +2,13 @@
 import jax.numpy as jnp
 from jax import lax
 from jax.experimental import pallas as pl
+from jax.experimental.pallas import tpu as pltpu
 from jax.sharding import PartitionSpec as P
 
 
 RIM = 15
 EPS = 1e-06
-CHUNKS = 1
-WIDTHS = (1024, 1024)
+WIDTHS = (768, 1280)
 
 
 def passed_along(value, axis, steps):
@@ -65,13 +65,13 @@
 
     total = piece(0).astype(jnp.float32)
     for k in range(1, count):
-        total = total + swapped(piece(k), k).astype(jnp.float32)
+        part = piece(k)
+        total = total + swapped(part, k).astype(jnp.float32)
     return total.astype(jnp.bfloat16)
 
 
 def dispatch_kernel(x_ref, gain_ref, routes_ref, *outs):
-    normed_ref, pick_ref = outs[0], outs[1]
-    payloads = outs[2:]
+    normed_ref, pick_ref, payload_ref = outs
     tokens = x_ref.shape[0]
     floats = x_ref[...].astype(jnp.float32)
     scale = lax.rsqrt(jnp.mean(floats * floats, axis=-1, keepdims=True) + EPS)
@@ -106,14 +106,10 @@
     pick_ref[0] = chosen[0].astype(jnp.bfloat16)
     pick_ref[1] = chosen[1].astype(jnp.bfloat16)
     either = (chosen[0] + chosen[1]).astype(jnp.bfloat16)
-    for index, out in enumerate(payloads):
-        width = out.shape[1]
-        out[...] = lax.dot_general(
-            either,
-            normed[:, index * width : (index + 1) * width],
-            (((0,), (0,)), ((), ())),
-            preferred_element_type=jnp.float32,
-        ).astype(jnp.bfloat16)
+    payload = lax.dot_general(
+        either, normed, (((0,), (0,)), ((), ())), preferred_element_type=jnp.float32
+    )
+    payload_ref[...] = payload.astype(jnp.bfloat16).reshape(payload_ref.shape)
 
 
 def dispatch(x, gain, routes, experts, slots_each):
@@ -124,8 +120,9 @@
         out_shape=[
             jax.ShapeDtypeStruct((tokens, model), jnp.bfloat16),
             jax.ShapeDtypeStruct((2, tokens, slots), jnp.bfloat16),
-        ]
-        + [jax.ShapeDtypeStruct((slots, model // CHUNKS), jnp.bfloat16)] * CHUNKS,
+            jax.ShapeDtypeStruct((experts, slots_each // 2, 2, model), jnp.bfloat16),
+        ],
+        compiler_params=pltpu.CompilerParams(vmem_limit_bytes=16 << 20),
         name="dispatch",
     )(x, gain.reshape(1, model), routes)
 
@@ -153,60 +150,53 @@
 
 def combine_kernel(returned_ref, pick_ref, weight_ref, *refs):
     out_ref = refs[-1]
-    returned = returned_ref[...]
+    width = returned_ref.shape[-1]
+    returned = returned_ref[...].reshape(pick_ref.shape[2], width)
     weight = weight_ref[...]
     total = jnp.dot(pick_ref[0], returned, preferred_element_type=jnp.float32) * weight[:, 0:1]
     total = total + jnp.dot(pick_ref[1], returned, preferred_element_type=jnp.float32) * weight[:, 1:2]
-    out_ref[...] = total.astype(jnp.bfloat16)
-
-
-def combine(returned, pick, weight, index, so_far):
-    width = returned.shape[1]
-    tokens = pick.shape[1]
-    whole = [
-        pl.BlockSpec(array.shape, lambda i, n=array.ndim: (0,) * n)
-        for array in (returned, pick, weight)
-    ]
-    extra = [] if so_far is None else [so_far]
+    start = out_ref.shape[1] - width
+    out_ref[:, start:] = total.astype(jnp.bfloat16)
+    if start:
+        out_ref[:, :start] = refs[0][...]
+
+
+def combine(returned, pick, weight, so_far):
+    before = [] if so_far is None else [so_far]
+    width = returned.shape[-1] + sum(part.shape[1] for part in before)
     return pl.pallas_call(
         combine_kernel,
-        grid=(1,),
-        in_specs=whole + [pl.BlockSpec(memory_space=pl.ANY)] * len(extra),
-        out_specs=pl.BlockSpec((tokens, width), lambda i: (0, index)),
-        out_shape=jax.ShapeDtypeStruct((tokens, sum(WIDTHS)), jnp.bfloat16),
-        input_output_aliases={3: 0} if extra else {},
+        out_shape=jax.ShapeDtypeStruct((pick.shape[1], width), jnp.bfloat16),
+        compiler_params=pltpu.CompilerParams(vmem_limit_bytes=8 << 20),
         name="combine",
-    )(returned, pick, weight, *extra)
-
-
-def hidden_kernel(rows_ref, *refs):
-    gate_refs, up_refs, out_ref = refs[: len(refs) // 2], refs[len(refs) // 2 : -1], refs[-1]
-
-    def product(parts):
-        total, start = None, 0
-        for part in parts:
-            depth = part.shape[0]
-            piece = jnp.dot(
-                rows_ref[:, start : start + depth], part[...], preferred_element_type=jnp.float32
-            )
-            start += depth
-            total = piece if total is None else total + piece
-        return total
-
-    gate = product(gate_refs)
-    out_ref[...] = (gate / (1.0 + jnp.exp(-gate)) * product(up_refs)).astype(jnp.bfloat16)
-
-
-def hidden_of(rows, gate_parts, up_parts):
-    units = gate_parts[0].shape[1]
+    )(returned, pick, weight, *before)
+
+
+def hidden_kernel(rows_ref, gate_ref, up_ref, out_ref, *flat_ref):
+    rows = rows_ref[...]
+    if flat_ref:
+        rows = rows.reshape(flat_ref[0].shape)
+        flat_ref[0][...] = rows
+    gate = jnp.dot(rows, gate_ref[...], preferred_element_type=jnp.float32)
+    up = jnp.dot(rows, up_ref[...], preferred_element_type=jnp.float32)
+    out_ref[...] = (gate / (1.0 + jnp.exp(-gate)) * up).astype(jnp.bfloat16)
+
+
+def hidden_of(rows, gate_part, up_part):
+    model, units = gate_part.shape
+    count = rows.size // model
+    shapes = [jax.ShapeDtypeStruct((count, units), jnp.bfloat16)]
+    if rows.ndim > 2:
+        shapes.append(jax.ShapeDtypeStruct((count, model), jnp.bfloat16))
     return pl.pallas_call(
         hidden_kernel,
-        out_shape=jax.ShapeDtypeStruct((rows.shape[0], units), jnp.bfloat16),
+        out_shape=shapes,
+        compiler_params=pltpu.CompilerParams(vmem_limit_bytes=12 << 20),
         cost_estimate=pl.CostEstimate(
-            flops=4 * rows.shape[0] * rows.shape[1] * units, bytes_accessed=4 << 20, transcendentals=0
+            flops=4 * count * model * units, bytes_accessed=4 << 20, transcendentals=0
         ),
         name="hidden",
-    )(rows, *gate_parts, *up_parts)
+    )(rows, gate_part, up_part)
 
 
 def down_kernel(hidden_refs, down_refs, base_ref, out_ref):
@@ -223,10 +213,10 @@
         start += depth
         if start == hidden_refs[index].shape[1]:
             index, start = index + 1, 0
-    out_ref[...] = total.astype(out_ref.dtype)
-
-
-def down_of(hidden, parts, base, dtype):
+    out_ref[...] = total.astype(out_ref.dtype).reshape(out_ref.shape)
+
+
+def down_of(hidden, parts, base, out_shape):
     rows, width = hidden[0].shape[0], parts[0].shape[1]
     depth = sum(part.shape[0] for part in parts)
     bases = [] if base is None else [base]
@@ -239,7 +229,8 @@
 
     return pl.pallas_call(
         kernel,
-        out_shape=jax.ShapeDtypeStruct((rows, width), dtype),
+        out_shape=out_shape,
+        compiler_params=pltpu.CompilerParams(vmem_limit_bytes=12 << 20),
         cost_estimate=pl.CostEstimate(
             flops=2 * rows * depth * width, bytes_accessed=4 << 20, transcendentals=0
         ),
@@ -247,13 +238,8 @@
     )(*hidden, *parts, *bases)
 
 
-def exchange(rows, experts):
-    slots, width = rows.shape
-    each = slots // experts
-    moved = lax.all_to_all(
-        rows.reshape(experts, each // 2, 2, width), "ep", split_axis=0, concat_axis=0, tiled=True
-    )
-    return moved.reshape(slots, width)
+def exchange(rows):
+    return lax.all_to_all(rows, "ep", split_axis=0, concat_axis=0, tiled=True)
 
 
 def layer(
@@ -287,18 +273,19 @@
     ups.append(swapped(ups[1], 3))
     downs, start = [], 0
     for width in WIDTHS:
-        own = down_weight[0][:, start : start + width]
+        half = down_weight.shape[1] // 2
+        own = [down_weight[0, i * half : (i + 1) * half, start : start + width] for i in range(2)]
         start += width
-        half = own.shape[0] // 2
-        near_a, near_b = near(own)
-        far_a = swapped(near_b[:half], 1)
-        far_b = swapped(near_a[half:], 3)
-        downs.append([own, near_a, near_b, far_a, far_b])
+        lows = near(own[0])
+        highs = near(own[1])
+        far_low = swapped(lows[1], 1)
+        far_high = swapped(highs[0], 3)
+        downs.append(own + [lows[0], highs[0], lows[1], highs[1], far_low, far_high])
 
     own_input = lax.dynamic_slice_in_dim(expert_input, tp_place * block_len, block_len, 0)
     own_routes = lax.dynamic_slice_in_dim(routes, tp_place * block_len, block_len, 0)
     normed, pick, payload = dispatch(own_input, expert_gain, own_routes, experts, slots_each)
-    rows = exchange(payload, experts)
+    rows = exchange(payload)
 
     partial_rows = mixer_partial(mixer_input, mixer_gain, pool_in, pool_map, pool_scale, pool_out)
     mixer_output = mixer_reduce(partial_rows)
@@ -306,13 +293,25 @@
 
     hidden = []
     for gate_w, up_w in zip(gates, ups):
-        hidden.append(hidden_of(rows, [gate_w], [up_w]))
+        part, *flat = hidden_of(rows, gate_w, up_w)
+        hidden.append(part)
+        rows = flat[0] if flat else rows
     expert_output = None
     for index, parts in enumerate(downs):
-        most = down_of(hidden[:3], parts[:3], None, jnp.float32)
-        result = down_of(hidden[3:], parts[3:], most, jnp.bfloat16)
-        returned = exchange(result, experts)
-        expert_output = combine(returned, pick, weight, index, expert_output)
+        most = down_of(
+            hidden[:3],
+            parts[:-2],
+            None,
+            jax.ShapeDtypeStruct((rows.shape[0], WIDTHS[index]), jnp.float32),
+        )
+        result = down_of(
+            hidden[3:],
+            parts[-2:],
+            most,
+            jax.ShapeDtypeStruct(payload.shape[:3] + (WIDTHS[index],), jnp.bfloat16),
+        )
+        returned = exchange(result)
+        expert_output = combine(returned, pick, weight, expert_output)
     return (mixer_output, expert_output)
 
 

time: 240 us -> 218 us (0.908)
  Pallas kernels: 35.9 us -> 20.5 us
  local copies, waits for them, and re-layouts: 29.6 us -> 16.4 us
  starting transfers between devices: 55.4 us -> 60 us
  matrix products: 12.8 us -> 15.3 us
    reshape x6 -> x0, local copies, waits for them, and re-layouts: 13.8 us -> none  [the longest x3 9.47 us: exchange(): rows.reshape(experts, each // 2, 2, width)]
    pallas_call x10, Pallas kernels: 32.7 us -> 19.5 us  [the longest x4 9.12 us: down_of(): pl.pallas_call(kernel, out_shape=out_shape, compiler_params=pltpu.Compile...]
    slice x5 -> x0, local copies, waits for them, and re-layouts: 6.17 us -> none  [the longest x2 2.42 us: layer(): far_a = swapped(near_b[:half], 1)]
    ppermute x17 -> x21, starting transfers between devices: 19.7 us -> 24.7 us  [swapped(): lax.ppermute(value, 'tp', [(source, source ^ mask) for source in range(co...]
    unnamed x39 -> x49, local copies, waits for them, and re-layouts: 3.41 us -> 7.86 us
    squeeze x0 -> x2, local copies, waits for them, and re-layouts: none -> 3.68 us  [layer(): down_weight[0, i * half:(i + 1) * half, start:start + width]]
    ppermute x17 -> x21, waiting for transfers between devices: 97.6 us -> 97.7 us  [swapped(): lax.ppermute(value, 'tp', [(source, source ^ mask) for source in range(co...]
  transfers between devices with their start and end apart: 21 -> 25, of which waited for: 7 -> 9; matrix products, arithmetic and copies ran while one was open for 16% -> 13% of each run, Pallas kernels for 13% -> 8%
where the time goes in v2:
time: 218 us; the launch traced here: 217 us
  waiting for transfers between devices  97.7 us (45%)
  starting transfers between devices  60 us (28%)
  Pallas kernels  20.5 us (9%)
  local copies, waits for them, and re-layouts  16.4 us (8%)
  matrix products  15.3 us (7%)
  other arithmetic  6.32 us (3%)
    ppermute x21, waiting for transfers between devices, swapped(): lax.ppermute(value, 'tp', [(source, source ^ mask) for source in range(co...  97.7 us
    all_to_all x3, starting transfers between devices, exchange(): return lax.all_to_all(rows, 'ep', split_axis=0, concat_axis=0, tiled=True)  33.3 us
    ppermute x21, starting transfers between devices, swapped(): lax.ppermute(value, 'tp', [(source, source ^ mask) for source in range(co...  24.7 us
    pallas_call x4, Pallas kernels, down_of(): pl.pallas_call(kernel, out_shape=out_shape, compiler_params=pltpu.Compile...  9.12 us
    dot_general x1, matrix products, mixer_partial(): jnp.dot(mixed_rows, pool_out, preferred_element_type=jnp.float32)  8.88 us
    pallas_call x4, Pallas kernels, hidden_of(): pl.pallas_call(hidden_kernel, out_shape=shapes, compiler_params=pltpu.Com...  8.72 us
    unnamed x49, local copies, waits for them, and re-layouts  7.86 us
  transfers between devices with their start and end apart: 25, of which 9 were waited for; matrix products, arithmetic and copies ran while one was open for 13% of the time, Pallas kernels for 8%

profile of v2, /device:TPU:8, one launch (start us, length us, event | category | flops | bytes accessed | tf_op | source)
XLA Modules:
  0.0 217.3 jit_solution(6811139284639107522)
XLA Ops:
  5.7 12.2 %all-to-all-start = ((bf16[64,3,2,2048]{3,2,1,0:T(2,128)(2,1)}), bf16[64,3,2,2048]{3,2,1,0:T(2,128)(2,1)S(1)}, u32[]{:S(2)}, u32[]{:S(2)}) async-start(bf16[64,3,2,2048]{3,2,1,0:T(2,128)(2,1)} %copy-done.1), calls=%async_computation | async-start | bytes 3145728 | tf_op jit(solution)/shard_map/all_to_all | solution.py:242
  17.9 2.8 %collective-permute-start.4 = (bf16[2048,256]{1,0:T(8,128)(2,1)}, bf16[2048,256]{1,0:T(8,128)(2,1)}, u32[]{:S(2)}, u32[]{:S(2)}) collective-permute-start(bf16[2048,256]{1,0:T(8,128)(2,1)} %bitcast.22), channel_id=1, source_target_pairs={{0,3},{1,2},{2,1},{3,0},{4,7},{5,6},{6,5},{7,4},{8,11},{9,10},{10,... | collective-permute-start | bytes 3145736 | tf_op jit(solution)/shard_map/ppermute | solution.py:22
  25.0 2.8 %collective-permute-start.16 = (bf16[128,768]{1,0:T(8,128)(2,1)S(1)}, bf16[128,768]{1,0:T(8,128)(2,1)S(1)}, u32[]{:S(2)}, u32[]{:S(2)}) collective-permute-start(bf16[128,768]{1,0:T(8,128)(2,1)S(1)} %get-tuple-element.18.refs_3_), channel_id=1, source_target_pairs={{0,3},{1,2},{2,1},{3,0},{4,7},{5,6},{6,5},{7,4},{8,11},{9,10},{10,... | collective-permute-start | bytes 589832 | tf_op jit(solution)/shard_map/ppermute | solution.py:22
  27.8 17.8 %collective-permute-done.4.gate_ref = bf16[2048,256]{1,0:T(8,128)(2,1)} collective-permute-done((bf16[2048,256]{1,0:T(8,128)(2,1)}, bf16[2048,256]{1,0:T(8,128)(2,1)}, u32[]{:S(2)}, u32[]{:S(2)}) %collective-permute-start.4) | collective-permute-done | bytes 1048608 | tf_op jit(solution)/shard_map/ppermute | solution.py:22
  50.3 21.9 %collective-permute-done.16.refs_7_ = bf16[128,768]{1,0:T(8,128)(2,1)S(1)} collective-permute-done((bf16[128,768]{1,0:T(8,128)(2,1)S(1)}, bf16[128,768]{1,0:T(8,128)(2,1)S(1)}, u32[]{:S(2)}, u32[]{:S(2)}) %collective-permute-start.16) | collective-permute-done | bytes 196640 | tf_op jit(solution)/shard_map/ppermute | solution.py:22
  73.6 21.5 %collective-permute-done.18.refs_6_ = bf16[128,768]{1,0:T(8,128)(2,1)S(1)} collective-permute-done((bf16[128,768]{1,0:T(8,128)(2,1)}, bf16[128,768]{1,0:T(8,128)(2,1)S(1)}, u32[]{:S(2)}, u32[]{:S(2)}) %collective-permute-start.18) | collective-permute-done | bytes 196640 | tf_op jit(solution)/shard_map/ppermute | solution.py:22
  95.3 5.5 %collective-permute-done.20.refs_5_ = bf16[128,768]{1,0:T(8,128)(2,1)S(1)} collective-permute-done((bf16[128,768]{1,0:T(8,128)(2,1)S(1)}, bf16[128,768]{1,0:T(8,128)(2,1)S(1)}, u32[]{:S(2)}, u32[]{:S(2)}) %collective-permute-start.20) | collective-permute-done | bytes 196640 | tf_op jit(solution)/shard_map/ppermute | solution.py:22
  108.5 2.5 %hidden.6.refs_1_ = bf16[384,256]{1,0:T(8,128)(2,1)S(1)} custom-call(bf16[384,2048]{1,0:T(8,128)(2,1)S(1)} %get-tuple-element.8.rows_ref, bf16[2048,256]{1,0:T(8,128)(2,1)} %collective-permute-done.12.gate_ref, bf16[2048,256]{1,0:T(8,128)(2,1)} %collective-permute-done.6.up_ref), custom_call_target="tpu_custom_call" | custom-call | flops 805306368 | bytes 4194304 | tf_op jit(solution)/shard_map/hidden/pallas_call | solution.py:191
  111.1 2.6 %hidden.7.refs_2_ = bf16[384,256]{1,0:T(8,128)(2,1)S(1)} custom-call(bf16[384,2048]{1,0:T(8,128)(2,1)S(1)} %get-tuple-element.8.rows_ref, bf16[2048,256]{1,0:T(8,128)(2,1)} %collective-permute-done.4.gate_ref, bf16[2048,256]{1,0:T(8,128)(2,1)} %collective-permute-done.13.up_ref), custom_call_target="tpu_custom_call" | custom-call | flops 805306368 | bytes 4194304 | tf_op jit(solution)/shard_map/hidden/pallas_call | solution.py:191
  118.9 2.5 %hidden.5.refs_0_ = bf16[384,256]{1,0:T(8,128)(2,1)S(1)} custom-call(bf16[384,2048]{1,0:T(8,128)(2,1)S(1)} %get-tuple-element.8.rows_ref, bf16[2048,256]{1,0:T(8,128)(2,1)} %collective-permute-done.5.gate_ref, bf16[2048,256]{1,0:T(8,128)(2,1)} %collective-permute-done.7.up_ref), custom_call_target="tpu_custom_call" | custom-call | flops 805306368 | bytes 4194304 | tf_op jit(solution)/shard_map/hidden/pallas_call | solution.py:191
  121.5 2.6 %collective-permute-start.15 = (bf16[128,1280]{1,0:T(8,128)(2,1)S(1)}, bf16[128,1280]{1,0:T(8,128)(2,1)}, u32[]{:S(2)}, u32[]{:S(2)}) collective-permute-start(bf16[128,1280]{1,0:T(8,128)(2,1)S(1)} %copy-done.2), channel_id=1, source_target_pairs={{0,3},{1,2},{2,1},{3,0},{4,7},{5,6},{6,5},{7,4},{8,11},{9,10},{10,... | collective-permute-start | bytes 983048 | tf_op jit(solution)/shard_map/ppermute | solution.py:22
  125.4 10.3 %all-to-all-start.2 = ((bf16[64,3,2,768]{3,2,1,0:T(2,128)(2,1)}), bf16[64,3,2,768]{3,2,1,0:T(2,128)(2,1)S(1)}, u32[]{:S(2)}, u32[]{:S(2)}) async-start(bf16[64,3,2,768]{3,2,1,0:T(2,128)(2,1)} %down.7), calls=%async_computation.2 | async-start | bytes 1179648 | tf_op jit(solution)/shard_map/all_to_all | solution.py:242
  135.7 2.6 %fusion.7 = bf16[512,256]{1,0:T(8,128)(2,1)S(1)} fusion(bf16[2048,256]{1,0:T(8,128)(2,1)} %param.16, bf16[512,2048]{1,0:T(8,128)(2,1)} %param.14, f32[2048]{0:T(1024)S(1)} %convert_element_type.119, f32[512]{0:T(512)S(1)} %add_rsqrt_fusion), kind=kOutput, calls=%fused_computation.10 | convolution fusion | flops 541196288 | bytes 3418112 | tf_op jit(solution)/shard_map/dot_general | solution.py:33
  148.4 3.0 %down.4.refs_3_ = f32[384,1280]{1,0:T(8,128)S(1)} custom-call(bf16[384,256]{1,0:T(8,128)(2,1)S(1)} %copy-done.6, bf16[384,256]{1,0:T(8,128)(2,1)S(1)} %hidden.6.refs_1_, bf16[384,256]{1,0:T(8,128)(2,1)S(1)} %hidden.7.refs_2_, bf16[128,1280]{1,0:T(8,128)(2,1)} %get-tuple-element.20.refs_3_, bf16[128,1280]{1,0:T(8,128)(2,1)S(1)} %copy-done.2, ...), custom_call_target="tpu_custom_call" | custom-call | flops 754974720 | bytes 4194304 | tf_op jit(solution)/shard_map/down/pallas_call | solution.py:230
  151.4 5.0 %collective-permute-done.11.refs_2_ = bf16[128,1280]{1,0:T(8,128)(2,1)S(1)} collective-permute-done((bf16[128,1280]{1,0:T(8,128)(2,1)}, bf16[128,1280]{1,0:T(8,128)(2,1)S(1)}, u32[]{:S(2)}, u32[]{:S(2)}) %collective-permute-start.11) | collective-permute-done | bytes 327712 | tf_op jit(solution)/shard_map/ppermute | solution.py:22
  156.4 2.7 %down.5 = bf16[64,3,2,1280]{3,2,1,0:T(2,128)(2,1)} custom-call(bf16[384,256]{1,0:T(8,128)(2,1)S(1)} %hidden.5.refs_0_, bf16[128,1280]{1,0:T(8,128)(2,1)} %collective-permute-done.9.refs_1_, bf16[128,1280]{1,0:T(8,128)(2,1)S(1)} %collective-permute-done.11.refs_2_, f32[384,1280]{1,0:T(8,128)S(1)} %down.4.refs_3_), custom_call_target="tpu_custom_call" | custom-call | flops 251658240 | bytes 4194304 | tf_op jit(solution)/shard_map/down/pallas_call | solution.py:230
  159.1 10.7 %all-to-all-start.1 = ((bf16[64,3,2,1280]{3,2,1,0:T(2,128)(2,1)}), bf16[64,3,2,1280]{3,2,1,0:T(2,128)(2,1)S(1)}, u32[]{:S(2)}, u32[]{:S(2)}) async-start(bf16[64,3,2,1280]{3,2,1,0:T(2,128)(2,1)} %down.5), calls=%async_computation.1 | async-start | bytes 1966080 | tf_op jit(solution)/shard_map/all_to_all | solution.py:242
  171.7 8.9 %convolution_convert_fusion = bf16[512,2048]{1,0:T(8,128)(2,1)} fusion(bf16[256,2048]{1,0:T(8,128)(2,1)} %param.19, f32[256]{0:T(256)S(1)} %convert_element_type.141, f32[527,256]{1,0:T(8,128)} %maximum_convert_fusion, f32[512]{0:T(512)S(1)} %copy-done.22, f32[]{:T(128)S(6)} %convert_element_type.138, f32[]{:T(128)S(6)} %convert_element_type.137, ...), kind=kOutput, calls=%fused_computation.5 | convolution fusion | flops 609746944 | bytes 11668544 | tf_op jit(solution)/shard_map/dot_general | solution.py:55
  180.6 2.5 %constant_dynamic-slice_fusion.4 = (bf16[128,2048]{1,0:T(8,128)(2,1)}, bf16[128,2048]{1,0:T(8,128)(2,1)}, bf16[128,2048]{1,0:T(8,128)(2,1)}) fusion(bf16[512,2048]{1,0:T(8,128)(2,1)} %convolution_convert_fusion, s32[]{:T(128)S(6)} %select_n.29, s32[]{:T(128)S(6)} %select_n.31, s32[]{:T(128)S(6)} %select_n.30), kind=kLoop, calls=%fused_computation.72 | loop fusion | bytes 3145740 | tf_op jit(solution)/shard_map/dynamic_slice | solution.py:64
  183.1 3.7 %collective-permute-start.2 = (bf16[128,2048]{1,0:T(8,128)(2,1)}, bf16[128,2048]{1,0:T(8,128)(2,1)}, u32[]{:S(2)}, u32[]{:S(2)}) collective-permute-start(bf16[128,2048]{1,0:T(8,128)(2,1)} %get-tuple-element.16), channel_id=1, source_target_pairs={{0,2},{1,3},{2,0},{3,1},{4,6},{5,7},{6,4},{7,5},{8,10},{9,11},{10,... | collective-permute-start | bytes 1572872 | tf_op jit(solution)/shard_map/ppermute | solution.py:22
  188.2 10.0 %collective-permute-done.1 = bf16[128,2048]{1,0:T(8,128)(2,1)} collective-permute-done((bf16[128,2048]{1,0:T(8,128)(2,1)}, bf16[128,2048]{1,0:T(8,128)(2,1)}, u32[]{:S(2)}, u32[]{:S(2)}) %collective-permute-start.1) | collective-permute-done | bytes 524320 | tf_op jit(solution)/shard_map/ppermute | solution.py:22
  198.2 12.2 %collective-permute-done.2 = bf16[128,2048]{1,0:T(8,128)(2,1)} collective-permute-done((bf16[128,2048]{1,0:T(8,128)(2,1)}, bf16[128,2048]{1,0:T(8,128)(2,1)}, u32[]{:S(2)}, u32[]{:S(2)}) %collective-permute-start.2) | collective-permute-done | bytes 524320 | tf_op jit(solution)/shard_map/ppermute | solution.py:22
  210.4 2.6 %collective-permute-done.3 = bf16[128,2048]{1,0:T(8,128)(2,1)} collective-permute-done((bf16[128,2048]{1,0:T(8,128)(2,1)}, bf16[128,2048]{1,0:T(8,128)(2,1)}, u32[]{:S(2)}, u32[]{:S(2)}) %collective-permute-start.3) | collective-permute-done | bytes 524320 | tf_op jit(solution)/shard_map/ppermute | solution.py:22
  213.0 2.6 %add_convert_fusion = bf16[128,2048]{1,0:T(8,128)(2,1)} fusion(bf16[128,2048]{1,0:T(8,128)(2,1)} %collective-permute-done.3, bf16[128,2048]{1,0:T(8,128)(2,1)} %collective-permute-done.2, bf16[128,2048]{1,0:T(8,128)(2,1)} %collective-permute-done.1, bf16[512,2048]{1,0:T(8,128)(2,1)} %convolution_convert_fusion, s32[]{:T(128)S(6)} %select_n.28), kind=kLoop, calls=%fused_computation.17 | loop fusion | flops 2097152 | bytes 2621444 | tf_op jit(solution)/shard_map/convert_element_type | solution.py:70
  (110 shorter events, 44.6 us)
Async XLA Ops:
  5.7 96.4 %all-to-all-start = ((bf16[64,3,2,2048]{3,2,1,0:T(2,128)(2,1)}), bf16[64,3,2,2048]{3,2,1,0:T(2,128)(2,1)S(1)}, u32[]{:S(2)}, u32[]{:S(2)}) async-start(bf16[64,3,2,2048]{3,2,1,0:T(2,128)(2,1)} %copy-done.1), calls=%async_computation | async-start | bytes 3145728 | tf_op jit(solution)/shard_map/all_to_all | solution.py:242
  17.9 27.6 %collective-permute-start.4 = (bf16[2048,256]{1,0:T(8,128)(2,1)}, bf16[2048,256]{1,0:T(8,128)(2,1)}, u32[]{:S(2)}, u32[]{:S(2)}) collective-permute-start(bf16[2048,256]{1,0:T(8,128)(2,1)} %bitcast.22), channel_id=1, source_target_pairs={{0,3},{1,2},{2,1},{3,0},{4,7},{5,6},{6,5},{7,4},{8,11},{9,10},{10,... | collective-permute-start | bytes 3145736 | tf_op jit(solution)/shard_map/ppermute | solution.py:22
  20.8 26.3 %collective-permute-start.6 = (bf16[2048,256]{1,0:T(8,128)(2,1)}, bf16[2048,256]{1,0:T(8,128)(2,1)}, u32[]{:S(2)}, u32[]{:S(2)}) collective-permute-start(bf16[2048,256]{1,0:T(8,128)(2,1)} %bitcast.25), channel_id=1, source_target_pairs={{0,1},{1,0},{2,3},{3,2},{4,5},{5,4},{6,7},{7,6},{8,9},{9,8},{10,11... | collective-permute-start | bytes 3145736 | tf_op jit(solution)/shard_map/ppermute | solution.py:22
  21.0 84.7 %collective-permute-start.12 = (bf16[2048,256]{1,0:T(8,128)(2,1)}, bf16[2048,256]{1,0:T(8,128)(2,1)}, u32[]{:S(2)}, u32[]{:S(2)}) collective-permute-start(bf16[2048,256]{1,0:T(8,128)(2,1)} %bitcast.23), channel_id=1, source_target_pairs={{0,1},{1,0},{2,3},{3,2},{4,5},{5,4},{6,7},{7,6},{8,9},{9,8},{10,11... | collective-permute-start | bytes 3145736 | tf_op jit(solution)/shard_map/ppermute | solution.py:22
  22.8 83.2 %collective-permute-start.13 = (bf16[2048,256]{1,0:T(8,128)(2,1)}, bf16[2048,256]{1,0:T(8,128)(2,1)}, u32[]{:S(2)}, u32[]{:S(2)}) collective-permute-start(bf16[2048,256]{1,0:T(8,128)(2,1)} %bitcast.26), channel_id=1, source_target_pairs={{0,3},{1,2},{2,1},{3,0},{4,7},{5,6},{6,5},{7,4},{8,11},{9,10},{10,... | collective-permute-start | bytes 3145736 | tf_op jit(solution)/shard_map/ppermute | solution.py:22
  25.0 47.1 %collective-permute-start.16 = (bf16[128,768]{1,0:T(8,128)(2,1)S(1)}, bf16[128,768]{1,0:T(8,128)(2,1)S(1)}, u32[]{:S(2)}, u32[]{:S(2)}) collective-permute-start(bf16[128,768]{1,0:T(8,128)(2,1)S(1)} %get-tuple-element.18.refs_3_), channel_id=1, source_target_pairs={{0,3},{1,2},{2,1},{3,0},{4,7},{5,6},{6,5},{7,4},{8,11},{9,10},{10,... | collective-permute-start | bytes 589832 | tf_op jit(solution)/shard_map/ppermute | solution.py:22
  45.6 71.2 %collective-permute-start.5 = (bf16[2048,256]{1,0:T(8,128)(2,1)}, bf16[2048,256]{1,0:T(8,128)(2,1)}, u32[]{:S(2)}, u32[]{:S(2)}) collective-permute-start(bf16[2048,256]{1,0:T(8,128)(2,1)} %collective-permute-done.4.gate_ref), channel_id=1, source_target_pairs={{0,1},{1,0},{2,3},{3,2},{4,5},{5,4},{6,7},{7,6},{8,9},{9,8},{10,11... | collective-permute-start | bytes 3145736 | tf_op jit(solution)/shard_map/ppermute | solution.py:22
  47.1 70.4 %collective-permute-start.7 = (bf16[2048,256]{1,0:T(8,128)(2,1)}, bf16[2048,256]{1,0:T(8,128)(2,1)}, u32[]{:S(2)}, u32[]{:S(2)}) collective-permute-start(bf16[2048,256]{1,0:T(8,128)(2,1)} %collective-permute-done.6.up_ref), channel_id=1, source_target_pairs={{0,3},{1,2},{2,1},{3,0},{4,7},{5,6},{6,5},{7,4},{8,11},{9,10},{10,... | collective-permute-start | bytes 3145736 | tf_op jit(solution)/shard_map/ppermute | solution.py:22
  72.8 22.2 %collective-permute-start.18 = (bf16[128,768]{1,0:T(8,128)(2,1)}, bf16[128,768]{1,0:T(8,128)(2,1)S(1)}, u32[]{:S(2)}, u32[]{:S(2)}) collective-permute-start(bf16[128,768]{1,0:T(8,128)(2,1)} %get-tuple-element.17.refs_4_), channel_id=1, source_target_pairs={{0,1},{1,0},{2,3},{3,2},{4,5},{5,4},{6,7},{7,6},{8,9},{9,8},{10,11... | collective-permute-start | bytes 589832 | tf_op jit(solution)/shard_map/ppermute | solution.py:22
  101.5 12.2 %collective-permute-start.21 = (bf16[128,768]{1,0:T(8,128)(2,1)}, bf16[128,768]{1,0:T(8,128)(2,1)}, u32[]{:S(2)}, u32[]{:S(2)}) collective-permute-start(bf16[128,768]{1,0:T(8,128)(2,1)} %get-tuple-element.17.refs_4_), channel_id=1, source_target_pairs={{0,3},{1,2},{2,1},{3,0},{4,7},{5,6},{6,5},{7,4},{8,11},{9,10},{10,... | collective-permute-start | bytes 589832 | tf_op jit(solution)/shard_map/ppermute | solution.py:22
  105.7 15.8 %collective-permute-start.17 = (bf16[128,768]{1,0:T(8,128)(2,1)S(1)}, bf16[128,768]{1,0:T(8,128)(2,1)S(1)}, u32[]{:S(2)}, u32[]{:S(2)}) collective-permute-start(bf16[128,768]{1,0:T(8,128)(2,1)S(1)} %copy-done.12), channel_id=1, source_target_pairs={{0,1},{1,0},{2,3},{3,2},{4,5},{5,4},{6,7},{7,6},{8,9},{9,8},{10,11... | collective-permute-start | bytes 589832 | tf_op jit(solution)/shard_map/ppermute | solution.py:22
  106.0 18.0 %collective-permute-start.19 = (bf16[128,768]{1,0:T(8,128)(2,1)S(1)}, bf16[128,768]{1,0:T(8,128)(2,1)S(1)}, u32[]{:S(2)}, u32[]{:S(2)}) collective-permute-start(bf16[128,768]{1,0:T(8,128)(2,1)S(1)} %copy-done.14), channel_id=1, source_target_pairs={{0,3},{1,2},{2,1},{3,0},{4,7},{5,6},{6,5},{7,4},{8,11},{9,10},{10,... | collective-permute-start | bytes 589832 | tf_op jit(solution)/shard_map/ppermute | solution.py:22
  113.7 32.0 %collective-permute-start.8 = (bf16[128,1280]{1,0:T(8,128)(2,1)}, bf16[128,1280]{1,0:T(8,128)(2,1)}, u32[]{:S(2)}, u32[]{:S(2)}) collective-permute-start(bf16[128,1280]{1,0:T(8,128)(2,1)} %get-tuple-element.20.refs_3_), channel_id=1, source_target_pairs={{0,3},{1,2},{2,1},{3,0},{4,7},{5,6},{6,5},{7,4},{8,11},{9,10},{10,... | collective-permute-start | bytes 983048 | tf_op jit(solution)/shard_map/ppermute | solution.py:22
  116.8 30.6 %collective-permute-start.14 = (bf16[128,1280]{1,0:T(8,128)(2,1)}, bf16[128,1280]{1,0:T(8,128)(2,1)}, u32[]{:S(2)}, u32[]{:S(2)}) collective-permute-start(bf16[128,1280]{1,0:T(8,128)(2,1)} %get-tuple-element.20.refs_3_), channel_id=1, source_target_pairs={{0,1},{1,0},{2,3},{3,2},{4,5},{5,4},{6,7},{7,6},{8,9},{9,8},{10,11... | collective-permute-start | bytes 983048 | tf_op jit(solution)/shard_map/ppermute | solution.py:22
  117.5 27.4 %collective-permute-start.10 = (bf16[128,1280]{1,0:T(8,128)(2,1)S(1)}, bf16[128,1280]{1,0:T(8,128)(2,1)}, u32[]{:S(2)}, u32[]{:S(2)}) collective-permute-start(bf16[128,1280]{1,0:T(8,128)(2,1)S(1)} %copy-done.2), channel_id=1, source_target_pairs={{0,1},{1,0},{2,3},{3,2},{4,5},{5,4},{6,7},{7,6},{8,9},{9,8},{10,11... | collective-permute-start | bytes 983048 | tf_op jit(solution)/shard_map/ppermute | solution.py:22
  121.5 26.0 %collective-permute-start.15 = (bf16[128,1280]{1,0:T(8,128)(2,1)S(1)}, bf16[128,1280]{1,0:T(8,128)(2,1)}, u32[]{:S(2)}, u32[]{:S(2)}) collective-permute-start(bf16[128,1280]{1,0:T(8,128)(2,1)S(1)} %copy-done.2), channel_id=1, source_target_pairs={{0,3},{1,2},{2,1},{3,0},{4,7},{5,6},{6,5},{7,4},{8,11},{9,10},{10,... | collective-permute-start | bytes 983048 | tf_op jit(solution)/shard_map/ppermute | solution.py:22
  125.4 33.8 %all-to-all-start.2 = ((bf16[64,3,2,768]{3,2,1,0:T(2,128)(2,1)}), bf16[64,3,2,768]{3,2,1,0:T(2,128)(2,1)S(1)}, u32[]{:S(2)}, u32[]{:S(2)}) async-start(bf16[64,3,2,768]{3,2,1,0:T(2,128)(2,1)} %down.7), calls=%async_computation.2 | async-start | bytes 1179648 | tf_op jit(solution)/shard_map/all_to_all | solution.py:242
  139.6 30.2 %collective-permute-start = (bf16[15,256]{1,0:T(8,128)(2,1)}, bf16[15,256]{1,0:T(8,128)(2,1)S(1)}, u32[]{:S(2)}, u32[]{:S(2)}) collective-permute-start(bf16[15,256]{1,0:T(8,128)(2,1)} %slice.101), channel_id=1, source_target_pairs={{0,4},{4,8},{8,12},{12,16},{16,20},{20,24},{24,28},{28,32},{32,36}... | collective-permute-start | bytes 23048 | tf_op jit(solution)/shard_map/ppermute | solution.py:17
  144.9 11.5 %collective-permute-start.11 = (bf16[128,1280]{1,0:T(8,128)(2,1)}, bf16[128,1280]{1,0:T(8,128)(2,1)S(1)}, u32[]{:S(2)}, u32[]{:S(2)}) collective-permute-start(bf16[128,1280]{1,0:T(8,128)(2,1)} %collective-permute-done.10.refs_6_), channel_id=1, source_target_pairs={{0,3},{1,2},{2,1},{3,0},{4,7},{5,6},{6,5},{7,4},{8,11},{9,10},{10,... | collective-permute-start | bytes 983048 | tf_op jit(solution)/shard_map/ppermute | solution.py:22
  145.7 10.8 %collective-permute-start.9 = (bf16[128,1280]{1,0:T(8,128)(2,1)}, bf16[128,1280]{1,0:T(8,128)(2,1)}, u32[]{:S(2)}, u32[]{:S(2)}) collective-permute-start(bf16[128,1280]{1,0:T(8,128)(2,1)} %collective-permute-done.8.refs_7_), channel_id=1, source_target_pairs={{0,1},{1,0},{2,3},{3,2},{4,5},{5,4},{6,7},{7,6},{8,9},{9,8},{10,11... | collective-permute-start | bytes 983048 | tf_op jit(solution)/shard_map/ppermute | solution.py:22
  159.1 56.9 %all-to-all-start.1 = ((bf16[64,3,2,1280]{3,2,1,0:T(2,128)(2,1)}), bf16[64,3,2,1280]{3,2,1,0:T(2,128)(2,1)S(1)}, u32[]{:S(2)}, u32[]{:S(2)}) async-start(bf16[64,3,2,1280]{3,2,1,0:T(2,128)(2,1)} %down.5), calls=%async_computation.1 | async-start | bytes 1966080 | tf_op jit(solution)/shard_map/all_to_all | solution.py:242
  183.1 15.1 %collective-permute-start.1 = (bf16[128,2048]{1,0:T(8,128)(2,1)}, bf16[128,2048]{1,0:T(8,128)(2,1)}, u32[]{:S(2)}, u32[]{:S(2)}) collective-permute-start(bf16[128,2048]{1,0:T(8,128)(2,1)} %get-tuple-element.14), channel_id=1, source_target_pairs={{0,1},{1,0},{2,3},{3,2},{4,5},{5,4},{6,7},{7,6},{8,9},{9,8},{10,11... | collective-permute-start | bytes 1572872 | tf_op jit(solution)/shard_map/ppermute | solution.py:22
  183.1 27.3 %collective-permute-start.2 = (bf16[128,2048]{1,0:T(8,128)(2,1)}, bf16[128,2048]{1,0:T(8,128)(2,1)}, u32[]{:S(2)}, u32[]{:S(2)}) collective-permute-start(bf16[128,2048]{1,0:T(8,128)(2,1)} %get-tuple-element.16), channel_id=1, source_target_pairs={{0,2},{1,3},{2,0},{3,1},{4,6},{5,7},{6,4},{7,5},{8,10},{9,11},{10,... | collective-permute-start | bytes 1572872 | tf_op jit(solution)/shard_map/ppermute | solution.py:22
  186.8 26.1 %collective-permute-start.3 = (bf16[128,2048]{1,0:T(8,128)(2,1)}, bf16[128,2048]{1,0:T(8,128)(2,1)}, u32[]{:S(2)}, u32[]{:S(2)}) collective-permute-start(bf16[128,2048]{1,0:T(8,128)(2,1)} %get-tuple-element.15), channel_id=1, source_target_pairs={{0,3},{1,2},{2,1},{3,0},{4,7},{5,6},{6,5},{7,4},{8,11},{9,10},{10,... | collective-permute-start | bytes 1572872 | tf_op jit(solution)/shard_map/ppermute | solution.py:22
  (25 other events, 289.6 us)

commit v3 on v2

v3 whole, which is shorter than its diff:
```python
import jax
import jax.numpy as jnp
from jax import lax
from jax.experimental import pallas as pl
from jax.experimental.pallas import tpu as pltpu
from jax.sharding import PartitionSpec as P


RIM = 15
EPS = 1e-06


def passed_along(value, axis, steps):
    count = lax.axis_size(axis)
    leading, last = (max(0, -steps), min(count, count - steps))
    return lax.ppermute(value, axis, [(source, source + steps) for source in range(leading, last)])


def swapped(value, mask):
    count = lax.axis_size("tp")
    return lax.ppermute(value, "tp", [(source, source ^ mask) for source in range(count)])


def sent(value, holder_moves, other_moves):
    count = lax.axis_size("tp")
    pairs = []
    for device in range(lax.axis_size("ep")):
        for place in range(count):
            mask, to_holder = holder_moves if device % 2 == place % 2 else other_moves
            goal = place ^ mask
            core = goal % 2 if to_holder else 1 - goal % 2
            pairs.append((device * count + place, (device - device % 2 + core) * count + goal))
    return lax.ppermute(value, ("ep", "tp"), pairs)


def parts_of(own):
    first = sent(own, (0, False), (1, True))
    second = sent(own, (2, False), (3, True))
    first_over = sent(first, (0, False), (0, True))
    second_over = sent(second, (0, False), (0, True))
    return [(own, first), (first, first_over), (second, second_over), (second_over, second)]


def norm_rows(values, gain):
    floats = values.astype(jnp.float32)
    scale = lax.rsqrt(jnp.mean(floats * floats, axis=-1, keepdims=True) + EPS)
    return (floats * scale * gain.astype(jnp.float32)).astype(jnp.bfloat16)


def mixer_partial(mixer_input, mixer_gain, pool_in, pool_map, pool_scale, pool_out):
    normed = norm_rows(mixer_input, mixer_gain)
    pooled_in = jnp.dot(normed, pool_in, preferred_element_type=jnp.float32).astype(jnp.bfloat16)
    local_rows = pooled_in.shape[0]
    groups_here = pool_map.shape[0]
    channels = pool_map.shape[1]
    last = norm_rows(mixer_input[local_rows - RIM - 1 :], mixer_gain)
    last = jnp.dot(last, pool_in, preferred_element_type=jnp.float32).astype(jnp.bfloat16)
    border = passed_along(last[1:], "ep", 1)
    padded = jnp.concatenate([border, pooled_in], axis=0).astype(jnp.float32)
    padded = padded.reshape(local_rows + RIM, groups_here, channels)
    leading = lax.axis_index("tp") * groups_here
    windows = jnp.left_shift(jnp.int32(2), leading + jnp.arange(groups_here, dtype=jnp.int32))
    window_sum = jnp.zeros((local_rows, groups_here, channels), jnp.float32)
    for offset in range(RIM + 1):
        active = (offset < windows).astype(jnp.float32)
        window_sum = (
            window_sum + padded[RIM - offset : RIM - offset + local_rows] * active[None, :, None]
        )
    position = lax.axis_index("ep") * local_rows + jnp.arange(local_rows, dtype=jnp.int32)
    counts_here = jnp.minimum(position[:, None] + 1, windows[None, :]).astype(jnp.float32)
    pooled = (window_sum / counts_here[:, :, None] - padded[RIM:]).astype(jnp.bfloat16)
    mapped = jnp.einsum("tgc,gce->tge", pooled, pool_map, preferred_element_type=jnp.float32)
    mixed_rows = (
        mapped.reshape(local_rows, groups_here * channels) * pool_scale.astype(jnp.float32)
    ).astype(jnp.bfloat16)
    return jnp.dot(mixed_rows, pool_out, preferred_element_type=jnp.float32).astype(jnp.bfloat16)


def mixer_reduce(partial_rows):
    count = lax.axis_size("tp")
    place = lax.axis_index("tp")
    rows = partial_rows.shape[0] // count

    def piece(k):
        return lax.dynamic_slice_in_dim(partial_rows, (place ^ k) * rows, rows, 0)

    total = piece(0).astype(jnp.float32)
    for k in range(1, count):
        part = piece(k)
        total = total + swapped(part, k).astype(jnp.float32)
    return total.astype(jnp.bfloat16)


def dispatch_kernel(x_ref, gain_ref, targets_ref, *outs):
    normed_ref, pick_ref, payload_ref = outs
    tokens = x_ref.shape[0]
    floats = x_ref[...].astype(jnp.float32)
    scale = lax.rsqrt(jnp.mean(floats * floats, axis=-1, keepdims=True) + EPS)
    normed = (floats * scale * gain_ref[...].astype(jnp.float32)).astype(jnp.bfloat16)
    normed_ref[...] = normed
    targets = targets_ref[...]
    slots = pick_ref.shape[2]
    experts = 64
    each = slots // experts
    expert = lax.broadcasted_iota(jnp.int32, (tokens, experts), 1)
    first = targets[:, 0:1] == expert
    second = targets[:, 1:2] == expert
    named = jnp.where(first | second, 1.0, 0.0)
    earlier = lax.broadcasted_iota(jnp.int32, (tokens, tokens), 1) < lax.broadcasted_iota(
        jnp.int32, (tokens, tokens), 0
    )
    before = jnp.dot(
        jnp.where(earlier, 1.0, 0.0).astype(jnp.bfloat16),
        named.astype(jnp.bfloat16),
        preferred_element_type=jnp.float32,
    )
    spread = lax.broadcasted_iota(jnp.int32, (experts, slots), 1) // each == lax.broadcasted_iota(
        jnp.int32, (experts, slots), 0
    )
    spread = jnp.where(spread, 1.0, 0.0).astype(jnp.bfloat16)
    within = (lax.broadcasted_iota(jnp.int32, (tokens, slots), 1) % each).astype(jnp.float32)
    chosen = []
    for mask in (first, second):
        place = jnp.where(mask, before, -1.0).astype(jnp.bfloat16)
        spread_place = jnp.dot(place, spread, preferred_element_type=jnp.float32)
        chosen.append(jnp.where(spread_place == within, 1.0, 0.0))
    pick_ref[0] = chosen[0].astype(jnp.bfloat16)
    pick_ref[1] = chosen[1].astype(jnp.bfloat16)
    either = (chosen[0] + chosen[1]).astype(jnp.bfloat16)
    payload = lax.dot_general(
        either, normed, (((0,), (0,)), ((), ())), preferred_element_type=jnp.float32
    )
    payload_ref[...] = payload.astype(jnp.bfloat16).reshape(payload_ref.shape)


def dispatch(x, gain, targets, experts, slots_each):
    tokens, model = x.shape
    slots = experts * slots_each
    return pl.pallas_call(
        dispatch_kernel,
        out_shape=[
            jax.ShapeDtypeStruct((tokens, model), jnp.bfloat16),
            jax.ShapeDtypeStruct((2, tokens, slots), jnp.bfloat16),
            jax.ShapeDtypeStruct((experts, slots_each // 2, 2, model), jnp.bfloat16),
        ],
        compiler_params=pltpu.CompilerParams(vmem_limit_bytes=16 << 20),
        name="dispatch",
    )(x, gain.reshape(1, model), targets)


def route_weights(rows, group_router, expert_router, route_rows):
    group_logits = jnp.dot(rows, group_router, preferred_element_type=jnp.float32)
    expert_logits = jnp.dot(rows, expert_router, preferred_element_type=jnp.float32)
    groups = group_logits.shape[1]
    experts = expert_logits.shape[1]
    member = (
        jnp.arange(experts, dtype=jnp.int32)[:, None] // (experts // groups)
        == jnp.arange(groups, dtype=jnp.int32)[None, :]
    ).astype(jnp.float32)
    group_exp = jnp.exp(group_logits)
    group_prob = group_exp / jnp.sum(group_exp, axis=1, keepdims=True)
    expert_exp = jnp.exp(expert_logits)
    within = jnp.dot(expert_exp, member, precision=lax.Precision.HIGHEST)
    prob = expert_exp * jnp.dot(group_prob / within, member.T, precision=lax.Precision.HIGHEST)
    chosen = (route_rows[:, :, None] == jnp.arange(experts, dtype=jnp.int32)[None, None, :]).astype(
        jnp.float32
    )
    picked = jnp.sum(chosen * prob[:, None, :], axis=2)
    return picked / jnp.sum(picked, axis=1, keepdims=True)


def combine_kernel(returned_ref, pick_ref, weight_ref, own_ref, other_ref):
    returned = returned_ref[...].reshape(pick_ref.shape[2], returned_ref.shape[-1])
    weight = weight_ref[...]
    total = jnp.dot(pick_ref[0], returned, preferred_element_type=jnp.float32) * weight[:, 0:1]
    total = total + jnp.dot(pick_ref[1], returned, preferred_element_type=jnp.float32) * weight[:, 1:2]
    rows = own_ref.shape[0]
    own_ref[...] = total[:rows]
    other_ref[...] = total[rows:].astype(jnp.bfloat16)


def combine(returned, pick, weight):
    shape = (pick.shape[1] // 2, returned.shape[-1])
    return pl.pallas_call(
        combine_kernel,
        out_shape=[
            jax.ShapeDtypeStruct(shape, jnp.float32),
            jax.ShapeDtypeStruct(shape, jnp.bfloat16),
        ],
        compiler_params=pltpu.CompilerParams(vmem_limit_bytes=12 << 20),
        name="combine",
    )(returned, pick, weight)


def fetch(flag_ref, pair, target, sem):
    @pl.when(flag_ref[0] == 1)
    def _():
        pltpu.make_async_copy(pair[0], target, sem).start()

    @pl.when(flag_ref[0] != 1)
    def _():
        pltpu.make_async_copy(pair[1], target, sem).start()

    return pltpu.make_async_copy(pair[0], target, sem)


def hidden_kernel(flag_ref, rows_ref, *refs):
    out_ref, gate_scratch, up_scratch, sems = refs[-4:]
    count = gate_scratch.shape[0]
    units = gate_scratch.shape[2]

    def start(q):
        pairs = (refs[4 * q], refs[4 * q + 1]), (refs[4 * q + 2], refs[4 * q + 3])
        targets = gate_scratch.at[q], up_scratch.at[q]
        return [fetch(flag_ref, pairs[i], targets[i], sems.at[q, i]) for i in range(2)]

    waits = [start(0), start(1)]
    rows = rows_ref[...].reshape(out_ref.shape[0], rows_ref.shape[-1])
    for q in range(count):
        waits[q][0].wait()
        waits[q][1].wait()
        if q + 2 < count:
            waits.append(start(q + 2))
        gate = jnp.dot(rows, gate_scratch[q], preferred_element_type=jnp.float32)
        up = jnp.dot(rows, up_scratch[q], preferred_element_type=jnp.float32)
        out_ref[:, q * units : (q + 1) * units] = (gate / (1.0 + jnp.exp(-gate)) * up).astype(
            jnp.bfloat16
        )


def hidden_of(flag, rows, gates, ups):
    model, units = gates[0][0].shape
    count = rows.size // model
    parts = len(gates)
    arrays = [array for gate, up in zip(gates, ups) for array in (*gate, *up)]
    return pl.pallas_call(
        hidden_kernel,
        out_shape=jax.ShapeDtypeStruct((count, parts * units), jnp.bfloat16),
        in_specs=[
            pl.BlockSpec(memory_space=pltpu.SMEM),
            pl.BlockSpec(memory_space=pltpu.VMEM),
        ]
        + [pl.BlockSpec(memory_space=pltpu.HBM)] * len(arrays),
        scratch_shapes=[
            pltpu.VMEM((parts, model, units), jnp.bfloat16),
            pltpu.VMEM((parts, model, units), jnp.bfloat16),
            pltpu.SemaphoreType.DMA((parts, 2)),
        ],
        compiler_params=pltpu.CompilerParams(vmem_limit_bytes=58 << 20),
        cost_estimate=pl.CostEstimate(
            flops=4 * count * model * units * parts, bytes_accessed=9 << 20, transcendentals=0
        ),
        name="hidden",
    )(flag, rows, *arrays)


DOWN_COLUMNS = 512


def down_kernel(flag_ref, hidden_ref, *refs):
    out_ref, scratch, result, sems, out_sems = refs[-5:]
    parts, units, model = scratch.shape
    steps = model // DOWN_COLUMNS
    waits = []
    for n in range(steps):
        columns = pl.ds(n * DOWN_COLUMNS, DOWN_COLUMNS)
        waits.append(
            [
                fetch(
                    flag_ref,
                    (refs[2 * q].at[:, columns], refs[2 * q + 1].at[:, columns]),
                    scratch.at[q, :, columns],
                    sems.at[n, q],
                )
                for q in range(parts)
            ]
        )
    leaving = []
    for n in range(steps):
        columns = slice(n * DOWN_COLUMNS, (n + 1) * DOWN_COLUMNS)
        total = None
        for q in range(parts):
            waits[n][q].wait()
            piece = jnp.dot(
                hidden_ref[:, q * units : (q + 1) * units],
                scratch[q, :, columns],
                preferred_element_type=jnp.float32,
            )
            total = piece if total is None else total + piece
        result[n] = total.astype(jnp.bfloat16).reshape(result.shape[1:])
        leaving.append(
            pltpu.make_async_copy(
                result.at[n],
                out_ref.at[:, :, :, pl.ds(n * DOWN_COLUMNS, DOWN_COLUMNS)],
                out_sems.at[n],
            )
        )
        leaving[-1].start()
    for copy in leaving:
        copy.wait()


def down_of(flag, hidden, downs, out_shape):
    units, model = downs[0][0].shape
    parts = len(downs)
    arrays = [array for pair in downs for array in pair]
    return pl.pallas_call(
        down_kernel,
        out_shape=out_shape,
        in_specs=[
            pl.BlockSpec(memory_space=pltpu.SMEM),
            pl.BlockSpec(memory_space=pltpu.VMEM),
        ]
        + [pl.BlockSpec(memory_space=pltpu.HBM)] * len(arrays),
        out_specs=pl.BlockSpec(memory_space=pltpu.HBM),
        scratch_shapes=[
            pltpu.VMEM((parts, units, model), jnp.bfloat16),
            pltpu.VMEM(
                (model // DOWN_COLUMNS,) + out_shape.shape[:3] + (DOWN_COLUMNS,), jnp.bfloat16
            ),
            pltpu.SemaphoreType.DMA((model // DOWN_COLUMNS, parts)),
            pltpu.SemaphoreType.DMA((model // DOWN_COLUMNS,)),
        ],
        compiler_params=pltpu.CompilerParams(vmem_limit_bytes=58 << 20),
        cost_estimate=pl.CostEstimate(
            flops=2 * hidden.size * model, bytes_accessed=6 << 20, transcendentals=0
        ),
        name="down",
    )(flag, hidden, *arrays)


def exchange(rows):
    return lax.all_to_all(rows, "ep", split_axis=0, concat_axis=0, tiled=True)


def layer(
    mixer_input,
    mixer_gain,
    pool_in,
    pool_map,
    pool_scale,
    pool_out,
    expert_input,
    expert_gain,
    group_router,
    expert_router,
    routes,
    gate_weight,
    up_weight,
    down_weight,
):
    tp_count = lax.axis_size("tp")
    tp_place = lax.axis_index("tp")
    experts = expert_router.shape[1]
    block_len = expert_input.shape[0] // tp_count
    slots_each = 4 * block_len // experts

    gates = parts_of(gate_weight[0])
    ups = parts_of(up_weight[0])
    downs = parts_of(down_weight[0])

    starts = [tp_place * block_len, (tp_place ^ 1) * block_len]
    pair_input = jnp.concatenate(
        [lax.dynamic_slice_in_dim(expert_input, start, block_len, 0) for start in starts], axis=0
    )
    pair_routes = jnp.concatenate(
        [lax.dynamic_slice_in_dim(routes, start, block_len, 0) for start in starts], axis=0
    )
    parity = tp_place % 2
    core = jnp.where(jnp.arange(2 * block_len) < block_len, parity, 1 - parity)[:, None]
    targets = jnp.where(pair_routes % 2 == parity, pair_routes - parity + core, -1)
    normed, pick, payload = dispatch(pair_input, expert_gain, targets, experts, slots_each)
    rows = exchange(payload)

    partial_rows = mixer_partial(mixer_input, mixer_gain, pool_in, pool_map, pool_scale, pool_out)
    mixer_output = mixer_reduce(partial_rows)
    weight = route_weights(normed, group_router, expert_router, pair_routes)

    flag = (lax.axis_index("ep") % 2 == parity).astype(jnp.int32).reshape(1)
    hidden = hidden_of(flag, rows, gates, ups)
    result = down_of(
        flag, hidden, downs, jax.ShapeDtypeStruct(payload.shape, jnp.bfloat16)
    )
    returned = exchange(result)
    own, other = combine(returned, pick, weight)
    expert_output = (own + swapped(other, 1).astype(jnp.float32)).astype(jnp.bfloat16)
    return (mixer_output, expert_output)


def solution(mesh):
    return jax.shard_map(
        layer,
        mesh=mesh,
        in_specs=(
            P("ep", None),
            P(),
            P(None, "tp"),
            P("tp", None, None),
            P("tp"),
            P("tp", None),
            P("ep", None),
            P(),
            P(),
            P(),
            P("ep", None),
            P("ep", None, "tp"),
            P("ep", None, "tp"),
            P("ep", "tp", None),
        ),
        out_specs=(P(("ep", "tp"), None), P(("ep", "tp"), None)),
        check_vma=False,
    )
```

time: 218 us -> 177 us (0.81)
  starting transfers between devices: 60 us -> 39.2 us
  waiting for transfers between devices: 97.7 us -> 90.1 us
  local copies, waits for them, and re-layouts: 16.4 us -> 9.94 us
  matrix products: 15.3 us -> 10.3 us
  Pallas kernels: 20.5 us -> 17.2 us
    ppermute x21 -> x4, waiting for transfers between devices: 97.7 us -> 5.43 us  [swapped(): lax.ppermute(value, 'tp', [(source, source ^ mask) for source in range(co...]
    ppermute x0 -> x12, waiting for transfers between devices: none -> 65.4 us  [sent(): return lax.ppermute(value, ('ep', 'tp'), pairs)]
    all_to_all x3 -> x2, waiting for transfers between devices: 0.01 us -> 19.3 us  [exchange(): return lax.all_to_all(rows, 'ep', split_axis=0, concat_axis=0, tiled=True)]
    ppermute x21 -> x4, starting transfers between devices: 24.7 us -> 6.16 us  [swapped(): lax.ppermute(value, 'tp', [(source, source ^ mask) for source in range(co...]
    all_to_all x3 -> x2, starting transfers between devices: 33.3 us -> 22.9 us  [exchange(): return lax.all_to_all(rows, 'ep', split_axis=0, concat_axis=0, tiled=True)]
    ppermute x0 -> x12, starting transfers between devices: none -> 7.69 us  [sent(): return lax.ppermute(value, ('ep', 'tp'), pairs)]
    dot_general x1, matrix products: 8.88 us -> 3.91 us  [mixer_partial(): jnp.dot(mixed_rows, pool_out, preferred_element_type=jnp.float32)]
    pallas_call x10 -> x3, Pallas kernels: 19.5 us -> 14.9 us  [the longest x1 7.94 us: hidden_of(): pl.pallas_call(hidden_kernel, out_shape=jax.ShapeDtypeStruct((count, part...]
  transfers between devices with their start and end apart: 25 -> 19, of which waited for: 9 -> 7; matrix products, arithmetic and copies ran while one was open for 13% -> 12% of each run, Pallas kernels for 8% -> 8%
where the time goes in v3:
time: 177 us; the launch traced here: 176 us
  waiting for transfers between devices  90.1 us (51%)
  starting transfers between devices  39.2 us (22%)
  Pallas kernels  17.2 us (10%)
  matrix products  10.3 us (6%)
  local copies, waits for them, and re-layouts  9.94 us (6%)
  other arithmetic  7.9 us (4%)
    ppermute x12, waiting for transfers between devices, sent(): return lax.ppermute(value, ('ep', 'tp'), pairs)  65.4 us
    all_to_all x2, starting transfers between devices, exchange(): return lax.all_to_all(rows, 'ep', split_axis=0, concat_axis=0, tiled=True)  22.9 us
    all_to_all x2, waiting for transfers between devices, exchange(): return lax.all_to_all(rows, 'ep', split_axis=0, concat_axis=0, tiled=True)  19.3 us
    pallas_call x1, Pallas kernels, hidden_of(): pl.pallas_call(hidden_kernel, out_shape=jax.ShapeDtypeStruct((count, part...  7.94 us
    ppermute x12, starting transfers between devices, sent(): return lax.ppermute(value, ('ep', 'tp'), pairs)  7.69 us
    ppermute x4, starting transfers between devices, swapped(): lax.ppermute(value, 'tp', [(source, source ^ mask) for source in range(co...  6.16 us
    pallas_call x1, Pallas kernels, down_of(): pl.pallas_call(down_kernel, out_shape=out_shape, in_specs=[pl.BlockSpec(m...  5.92 us
    ppermute x4, waiting for transfers between devices, swapped(): lax.ppermute(value, 'tp', [(source, source ^ mask) for source in range(co...  5.43 us
  transfers between devices with their start and end apart: 19, of which 7 were waited for; matrix products, arithmetic and copies ran while one was open for 12% of the time, Pallas kernels for 8%

profile of v3, /device:TPU:8, one launch (start us, length us, event | category | flops | bytes accessed | tf_op | source)
XLA Modules:
  0.0 175.7 jit_solution(16156590707038737157)
XLA Ops:
  4.1 2.3 %dispatch.1 = (bf16[192,2048]{1,0:T(8,128)(2,1)S(1)}, bf16[2,192,384]{2,1,0:T(8,128)(2,1)S(1)}, bf16[64,3,2,2048]{3,2,1,0:T(2,128)(2,1)}) custom-call(bf16[192,2048]{1,0:T(8,128)(2,1)S(1)} %pad_maximum_fusion.x_ref, bf16[1,2048]{1,0:T(2,128)(2,1)S(1)} %reshape.268.gain_ref, s32[192,2]{1,0:T(8,128)S(1)} %fusion.40.targets_ref), custom_call_target="tpu_custom_call" | custom-call | tf_op jit(solution)/shard_map/dispatch/pallas_call | solution.py:139
  7.2 12.1 %all-to-all-start = ((bf16[64,3,2,2048]{3,2,1,0:T(2,128)(2,1)}), bf16[64,3,2,2048]{3,2,1,0:T(2,128)(2,1)S(1)}, u32[]{:S(2)}, u32[]{:S(2)}) async-start(bf16[64,3,2,2048]{3,2,1,0:T(2,128)(2,1)} %get-tuple-element.7), calls=%async_computation | async-start | bytes 3145728 | tf_op jit(solution)/shard_map/all_to_all | solution.py:333
  19.3 2.8 %collective-permute-start.10 = (bf16[2048,256]{1,0:T(8,128)(2,1)}, bf16[2048,256]{1,0:T(8,128)(2,1)S(1)}, u32[]{:S(2)}, u32[]{:S(2)}) collective-permute-start(bf16[2048,256]{1,0:T(8,128)(2,1)} %bitcast.20), channel_id=1, source_target_pairs={{0,6},{1,2},{2,4},{3,0},{4,7},{5,3},{6,5},{7,1},{8,14},{9,10},{10,... | collective-permute-start | bytes 3145736 | tf_op jit(solution)/shard_map/ppermute | solution.py:33
  22.8 1.6 collective-permute-start.8
  24.5 23.8 %collective-permute-done.10.refs_10_.refs_15_ = bf16[2048,256]{1,0:T(8,128)(2,1)S(1)} collective-permute-done((bf16[2048,256]{1,0:T(8,128)(2,1)}, bf16[2048,256]{1,0:T(8,128)(2,1)S(1)}, u32[]{:S(2)}, u32[]{:S(2)}) %collective-permute-start.10) | collective-permute-done | bytes 1048608 | tf_op jit(solution)/shard_map/ppermute | solution.py:33
  49.7 21.2 %collective-permute-done.5.refs_3_.refs_6_ = bf16[2048,256]{1,0:T(8,128)(2,1)} collective-permute-done((bf16[2048,256]{1,0:T(8,128)(2,1)}, bf16[2048,256]{1,0:T(8,128)(2,1)}, u32[]{:S(2)}, u32[]{:S(2)}) %collective-permute-start.5) | collective-permute-done | bytes 1048608 | tf_op jit(solution)/shard_map/ppermute | solution.py:33
  71.4 20.3 %collective-permute-done.12.refs_1_.refs_2_ = bf16[256,2048]{1,0:T(8,128)(2,1)} collective-permute-done((bf16[256,2048]{1,0:T(8,128)(2,1)}, bf16[256,2048]{1,0:T(8,128)(2,1)}, u32[]{:S(2)}, u32[]{:S(2)}) %collective-permute-start.12) | collective-permute-done | bytes 1048608 | tf_op jit(solution)/shard_map/ppermute | solution.py:33
  94.3 1.6 fusion.41
  95.9 2.5 %collective-permute-start = (bf16[15,256]{1,0:T(8,128)(2,1)S(1)}, bf16[15,256]{1,0:T(8,128)(2,1)S(1)}, u32[]{:S(2)}, u32[]{:S(2)}) collective-permute-start(bf16[15,256]{1,0:T(8,128)(2,1)S(1)} %slice.254), channel_id=1, source_target_pairs={{0,4},{4,8},{8,12},{12,16},{16,20},{20,24},{24,28},{28,32},{32,36}... | collective-permute-start | bytes 23048 | tf_op jit(solution)/shard_map/ppermute | solution.py:16
  99.6 7.9 %hidden.1.hidden_ref = bf16[384,1024]{1,0:T(8,128)(2,1)} custom-call(s32[1]{0:T(128)} %bitcast.1.flag_ref, bf16[64,3,2,2048]{3,2,1,0:T(2,128)(2,1)} %copy-done.3, bf16[2048,256]{1,0:T(8,128)(2,1)} %bitcast.19, bf16[2048,256]{1,0:T(8,128)(2,1)} %collective-permute-done.4.refs_1_.refs_4_, bf16[2048,256]{1,0:T(8,128)(2,1)} %bitcast.22, ...), custom_call_target="tpu_custom_call" | custom-call | flops 3221225472 | bytes 9437184 | tf_op jit(solution)/shard_map/hidden/pallas_call | solution.py:236
  107.6 5.9 %down.1 = bf16[64,3,2,2048]{3,2,1,0:T(2,128)(2,1)} custom-call(s32[1]{0:T(128)} %bitcast.1.flag_ref, bf16[384,1024]{1,0:T(8,128)(2,1)} %hidden.1.hidden_ref, bf16[256,2048]{1,0:T(8,128)(2,1)} %bitcast.25, bf16[256,2048]{1,0:T(8,128)(2,1)} %collective-permute-done.12.refs_1_.refs_2_, bf16[256,2048]{1,0:T(8,128)(2,1)} %collective-permute-done.12.refs_1_.refs_2_, ...), custom_call_target="tpu_custom_call" | custom-call | flops 1610612736 | bytes 6291456 | tf_op jit(solution)/shard_map/down/pallas_call | solution.py:307
  113.5 10.8 %all-to-all-start.1 = ((bf16[64,3,2,2048]{3,2,1,0:T(2,128)(2,1)}), bf16[64,3,2,2048]{3,2,1,0:T(2,128)(2,1)S(1)}, u32[]{:S(2)}, u32[]{:S(2)}) async-start(bf16[64,3,2,2048]{3,2,1,0:T(2,128)(2,1)} %down.1), calls=%async_computation.1 | async-start | bytes 3145728 | tf_op jit(solution)/shard_map/all_to_all | solution.py:333
  124.3 2.1 %fusion = f32[512]{0:T(512)S(1)} fusion(bf16[512,2048]{1,0:T(8,128)(2,1)} %param.14), kind=kLoop, calls=%fused_computation.2 | loop fusion | flops 3145216 | bytes 2099200 | tf_op jit(solution)/shard_map/reduce_sum | solution.py:46
  126.8 1.3 convolution_exponential_fusion
  129.0 2.6 %fusion.7 = bf16[512,256]{1,0:T(8,128)(2,1)S(1)} fusion(bf16[2048,256]{1,0:T(8,128)(2,1)} %param.16, bf16[512,2048]{1,0:T(8,128)(2,1)} %param.14, f32[2048]{0:T(1024)S(1)} %convert_element_type.136, f32[512]{0:T(512)S(1)} %add_rsqrt_fusion), kind=kOutput, calls=%fused_computation.10 | convolution fusion | flops 541196288 | bytes 3418112 | tf_op jit(solution)/shard_map/dot_general | solution.py:52
  131.9 3.9 %convolution_convert_fusion = bf16[512,2048]{1,0:T(8,128)(2,1)} fusion(bf16[256,2048]{1,0:T(8,128)(2,1)S(1)} %copy-done, f32[256]{0:T(256)S(1)} %convert_element_type.161, f32[527,256]{1,0:T(8,128)S(1)} %maximum_convert_fusion, f32[512]{0:T(512)S(1)} %minimum_convert_fusion, f32[]{:T(128)S(6)} %convert_element_type.158, f32[]{:T(128)S(6)} %convert_element_type.157, ...), kind=kOutput, calls=%fused_computation.5 | convolution fusion | flops 609746944 | bytes 11668544 | tf_op jit(solution)/shard_map/dot_general | solution.py:76
  135.8 2.5 %constant_dynamic-slice_fusion.6 = (bf16[128,2048]{1,0:T(8,128)(2,1)}, bf16[128,2048]{1,0:T(8,128)(2,1)S(1)}, bf16[128,2048]{1,0:T(8,128)(2,1)}) fusion(bf16[512,2048]{1,0:T(8,128)(2,1)} %convolution_convert_fusion, s32[]{:T(128)S(6)} %select_n.62, s32[]{:T(128)S(6)} %select_n.64, s32[]{:T(128)S(6)} %select_n.63), kind=kLoop, calls=%fused_computation.88 | loop fusion | bytes 3145740 | tf_op jit(solution)/shard_map/dynamic_slice | solution.py:85
  138.3 1.4 collective-permute-start.1
  139.7 1.3 collective-permute-start.2
  141.0 2.0 %collective-permute-start.3 = (bf16[128,2048]{1,0:T(8,128)(2,1)S(1)}, bf16[128,2048]{1,0:T(8,128)(2,1)}, u32[]{:S(2)}, u32[]{:S(2)}) collective-permute-start(bf16[128,2048]{1,0:T(8,128)(2,1)S(1)} %get-tuple-element.15), channel_id=1, source_target_pairs={{0,3},{1,2},{2,1},{3,0},{4,7},{5,6},{6,5},{7,4},{8,11},{9,10},{10,... | collective-permute-start | bytes 1572872 | tf_op jit(solution)/shard_map/ppermute | solution.py:21
  145.1 19.3 %all-to-all-done.1.returned_ref = bf16[64,3,2,2048]{3,2,1,0:T(2,128)(2,1)S(1)} async-done(((bf16[64,3,2,2048]{3,2,1,0:T(2,128)(2,1)}), bf16[64,3,2,2048]{3,2,1,0:T(2,128)(2,1)S(1)}, u32[]{:S(2)}, u32[]{:S(2)}) %all-to-all-start.1) | async-done | bytes 1572896 | tf_op jit(solution)/shard_map/all_to_all | solution.py:333
  165.4 1.5 collective-permute-start.16
  167.0 2.6 %add_convert_fusion = bf16[128,2048]{1,0:T(8,128)(2,1)} fusion(bf16[128,2048]{1,0:T(8,128)(2,1)} %collective-permute-done.3, bf16[128,2048]{1,0:T(8,128)(2,1)} %collective-permute-done.2, bf16[128,2048]{1,0:T(8,128)(2,1)} %collective-permute-done.1, bf16[512,2048]{1,0:T(8,128)(2,1)} %convolution_convert_fusion, s32[]{:T(128)S(6)} %select_n.61), kind=kLoop, calls=%fused_computation.17 | loop fusion | flops 2097152 | bytes 2621444 | tf_op jit(solution)/shard_map/convert_element_type | solution.py:91
  169.6 5.3 %collective-permute-done.16 = bf16[96,2048]{1,0:T(8,128)(2,1)S(1)} collective-permute-done((bf16[96,2048]{1,0:T(8,128)(2,1)S(1)}, bf16[96,2048]{1,0:T(8,128)(2,1)S(1)}, u32[]{:S(2)}, u32[]{:S(2)}) %collective-permute-start.16) | collective-permute-done | bytes 393248 | tf_op jit(solution)/shard_map/ppermute | solution.py:21
  (74 shorter events, 15.9 us)
Async XLA Ops:
  0.6 131.2 %copy-start = (bf16[256,2048]{1,0:T(8,128)(2,1)S(1)}, bf16[256,2048]{1,0:T(8,128)(2,1)}, u32[]{:S(2)}) copy-start(bf16[256,2048]{1,0:T(8,128)(2,1)} %param.19) | copy-start | bytes 3145732
  4.1 89.3 %copy-start.9 = (bf16[2048]{0:T(1024)(128)(2,1)S(1)}, bf16[2048]{0:T(1024)(128)(2,1)}, u32[]{:S(2)}) copy-start(bf16[2048]{0:T(1024)(128)(2,1)} %param.15) | copy-start | bytes 12292
  7.2 91.2 %all-to-all-start = ((bf16[64,3,2,2048]{3,2,1,0:T(2,128)(2,1)}), bf16[64,3,2,2048]{3,2,1,0:T(2,128)(2,1)S(1)}, u32[]{:S(2)}, u32[]{:S(2)}) async-start(bf16[64,3,2,2048]{3,2,1,0:T(2,128)(2,1)} %get-tuple-element.7), calls=%async_computation | async-start | bytes 3145728 | tf_op jit(solution)/shard_map/all_to_all | solution.py:333
  19.3 29.0 %collective-permute-start.10 = (bf16[2048,256]{1,0:T(8,128)(2,1)}, bf16[2048,256]{1,0:T(8,128)(2,1)S(1)}, u32[]{:S(2)}, u32[]{:S(2)}) collective-permute-start(bf16[2048,256]{1,0:T(8,128)(2,1)} %bitcast.20), channel_id=1, source_target_pairs={{0,6},{1,2},{2,4},{3,0},{4,7},{5,3},{6,5},{7,1},{8,14},{9,10},{10,... | collective-permute-start | bytes 3145736 | tf_op jit(solution)/shard_map/ppermute | solution.py:33
  22.1 27.4 %collective-permute-start.4 = (bf16[2048,256]{1,0:T(8,128)(2,1)}, bf16[2048,256]{1,0:T(8,128)(2,1)}, u32[]{:S(2)}, u32[]{:S(2)}) collective-permute-start(bf16[2048,256]{1,0:T(8,128)(2,1)} %bitcast.17), channel_id=1, source_target_pairs={{0,4},{1,0},{2,6},{3,2},{4,5},{5,1},{6,7},{7,3},{8,12},{9,8},{10,1... | collective-permute-start | bytes 3145736 | tf_op jit(solution)/shard_map/ppermute | solution.py:33
  22.1 48.8 %collective-permute-start.5 = (bf16[2048,256]{1,0:T(8,128)(2,1)}, bf16[2048,256]{1,0:T(8,128)(2,1)}, u32[]{:S(2)}, u32[]{:S(2)}) collective-permute-start(bf16[2048,256]{1,0:T(8,128)(2,1)} %bitcast.21), channel_id=1, source_target_pairs={{0,4},{1,0},{2,6},{3,2},{4,5},{5,1},{6,7},{7,3},{8,12},{9,8},{10,1... | collective-permute-start | bytes 3145736 | tf_op jit(solution)/shard_map/ppermute | solution.py:33
  22.8 48.1 %collective-permute-start.8 = (bf16[2048,256]{1,0:T(8,128)(2,1)}, bf16[2048,256]{1,0:T(8,128)(2,1)}, u32[]{:S(2)}, u32[]{:S(2)}) collective-permute-start(bf16[2048,256]{1,0:T(8,128)(2,1)} %bitcast.18), channel_id=1, source_target_pairs={{0,6},{1,2},{2,4},{3,0},{4,7},{5,3},{6,5},{7,1},{8,14},{9,10},{10,... | collective-permute-start | bytes 3145736 | tf_op jit(solution)/shard_map/ppermute | solution.py:33
  24.5 67.3 %collective-permute-start.12 = (bf16[256,2048]{1,0:T(8,128)(2,1)}, bf16[256,2048]{1,0:T(8,128)(2,1)}, u32[]{:S(2)}, u32[]{:S(2)}) collective-permute-start(bf16[256,2048]{1,0:T(8,128)(2,1)} %bitcast.23), channel_id=1, source_target_pairs={{0,4},{1,0},{2,6},{3,2},{4,5},{5,1},{6,7},{7,3},{8,12},{9,8},{10,1... | collective-permute-start | bytes 3145736 | tf_op jit(solution)/shard_map/ppermute | solution.py:33
  48.2 43.6 %collective-permute-start.14 = (bf16[256,2048]{1,0:T(8,128)(2,1)}, bf16[256,2048]{1,0:T(8,128)(2,1)}, u32[]{:S(2)}, u32[]{:S(2)}) collective-permute-start(bf16[256,2048]{1,0:T(8,128)(2,1)} %bitcast.24), channel_id=1, source_target_pairs={{0,6},{1,2},{2,4},{3,0},{4,7},{5,3},{6,5},{7,1},{8,14},{9,10},{10,... | collective-permute-start | bytes 3145736 | tf_op jit(solution)/shard_map/ppermute | solution.py:33
  49.6 42.7 %collective-permute-start.11 = (bf16[2048,256]{1,0:T(8,128)(2,1)S(1)}, bf16[2048,256]{1,0:T(8,128)(2,1)S(1)}, u32[]{:S(2)}, u32[]{:S(2)}) collective-permute-start(bf16[2048,256]{1,0:T(8,128)(2,1)S(1)} %collective-permute-done.10.refs_10_.refs_15_), channel_id=1, source_target_pairs={{0,4},{1,5},{2,6},{3,7},{4,0},{5,1},{6,2},{7,3},{8,12},{9,13},{10,... | collective-permute-start | bytes 3145736 | tf_op jit(solution)/shard_map/ppermute | solution.py:33
  70.9 25.0 %collective-permute-start.6 = (bf16[2048,256]{1,0:T(8,128)(2,1)}, bf16[2048,256]{1,0:T(8,128)(2,1)}, u32[]{:S(2)}, u32[]{:S(2)}) collective-permute-start(bf16[2048,256]{1,0:T(8,128)(2,1)} %collective-permute-done.4.refs_1_.refs_4_), channel_id=1, source_target_pairs={{0,4},{1,5},{2,6},{3,7},{4,0},{5,1},{6,2},{7,3},{8,12},{9,13},{10,... | collective-permute-start | bytes 3145736 | tf_op jit(solution)/shard_map/ppermute | solution.py:33
  70.9 27.5 %collective-permute-start.7 = (bf16[2048,256]{1,0:T(8,128)(2,1)}, bf16[2048,256]{1,0:T(8,128)(2,1)}, u32[]{:S(2)}, u32[]{:S(2)}) collective-permute-start(bf16[2048,256]{1,0:T(8,128)(2,1)} %collective-permute-done.5.refs_3_.refs_6_), channel_id=1, source_target_pairs={{0,4},{1,5},{2,6},{3,7},{4,0},{5,1},{6,2},{7,3},{8,12},{9,13},{10,... | collective-permute-start | bytes 3145736 | tf_op jit(solution)/shard_map/ppermute | solution.py:33
  91.7 6.7 %collective-permute-start.9 = (bf16[2048,256]{1,0:T(8,128)(2,1)}, bf16[2048,256]{1,0:T(8,128)(2,1)}, u32[]{:S(2)}, u32[]{:S(2)}) collective-permute-start(bf16[2048,256]{1,0:T(8,128)(2,1)} %collective-permute-done.8.refs_8_.refs_13_), channel_id=1, source_target_pairs={{0,4},{1,5},{2,6},{3,7},{4,0},{5,1},{6,2},{7,3},{8,12},{9,13},{10,... | collective-permute-start | bytes 3145736 | tf_op jit(solution)/shard_map/ppermute | solution.py:33
  91.9 15.7 %collective-permute-start.13 = (bf16[256,2048]{1,0:T(8,128)(2,1)}, bf16[256,2048]{1,0:T(8,128)(2,1)}, u32[]{:S(2)}, u32[]{:S(2)}) collective-permute-start(bf16[256,2048]{1,0:T(8,128)(2,1)} %collective-permute-done.12.refs_1_.refs_2_), channel_id=1, source_target_pairs={{0,4},{1,5},{2,6},{3,7},{4,0},{5,1},{6,2},{7,3},{8,12},{9,13},{10,... | collective-permute-start | bytes 3145736 | tf_op jit(solution)/shard_map/ppermute | solution.py:33
  93.2 14.3 %collective-permute-start.15 = (bf16[256,2048]{1,0:T(8,128)(2,1)}, bf16[256,2048]{1,0:T(8,128)(2,1)}, u32[]{:S(2)}, u32[]{:S(2)}) collective-permute-start(bf16[256,2048]{1,0:T(8,128)(2,1)} %collective-permute-done.14.refs_4_.refs_7_), channel_id=1, source_target_pairs={{0,4},{1,5},{2,6},{3,7},{4,0},{5,1},{6,2},{7,3},{8,12},{9,13},{10,... | collective-permute-start | bytes 3145736 | tf_op jit(solution)/shard_map/ppermute | solution.py:33
  95.9 35.9 %collective-permute-start = (bf16[15,256]{1,0:T(8,128)(2,1)S(1)}, bf16[15,256]{1,0:T(8,128)(2,1)S(1)}, u32[]{:S(2)}, u32[]{:S(2)}) collective-permute-start(bf16[15,256]{1,0:T(8,128)(2,1)S(1)} %slice.254), channel_id=1, source_target_pairs={{0,4},{4,8},{8,12},{12,16},{16,20},{20,24},{24,28},{28,32},{32,36}... | collective-permute-start | bytes 23048 | tf_op jit(solution)/shard_map/ppermute | solution.py:16
  113.5 12.9 %copy-start.8 = (bf16[2048,4]{0,1:T(4,128)(2,1)S(1)}, bf16[2048,4]{0,1:T(4,128)(2,1)}, u32[]{:S(2)}) copy-start(bf16[2048,4]{0,1:T(4,128)(2,1)} %param.22) | copy-start | bytes 49156
  113.5 50.8 %all-to-all-start.1 = ((bf16[64,3,2,2048]{3,2,1,0:T(2,128)(2,1)}), bf16[64,3,2,2048]{3,2,1,0:T(2,128)(2,1)S(1)}, u32[]{:S(2)}, u32[]{:S(2)}) async-start(bf16[64,3,2,2048]{3,2,1,0:T(2,128)(2,1)} %down.1), calls=%async_computation.1 | async-start | bytes 3145728 | tf_op jit(solution)/shard_map/all_to_all | solution.py:333
  135.8 7.2 %copy-start.7 = (f32[192,64]{0,1:T(8,128)S(1)}, f32[192,64]{0,1:T(8,128)}, u32[]{:S(2)}) copy-start(f32[192,64]{0,1:T(8,128)} %copy-done.6) | copy-start | bytes 147460
  135.8 28.5 %copy-start.2 = (bf16[2,192,384]{2,1,0:T(8,128)(2,1)S(1)}, bf16[2,192,384]{2,1,0:T(8,128)(2,1)}, u32[]{:S(2)}) copy-start(bf16[2,192,384]{2,1,0:T(8,128)(2,1)} %copy-done.1) | copy-start | bytes 884740
  138.3 28.5 %collective-permute-start.1 = (bf16[128,2048]{1,0:T(8,128)(2,1)}, bf16[128,2048]{1,0:T(8,128)(2,1)}, u32[]{:S(2)}, u32[]{:S(2)}) collective-permute-start(bf16[128,2048]{1,0:T(8,128)(2,1)} %get-tuple-element.14), channel_id=1, source_target_pairs={{0,1},{1,0},{2,3},{3,2},{4,5},{5,4},{6,7},{7,6},{8,9},{9,8},{10,11... | collective-permute-start | bytes 1572872 | tf_op jit(solution)/shard_map/ppermute | solution.py:21
  139.7 27.1 %collective-permute-start.2 = (bf16[128,2048]{1,0:T(8,128)(2,1)}, bf16[128,2048]{1,0:T(8,128)(2,1)}, u32[]{:S(2)}, u32[]{:S(2)}) collective-permute-start(bf16[128,2048]{1,0:T(8,128)(2,1)} %get-tuple-element.16), channel_id=1, source_target_pairs={{0,2},{1,3},{2,0},{3,1},{4,6},{5,7},{6,4},{7,5},{8,10},{9,11},{10,... | collective-permute-start | bytes 1572872 | tf_op jit(solution)/shard_map/ppermute | solution.py:21
  141.0 25.9 %collective-permute-start.3 = (bf16[128,2048]{1,0:T(8,128)(2,1)S(1)}, bf16[128,2048]{1,0:T(8,128)(2,1)}, u32[]{:S(2)}, u32[]{:S(2)}) collective-permute-start(bf16[128,2048]{1,0:T(8,128)(2,1)S(1)} %get-tuple-element.15), channel_id=1, source_target_pairs={{0,3},{1,2},{2,1},{3,0},{4,7},{5,6},{6,5},{7,4},{8,11},{9,10},{10,... | collective-permute-start | bytes 1572872 | tf_op jit(solution)/shard_map/ppermute | solution.py:21
  165.4 9.5 %collective-permute-start.16 = (bf16[96,2048]{1,0:T(8,128)(2,1)S(1)}, bf16[96,2048]{1,0:T(8,128)(2,1)S(1)}, u32[]{:S(2)}, u32[]{:S(2)}) collective-permute-start(bf16[96,2048]{1,0:T(8,128)(2,1)S(1)} %get-tuple-element.11), channel_id=1, source_target_pairs={{0,1},{1,0},{2,3},{3,2},{4,5},{5,4},{6,7},{7,6},{8,9},{9,8},{10,11... | collective-permute-start | bytes 1179656 | tf_op jit(solution)/shard_map/ppermute | solution.py:21
  (6 other events, 7.6 us)

commit v4 on v3

--- a/solution.py
+++ b/solution.py
@@ -258,7 +258,7 @@
 
 
 def down_kernel(flag_ref, hidden_ref, *refs):
-    out_ref, scratch, result, sems, out_sems = refs[-5:]
+    out_ref, scratch, sems = refs[-3:]
     parts, units, model = scratch.shape
     steps = model // DOWN_COLUMNS
     waits = []
@@ -275,7 +275,6 @@
                 for q in range(parts)
             ]
         )
-    leaving = []
     for n in range(steps):
         columns = slice(n * DOWN_COLUMNS, (n + 1) * DOWN_COLUMNS)
         total = None
@@ -287,17 +286,9 @@
                 preferred_element_type=jnp.float32,
             )
             total = piece if total is None else total + piece
-        result[n] = total.astype(jnp.bfloat16).reshape(result.shape[1:])
-        leaving.append(
-            pltpu.make_async_copy(
-                result.at[n],
-                out_ref.at[:, :, :, pl.ds(n * DOWN_COLUMNS, DOWN_COLUMNS)],
-                out_sems.at[n],
-            )
+        out_ref[:, :, :, columns] = total.astype(jnp.bfloat16).reshape(
+            out_ref.shape[:3] + (DOWN_COLUMNS,)
         )
-        leaving[-1].start()
-    for copy in leaving:
-        copy.wait()
 
 
 def down_of(flag, hidden, downs, out_shape):
@@ -312,16 +303,11 @@
             pl.BlockSpec(memory_space=pltpu.VMEM),
         ]
         + [pl.BlockSpec(memory_space=pltpu.HBM)] * len(arrays),
-        out_specs=pl.BlockSpec(memory_space=pltpu.HBM),
         scratch_shapes=[
             pltpu.VMEM((parts, units, model), jnp.bfloat16),
-            pltpu.VMEM(
-                (model // DOWN_COLUMNS,) + out_shape.shape[:3] + (DOWN_COLUMNS,), jnp.bfloat16
-            ),
             pltpu.SemaphoreType.DMA((model // DOWN_COLUMNS, parts)),
-            pltpu.SemaphoreType.DMA((model // DOWN_COLUMNS,)),
         ],
-        compiler_params=pltpu.CompilerParams(vmem_limit_bytes=58 << 20),
+        compiler_params=pltpu.CompilerParams(vmem_limit_bytes=16 << 20),
         cost_estimate=pl.CostEstimate(
             flops=2 * hidden.size * model, bytes_accessed=6 << 20, transcendentals=0
         ),
@@ -359,7 +345,8 @@
     ups = parts_of(up_weight[0])
     downs = parts_of(down_weight[0])
 
-    starts = [tp_place * block_len, (tp_place ^ 1) * block_len]
+    toward = jnp.where(lax.axis_index("ep") % 2 == 0, 1, 3)
+    starts = [tp_place * block_len, (tp_place ^ toward) * block_len]
     pair_input = jnp.concatenate(
         [lax.dynamic_slice_in_dim(expert_input, start, block_len, 0) for start in starts], axis=0
     )
@@ -383,7 +370,13 @@
     )
     returned = exchange(result)
     own, other = combine(returned, pick, weight)
-    expert_output = (own + swapped(other, 1).astype(jnp.float32)).astype(jnp.bfloat16)
+    pairs = [
+        (device * tp_count + place, device * tp_count + (place ^ (1 + 2 * (device % 2))))
+        for device in range(lax.axis_size("ep"))
+        for place in range(tp_count)
+    ]
+    other = lax.ppermute(other, ("ep", "tp"), pairs)
+    expert_output = (own + other.astype(jnp.float32)).astype(jnp.bfloat16)
     return (mixer_output, expert_output)
 
 

time: 177 us -> 175 us (0.989)
  local copies, waits for them, and re-layouts: 9.94 us -> 12.1 us
  Pallas kernels: 17.2 us -> 15.2 us
  waiting for transfers between devices: 90.1 us -> 88.3 us
    ppermute x4 -> x3, waiting for transfers between devices: 5.43 us -> 0.2 us  [swapped(): lax.ppermute(value, 'tp', [(source, source ^ mask) for source in range(co...]
    ppermute x0 -> x1, waiting for transfers between devices: none -> 3.56 us  [layer(): other = lax.ppermute(other, ('ep', 'tp'), pairs)]
    unnamed x22 -> x28, local copies, waits for them, and re-layouts: 3.51 us -> 5.53 us
    pallas_call x1, Pallas kernels: 5.92 us -> 3.91 us  [down_of(): pl.pallas_call(down_kernel, out_shape=out_shape, in_specs=[pl.BlockSpec(m...]
    ppermute x4 -> x3, starting transfers between devices: 6.16 us -> 4.7 us  [swapped(): lax.ppermute(value, 'tp', [(source, source ^ mask) for source in range(co...]
  transfers between devices with their start and end apart: 19 -> 19, of which waited for: 7 -> 7; matrix products, arithmetic and copies ran while one was open for 12% -> 12% of each run, Pallas kernels for 8% -> 7%
where the time goes in v4:
time: 175 us; the launch traced here: 174 us
  waiting for transfers between devices  88.3 us (50%)
  starting transfers between devices  39.5 us (23%)
  Pallas kernels  15.2 us (9%)
  local copies, waits for them, and re-layouts  12.1 us (7%)
  matrix products  10.3 us (6%)
  other arithmetic  7.89 us (5%)
    ppermute x12, waiting for transfers between devices, sent(): return lax.ppermute(value, ('ep', 'tp'), pairs)  65.3 us
    all_to_all x2, starting transfers between devices, exchange(): return lax.all_to_all(rows, 'ep', split_axis=0, concat_axis=0, tiled=True)  23.2 us
    all_to_all x2, waiting for transfers between devices, exchange(): return lax.all_to_all(rows, 'ep', split_axis=0, concat_axis=0, tiled=True)  19.2 us
    pallas_call x1, Pallas kernels, hidden_of(): pl.pallas_call(hidden_kernel, out_shape=jax.ShapeDtypeStruct((count, part...  7.96 us
    ppermute x12, starting transfers between devices, sent(): return lax.ppermute(value, ('ep', 'tp'), pairs)  7.69 us
    unnamed x28, local copies, waits for them, and re-layouts  5.53 us
    ppermute x3, starting transfers between devices, swapped(): lax.ppermute(value, 'tp', [(source, source ^ mask) for source in range(co...  4.7 us
    dot_general x1, matrix products, mixer_partial(): jnp.dot(mixed_rows, pool_out, preferred_element_type=jnp.float32)  3.92 us
  transfers between devices with their start and end apart: 19, of which 7 were waited for; matrix products, arithmetic and copies ran while one was open for 12% of the time, Pallas kernels for 7%

profile of v4, /device:TPU:8, one launch (start us, length us, event | category | flops | bytes accessed | tf_op | source)
XLA Modules:
  0.0 174.3 jit_solution(10741098226346996542)
XLA Ops:
  4.2 2.3 %dispatch.1 = (bf16[192,2048]{1,0:T(8,128)(2,1)S(1)}, bf16[2,192,384]{2,1,0:T(8,128)(2,1)S(1)}, bf16[64,3,2,2048]{3,2,1,0:T(2,128)(2,1)}) custom-call(bf16[192,2048]{1,0:T(8,128)(2,1)S(1)} %pad_maximum_fusion.x_ref, bf16[1,2048]{1,0:T(2,128)(2,1)S(1)} %reshape.268.gain_ref, s32[192,2]{1,0:T(8,128)S(1)} %fusion.40.targets_ref), custom_call_target="tpu_custom_call" | custom-call | tf_op jit(solution)/shard_map/dispatch/pallas_call | solution.py:139
  8.1 12.3 %all-to-all-start = ((bf16[64,3,2,2048]{3,2,1,0:T(2,128)(2,1)}), bf16[64,3,2,2048]{3,2,1,0:T(2,128)(2,1)}, u32[]{:S(2)}, u32[]{:S(2)}) async-start(bf16[64,3,2,2048]{3,2,1,0:T(2,128)(2,1)} %get-tuple-element.7), calls=%async_computation | async-start | bytes 3145728 | tf_op jit(solution)/shard_map/all_to_all | solution.py:319
  20.3 2.8 %collective-permute-start.10 = (bf16[2048,256]{1,0:T(8,128)(2,1)}, bf16[2048,256]{1,0:T(8,128)(2,1)S(1)}, u32[]{:S(2)}, u32[]{:S(2)}) collective-permute-start(bf16[2048,256]{1,0:T(8,128)(2,1)} %bitcast.3.refs_2_), channel_id=1, source_target_pairs={{0,6},{1,2},{2,4},{3,0},{4,7},{5,3},{6,5},{7,1},{8,14},{9,10},{10,... | collective-permute-start | bytes 3145736 | tf_op jit(solution)/shard_map/ppermute | solution.py:33
  23.9 1.6 collective-permute-start.8
  25.5 23.8 %collective-permute-done.10.refs_10_.refs_15_ = bf16[2048,256]{1,0:T(8,128)(2,1)S(1)} collective-permute-done((bf16[2048,256]{1,0:T(8,128)(2,1)}, bf16[2048,256]{1,0:T(8,128)(2,1)S(1)}, u32[]{:S(2)}, u32[]{:S(2)}) %collective-permute-start.10) | collective-permute-done | bytes 1048608 | tf_op jit(solution)/shard_map/ppermute | solution.py:33
  49.3 1.4 collective-permute-start.14
  50.8 21.2 %collective-permute-done.5.refs_3_.refs_6_ = bf16[2048,256]{1,0:T(8,128)(2,1)} collective-permute-done((bf16[2048,256]{1,0:T(8,128)(2,1)}, bf16[2048,256]{1,0:T(8,128)(2,1)}, u32[]{:S(2)}, u32[]{:S(2)}) %collective-permute-start.5) | collective-permute-done | bytes 1048608 | tf_op jit(solution)/shard_map/ppermute | solution.py:33
  72.5 20.2 %collective-permute-done.12.refs_1_.refs_2_ = bf16[256,2048]{1,0:T(8,128)(2,1)S(1)} collective-permute-done((bf16[256,2048]{1,0:T(8,128)(2,1)}, bf16[256,2048]{1,0:T(8,128)(2,1)S(1)}, u32[]{:S(2)}, u32[]{:S(2)}) %collective-permute-start.12) | collective-permute-done | bytes 1048608 | tf_op jit(solution)/shard_map/ppermute | solution.py:33
  95.3 1.6 fusion.41
  96.9 2.5 %collective-permute-start = (bf16[15,256]{1,0:T(8,128)(2,1)S(1)}, bf16[15,256]{1,0:T(8,128)(2,1)S(1)}, u32[]{:S(2)}, u32[]{:S(2)}) collective-permute-start(bf16[15,256]{1,0:T(8,128)(2,1)S(1)} %slice.254), channel_id=1, source_target_pairs={{0,4},{4,8},{8,12},{12,16},{16,20},{20,24},{24,28},{28,32},{32,36}... | collective-permute-start | bytes 23048 | tf_op jit(solution)/shard_map/ppermute | solution.py:16
  99.4 8.0 %hidden.1.hidden_ref = bf16[384,1024]{1,0:T(8,128)(2,1)} custom-call(s32[1]{0:T(128)} %bitcast.1.flag_ref, bf16[64,3,2,2048]{3,2,1,0:T(2,128)(2,1)} %all-to-all-done.rows_ref, bf16[2048,256]{1,0:T(8,128)(2,1)} %bitcast.2.refs_0_, bf16[2048,256]{1,0:T(8,128)(2,1)} %collective-permute-done.4.refs_1_.refs_4_, bf16[2048,256]{1,0:T(8,128)(2,1)} %bitcast.3.refs_2_, ...), custom_call_target="tpu_custom_call" | custom-call | flops 3221225472 | bytes 9437184 | tf_op jit(solution)/shard_map/hidden/pallas_call | solution.py:236
  108.5 3.9 %down.1 = bf16[64,3,2,2048]{3,2,1,0:T(2,128)(2,1)S(1)} custom-call(s32[1]{0:T(128)} %bitcast.1.flag_ref, bf16[384,1024]{1,0:T(8,128)(2,1)S(1)} %copy-done.2, bf16[256,2048]{1,0:T(8,128)(2,1)} %bitcast.4.refs_0_, bf16[256,2048]{1,0:T(8,128)(2,1)S(1)} %collective-permute-done.12.refs_1_.refs_2_, bf16[256,2048]{1,0:T(8,128)(2,1)S(1)} %collective-permute-done.12.refs_1_.refs_2_, ...), custom_call_target="tpu_custom_call" | custom-call | flops 1610612736 | bytes 6291456 | tf_op jit(solution)/shard_map/down/pallas_call | solution.py:298
  113.6 10.9 %all-to-all-start.1 = ((bf16[64,3,2,2048]{3,2,1,0:T(2,128)(2,1)}), bf16[64,3,2,2048]{3,2,1,0:T(2,128)(2,1)S(1)}, u32[]{:S(2)}, u32[]{:S(2)}) async-start(bf16[64,3,2,2048]{3,2,1,0:T(2,128)(2,1)} %copy-done.1), calls=%async_computation.1 | async-start | bytes 3145728 | tf_op jit(solution)/shard_map/all_to_all | solution.py:319
  124.6 2.1 %fusion = f32[512]{0:T(512)S(1)} fusion(bf16[512,2048]{1,0:T(8,128)(2,1)} %param.14), kind=kLoop, calls=%fused_computation.2 | loop fusion | flops 3145216 | bytes 2099200 | tf_op jit(solution)/shard_map/reduce_sum | solution.py:46
  127.0 1.3 convolution_exponential_fusion
  129.3 2.6 %fusion.7 = bf16[512,256]{1,0:T(8,128)(2,1)S(1)} fusion(bf16[2048,256]{1,0:T(8,128)(2,1)} %param.16, bf16[512,2048]{1,0:T(8,128)(2,1)} %param.14, f32[2048]{0:T(1024)S(1)} %convert_element_type.136, f32[512]{0:T(512)S(1)} %add_rsqrt_fusion), kind=kOutput, calls=%fused_computation.10 | convolution fusion | flops 541196288 | bytes 3418112 | tf_op jit(solution)/shard_map/dot_general | solution.py:52
  132.1 3.9 %convolution_convert_fusion = bf16[512,2048]{1,0:T(8,128)(2,1)} fusion(bf16[256,2048]{1,0:T(8,128)(2,1)S(1)} %copy-done, f32[256]{0:T(256)S(1)} %convert_element_type.161, f32[527,256]{1,0:T(8,128)S(1)} %maximum_convert_fusion, f32[512]{0:T(512)S(1)} %minimum_convert_fusion, f32[]{:T(128)S(6)} %convert_element_type.158, f32[]{:T(128)S(6)} %convert_element_type.157, ...), kind=kOutput, calls=%fused_computation.5 | convolution fusion | flops 609746944 | bytes 11668544 | tf_op jit(solution)/shard_map/dot_general | solution.py:76
  136.1 2.5 %constant_dynamic-slice_fusion.6 = (bf16[128,2048]{1,0:T(8,128)(2,1)}, bf16[128,2048]{1,0:T(8,128)(2,1)S(1)}, bf16[128,2048]{1,0:T(8,128)(2,1)}) fusion(bf16[512,2048]{1,0:T(8,128)(2,1)} %convolution_convert_fusion, s32[]{:T(128)S(6)} %select_n.68, s32[]{:T(128)S(6)} %select_n.70, s32[]{:T(128)S(6)} %select_n.69), kind=kLoop, calls=%fused_computation.88 | loop fusion | bytes 3145740 | tf_op jit(solution)/shard_map/dynamic_slice | solution.py:85
  138.6 1.4 collective-permute-start.1
  141.3 2.0 %collective-permute-start.3 = (bf16[128,2048]{1,0:T(8,128)(2,1)S(1)}, bf16[128,2048]{1,0:T(8,128)(2,1)}, u32[]{:S(2)}, u32[]{:S(2)}) collective-permute-start(bf16[128,2048]{1,0:T(8,128)(2,1)S(1)} %get-tuple-element.15), channel_id=1, source_target_pairs={{0,3},{1,2},{2,1},{3,0},{4,7},{5,6},{6,5},{7,4},{8,11},{9,10},{10,... | collective-permute-start | bytes 1572872 | tf_op jit(solution)/shard_map/ppermute | solution.py:21
  145.4 19.2 %all-to-all-done.1.returned_ref = bf16[64,3,2,2048]{3,2,1,0:T(2,128)(2,1)S(1)} async-done(((bf16[64,3,2,2048]{3,2,1,0:T(2,128)(2,1)}), bf16[64,3,2,2048]{3,2,1,0:T(2,128)(2,1)S(1)}, u32[]{:S(2)}, u32[]{:S(2)}) %all-to-all-start.1) | async-done | bytes 1572896 | tf_op jit(solution)/shard_map/all_to_all | solution.py:319
  165.6 1.5 collective-permute-start.16
  167.3 2.6 %add_convert_fusion = bf16[128,2048]{1,0:T(8,128)(2,1)} fusion(bf16[128,2048]{1,0:T(8,128)(2,1)} %collective-permute-done.3, bf16[128,2048]{1,0:T(8,128)(2,1)} %collective-permute-done.2, bf16[128,2048]{1,0:T(8,128)(2,1)} %collective-permute-done.1, bf16[512,2048]{1,0:T(8,128)(2,1)} %convolution_convert_fusion, s32[]{:T(128)S(6)} %select_n.67), kind=kLoop, calls=%fused_computation.17 | loop fusion | flops 2097152 | bytes 2621444 | tf_op jit(solution)/shard_map/convert_element_type | solution.py:91
  169.9 3.6 %collective-permute-done.16 = bf16[96,2048]{1,0:T(8,128)(2,1)S(1)} collective-permute-done((bf16[96,2048]{1,0:T(8,128)(2,1)S(1)}, bf16[96,2048]{1,0:T(8,128)(2,1)S(1)}, u32[]{:S(2)}, u32[]{:S(2)}) %collective-permute-start.16) | collective-permute-done | bytes 393248 | tf_op jit(solution)/shard_map/ppermute | solution.py:378
  (80 shorter events, 18.0 us)
Async XLA Ops:
  0.6 131.5 %copy-start = (bf16[256,2048]{1,0:T(8,128)(2,1)S(1)}, bf16[256,2048]{1,0:T(8,128)(2,1)}, u32[]{:S(2)}) copy-start(bf16[256,2048]{1,0:T(8,128)(2,1)} %param.19) | copy-start | bytes 3145732
  4.2 90.2 %copy-start.12 = (bf16[2048]{0:T(1024)(128)(2,1)S(1)}, bf16[2048]{0:T(1024)(128)(2,1)}, u32[]{:S(2)}) copy-start(bf16[2048]{0:T(1024)(128)(2,1)} %param.15) | copy-start | bytes 12292
  8.1 91.4 %all-to-all-start = ((bf16[64,3,2,2048]{3,2,1,0:T(2,128)(2,1)}), bf16[64,3,2,2048]{3,2,1,0:T(2,128)(2,1)}, u32[]{:S(2)}, u32[]{:S(2)}) async-start(bf16[64,3,2,2048]{3,2,1,0:T(2,128)(2,1)} %get-tuple-element.7), calls=%async_computation | async-start | bytes 3145728 | tf_op jit(solution)/shard_map/all_to_all | solution.py:319
  20.3 29.0 %collective-permute-start.10 = (bf16[2048,256]{1,0:T(8,128)(2,1)}, bf16[2048,256]{1,0:T(8,128)(2,1)S(1)}, u32[]{:S(2)}, u32[]{:S(2)}) collective-permute-start(bf16[2048,256]{1,0:T(8,128)(2,1)} %bitcast.3.refs_2_), channel_id=1, source_target_pairs={{0,6},{1,2},{2,4},{3,0},{4,7},{5,3},{6,5},{7,1},{8,14},{9,10},{10,... | collective-permute-start | bytes 3145736 | tf_op jit(solution)/shard_map/ppermute | solution.py:33
  23.2 27.6 %collective-permute-start.4 = (bf16[2048,256]{1,0:T(8,128)(2,1)}, bf16[2048,256]{1,0:T(8,128)(2,1)}, u32[]{:S(2)}, u32[]{:S(2)}) collective-permute-start(bf16[2048,256]{1,0:T(8,128)(2,1)} %bitcast.2.refs_0_), channel_id=1, source_target_pairs={{0,4},{1,0},{2,6},{3,2},{4,5},{5,1},{6,7},{7,3},{8,12},{9,8},{10,1... | collective-permute-start | bytes 3145736 | tf_op jit(solution)/shard_map/ppermute | solution.py:33
  23.2 48.8 %collective-permute-start.5 = (bf16[2048,256]{1,0:T(8,128)(2,1)}, bf16[2048,256]{1,0:T(8,128)(2,1)}, u32[]{:S(2)}, u32[]{:S(2)}) collective-permute-start(bf16[2048,256]{1,0:T(8,128)(2,1)} %bitcast.3.refs_2_), channel_id=1, source_target_pairs={{0,4},{1,0},{2,6},{3,2},{4,5},{5,1},{6,7},{7,3},{8,12},{9,8},{10,1... | collective-permute-start | bytes 3145736 | tf_op jit(solution)/shard_map/ppermute | solution.py:33
  23.9 48.1 %collective-permute-start.8 = (bf16[2048,256]{1,0:T(8,128)(2,1)}, bf16[2048,256]{1,0:T(8,128)(2,1)}, u32[]{:S(2)}, u32[]{:S(2)}) collective-permute-start(bf16[2048,256]{1,0:T(8,128)(2,1)} %bitcast.2.refs_0_), channel_id=1, source_target_pairs={{0,6},{1,2},{2,4},{3,0},{4,7},{5,3},{6,5},{7,1},{8,14},{9,10},{10,... | collective-permute-start | bytes 3145736 | tf_op jit(solution)/shard_map/ppermute | solution.py:33
  25.5 67.2 %collective-permute-start.12 = (bf16[256,2048]{1,0:T(8,128)(2,1)}, bf16[256,2048]{1,0:T(8,128)(2,1)S(1)}, u32[]{:S(2)}, u32[]{:S(2)}) collective-permute-start(bf16[256,2048]{1,0:T(8,128)(2,1)} %bitcast.4.refs_0_), channel_id=1, source_target_pairs={{0,4},{1,0},{2,6},{3,2},{4,5},{5,1},{6,7},{7,3},{8,12},{9,8},{10,1... | collective-permute-start | bytes 3145736 | tf_op jit(solution)/shard_map/ppermute | solution.py:33
  49.3 43.9 %copy-start.7 = (bf16[2048,256]{1,0:T(8,128)(2,1)}, bf16[2048,256]{1,0:T(8,128)(2,1)S(1)}, u32[]{:S(2)}) copy-start(bf16[2048,256]{1,0:T(8,128)(2,1)S(1)} %collective-permute-done.10.refs_10_.refs_15_) | copy-start | bytes 3145732
  49.3 43.5 %collective-permute-start.14 = (bf16[256,2048]{1,0:T(8,128)(2,1)}, bf16[256,2048]{1,0:T(8,128)(2,1)S(1)}, u32[]{:S(2)}, u32[]{:S(2)}) collective-permute-start(bf16[256,2048]{1,0:T(8,128)(2,1)} %bitcast.4.refs_0_), channel_id=1, source_target_pairs={{0,6},{1,2},{2,4},{3,0},{4,7},{5,3},{6,5},{7,1},{8,14},{9,10},{10,... | collective-permute-start | bytes 3145736 | tf_op jit(solution)/shard_map/ppermute | solution.py:33
  50.7 42.5 %collective-permute-start.11 = (bf16[2048,256]{1,0:T(8,128)(2,1)S(1)}, bf16[2048,256]{1,0:T(8,128)(2,1)S(1)}, u32[]{:S(2)}, u32[]{:S(2)}) collective-permute-start(bf16[2048,256]{1,0:T(8,128)(2,1)S(1)} %collective-permute-done.10.refs_10_.refs_15_), channel_id=1, source_target_pairs={{0,4},{1,5},{2,6},{3,7},{4,0},{5,1},{6,2},{7,3},{8,12},{9,13},{10,... | collective-permute-start | bytes 3145736 | tf_op jit(solution)/shard_map/ppermute | solution.py:33
  72.0 24.9 %collective-permute-start.6 = (bf16[2048,256]{1,0:T(8,128)(2,1)}, bf16[2048,256]{1,0:T(8,128)(2,1)}, u32[]{:S(2)}, u32[]{:S(2)}) collective-permute-start(bf16[2048,256]{1,0:T(8,128)(2,1)} %collective-permute-done.4.refs_1_.refs_4_), channel_id=1, source_target_pairs={{0,4},{1,5},{2,6},{3,7},{4,0},{5,1},{6,2},{7,3},{8,12},{9,13},{10,... | collective-permute-start | bytes 3145736 | tf_op jit(solution)/shard_map/ppermute | solution.py:33
  72.0 27.4 %collective-permute-start.7 = (bf16[2048,256]{1,0:T(8,128)(2,1)}, bf16[2048,256]{1,0:T(8,128)(2,1)}, u32[]{:S(2)}, u32[]{:S(2)}) collective-permute-start(bf16[2048,256]{1,0:T(8,128)(2,1)} %collective-permute-done.5.refs_3_.refs_6_), channel_id=1, source_target_pairs={{0,4},{1,5},{2,6},{3,7},{4,0},{5,1},{6,2},{7,3},{8,12},{9,13},{10,... | collective-permute-start | bytes 3145736 | tf_op jit(solution)/shard_map/ppermute | solution.py:33
  92.7 6.7 %collective-permute-start.9 = (bf16[2048,256]{1,0:T(8,128)(2,1)}, bf16[2048,256]{1,0:T(8,128)(2,1)}, u32[]{:S(2)}, u32[]{:S(2)}) collective-permute-start(bf16[2048,256]{1,0:T(8,128)(2,1)} %collective-permute-done.8.refs_8_.refs_13_), channel_id=1, source_target_pairs={{0,4},{1,5},{2,6},{3,7},{4,0},{5,1},{6,2},{7,3},{8,12},{9,13},{10,... | collective-permute-start | bytes 3145736 | tf_op jit(solution)/shard_map/ppermute | solution.py:33
  92.8 14.6 %collective-permute-start.13 = (bf16[256,2048]{1,0:T(8,128)(2,1)S(1)}, bf16[256,2048]{1,0:T(8,128)(2,1)}, u32[]{:S(2)}, u32[]{:S(2)}) collective-permute-start(bf16[256,2048]{1,0:T(8,128)(2,1)S(1)} %collective-permute-done.12.refs_1_.refs_2_), channel_id=1, source_target_pairs={{0,4},{1,5},{2,6},{3,7},{4,0},{5,1},{6,2},{7,3},{8,12},{9,13},{10,... | collective-permute-start | bytes 3145736 | tf_op jit(solution)/shard_map/ppermute | solution.py:33
  94.2 13.2 %collective-permute-start.15 = (bf16[256,2048]{1,0:T(8,128)(2,1)S(1)}, bf16[256,2048]{1,0:T(8,128)(2,1)}, u32[]{:S(2)}, u32[]{:S(2)}) collective-permute-start(bf16[256,2048]{1,0:T(8,128)(2,1)S(1)} %collective-permute-done.14.refs_4_.refs_7_), channel_id=1, source_target_pairs={{0,4},{1,5},{2,6},{3,7},{4,0},{5,1},{6,2},{7,3},{8,12},{9,13},{10,... | collective-permute-start | bytes 3145736 | tf_op jit(solution)/shard_map/ppermute | solution.py:33
  96.9 35.1 %collective-permute-start = (bf16[15,256]{1,0:T(8,128)(2,1)S(1)}, bf16[15,256]{1,0:T(8,128)(2,1)S(1)}, u32[]{:S(2)}, u32[]{:S(2)}) collective-permute-start(bf16[15,256]{1,0:T(8,128)(2,1)S(1)} %slice.254), channel_id=1, source_target_pairs={{0,4},{4,8},{8,12},{12,16},{16,20},{20,24},{24,28},{28,32},{32,36}... | collective-permute-start | bytes 23048 | tf_op jit(solution)/shard_map/ppermute | solution.py:16
  113.6 13.1 %copy-start.11 = (bf16[2048,4]{0,1:T(4,128)(2,1)S(1)}, bf16[2048,4]{0,1:T(4,128)(2,1)}, u32[]{:S(2)}) copy-start(bf16[2048,4]{0,1:T(4,128)(2,1)} %param.22) | copy-start | bytes 49156
  113.6 51.0 %all-to-all-start.1 = ((bf16[64,3,2,2048]{3,2,1,0:T(2,128)(2,1)}), bf16[64,3,2,2048]{3,2,1,0:T(2,128)(2,1)S(1)}, u32[]{:S(2)}, u32[]{:S(2)}) async-start(bf16[64,3,2,2048]{3,2,1,0:T(2,128)(2,1)} %copy-done.1), calls=%async_computation.1 | async-start | bytes 3145728 | tf_op jit(solution)/shard_map/all_to_all | solution.py:319
  136.1 28.5 %copy-start.6 = (bf16[2,192,384]{2,1,0:T(8,128)(2,1)S(1)}, bf16[2,192,384]{2,1,0:T(8,128)(2,1)}, u32[]{:S(2)}) copy-start(bf16[2,192,384]{2,1,0:T(8,128)(2,1)} %copy-done.5) | copy-start | bytes 884740
  138.6 28.4 %collective-permute-start.1 = (bf16[128,2048]{1,0:T(8,128)(2,1)}, bf16[128,2048]{1,0:T(8,128)(2,1)}, u32[]{:S(2)}, u32[]{:S(2)}) collective-permute-start(bf16[128,2048]{1,0:T(8,128)(2,1)} %get-tuple-element.14), channel_id=1, source_target_pairs={{0,1},{1,0},{2,3},{3,2},{4,5},{5,4},{6,7},{7,6},{8,9},{9,8},{10,11... | collective-permute-start | bytes 1572872 | tf_op jit(solution)/shard_map/ppermute | solution.py:21
  140.0 27.1 %collective-permute-start.2 = (bf16[128,2048]{1,0:T(8,128)(2,1)}, bf16[128,2048]{1,0:T(8,128)(2,1)}, u32[]{:S(2)}, u32[]{:S(2)}) collective-permute-start(bf16[128,2048]{1,0:T(8,128)(2,1)} %get-tuple-element.16), channel_id=1, source_target_pairs={{0,2},{1,3},{2,0},{3,1},{4,6},{5,7},{6,4},{7,5},{8,10},{9,11},{10,... | collective-permute-start | bytes 1572872 | tf_op jit(solution)/shard_map/ppermute | solution.py:21
  141.3 25.9 %collective-permute-start.3 = (bf16[128,2048]{1,0:T(8,128)(2,1)S(1)}, bf16[128,2048]{1,0:T(8,128)(2,1)}, u32[]{:S(2)}, u32[]{:S(2)}) collective-permute-start(bf16[128,2048]{1,0:T(8,128)(2,1)S(1)} %get-tuple-element.15), channel_id=1, source_target_pairs={{0,3},{1,2},{2,1},{3,0},{4,7},{5,6},{6,5},{7,4},{8,11},{9,10},{10,... | collective-permute-start | bytes 1572872 | tf_op jit(solution)/shard_map/ppermute | solution.py:21
  165.6 7.9 %collective-permute-start.16 = (bf16[96,2048]{1,0:T(8,128)(2,1)S(1)}, bf16[96,2048]{1,0:T(8,128)(2,1)S(1)}, u32[]{:S(2)}, u32[]{:S(2)}) collective-permute-start(bf16[96,2048]{1,0:T(8,128)(2,1)S(1)} %get-tuple-element.11), channel_id=1, source_target_pairs={{0,1},{1,0},{2,3},{3,2},{4,7},{5,6},{6,5},{7,4},{8,9},{9,8},{10,11... | collective-permute-start | bytes 1179656 | tf_op jit(solution)/shard_map/ppermute | solution.py:378
  (9 other events, 28.6 us)

commit v5 on v4

--- a/solution.py
+++ b/solution.py
@@ -257,62 +257,66 @@
 DOWN_COLUMNS = 512
 
 
-def down_kernel(flag_ref, hidden_ref, *refs):
-    out_ref, scratch, sems = refs[-3:]
-    parts, units, model = scratch.shape
-    steps = model // DOWN_COLUMNS
-    waits = []
-    for n in range(steps):
-        columns = pl.ds(n * DOWN_COLUMNS, DOWN_COLUMNS)
-        waits.append(
-            [
-                fetch(
-                    flag_ref,
-                    (refs[2 * q].at[:, columns], refs[2 * q + 1].at[:, columns]),
-                    scratch.at[q, :, columns],
-                    sems.at[n, q],
-                )
-                for q in range(parts)
-            ]
-        )
-    for n in range(steps):
-        columns = slice(n * DOWN_COLUMNS, (n + 1) * DOWN_COLUMNS)
-        total = None
-        for q in range(parts):
-            waits[n][q].wait()
-            piece = jnp.dot(
-                hidden_ref[:, q * units : (q + 1) * units],
-                scratch[q, :, columns],
-                preferred_element_type=jnp.float32,
-            )
-            total = piece if total is None else total + piece
+def slot_columns(hidden_ref, flag_ref, on_holder, on_other, units):
+    slot = jnp.where(flag_ref[0] == 1, on_holder, on_other)
+    return hidden_ref[:, pl.ds(pl.multiple_of(slot * units, units), units)]
+
+
+def down_near_kernel(flag_ref, hidden_ref, first_ref, second_ref, out_ref):
+    units, model = first_ref.shape
+    first = slot_columns(hidden_ref, flag_ref, 1, 0, units)
+    second = slot_columns(hidden_ref, flag_ref, 2, 3, units)
+    for start in range(0, model, DOWN_COLUMNS):
+        columns = slice(start, start + DOWN_COLUMNS)
+        out_ref[:, columns] = jnp.dot(
+            first, first_ref[:, columns], preferred_element_type=jnp.float32
+        ) + jnp.dot(second, second_ref[:, columns], preferred_element_type=jnp.float32)
+
+
+def down_last_kernel(
+    flag_ref, hidden_ref, near_ref, second_ref, own_ref, first_ref, out_ref, scratch, sem
+):
+    units, model = second_ref.shape
+    wait = fetch(flag_ref, (own_ref, first_ref), scratch, sem)
+    one = slot_columns(hidden_ref, flag_ref, 0, 1, units)
+    two = slot_columns(hidden_ref, flag_ref, 3, 2, units)
+    wait.wait()
+    for start in range(0, model, DOWN_COLUMNS):
+        columns = slice(start, start + DOWN_COLUMNS)
+        total = jnp.dot(one, scratch[:, columns], preferred_element_type=jnp.float32)
+        total = total + jnp.dot(two, second_ref[:, columns], preferred_element_type=jnp.float32)
+        total = total + near_ref[:, columns]
         out_ref[:, :, :, columns] = total.astype(jnp.bfloat16).reshape(
             out_ref.shape[:3] + (DOWN_COLUMNS,)
         )
 
 
 def down_of(flag, hidden, downs, out_shape):
-    units, model = downs[0][0].shape
-    parts = len(downs)
-    arrays = [array for pair in downs for array in pair]
+    (own, first), (_, first_over), (second, second_over) = downs[:3]
+    units, model = own.shape
+    flag_spec = pl.BlockSpec(memory_space=pltpu.SMEM)
+    spec = pl.BlockSpec(memory_space=pltpu.VMEM)
+    cost = pl.CostEstimate(
+        flops=hidden.size * model, bytes_accessed=4 << 20, transcendentals=0
+    )
+    near = pl.pallas_call(
+        down_near_kernel,
+        out_shape=jax.ShapeDtypeStruct((hidden.shape[0], model), jnp.float32),
+        in_specs=[flag_spec, spec, spec, spec],
+        compiler_params=pltpu.CompilerParams(vmem_limit_bytes=16 << 20),
+        cost_estimate=cost,
+        name="down",
+    )(flag, hidden, first, second)
     return pl.pallas_call(
-        down_kernel,
+        down_last_kernel,
         out_shape=out_shape,
-        in_specs=[
-            pl.BlockSpec(memory_space=pltpu.SMEM),
-            pl.BlockSpec(memory_space=pltpu.VMEM),
-        ]
-        + [pl.BlockSpec(memory_space=pltpu.HBM)] * len(arrays),
-        scratch_shapes=[
-            pltpu.VMEM((parts, units, model), jnp.bfloat16),
-            pltpu.SemaphoreType.DMA((model // DOWN_COLUMNS, parts)),
-        ],
+        in_specs=[flag_spec, spec, spec, spec]
+        + [pl.BlockSpec(memory_space=pltpu.HBM)] * 2,
+        scratch_shapes=[pltpu.VMEM((units, model), jnp.bfloat16), pltpu.SemaphoreType.DMA],
         compiler_params=pltpu.CompilerParams(vmem_limit_bytes=16 << 20),
-        cost_estimate=pl.CostEstimate(
-            flops=2 * hidden.size * model, bytes_accessed=6 << 20, transcendentals=0
-        ),
+        cost_estimate=cost,
         name="down",
-    )(flag, hidden, *arrays)
+    )(flag, hidden, near, second_over, own, first_over)
 
 
 def exchange(rows):

time: 175 us -> 176 us (level)
    unnamed x28 -> x26, local copies, waits for them, and re-layouts: 5.53 us -> 3.93 us
    pallas_call x1 -> x2, Pallas kernels: 3.91 us -> 4.89 us  [the longest x1 2.51 us: down_of(): pl.pallas_call(down_near_kernel, out_shape=jax.ShapeDtypeStruct((hidden.s...]
  transfers between devices with their start and end apart: 19 -> 19, of which waited for: 7 -> 7; matrix products, arithmetic and copies ran while one was open for 12% -> 12% of each run, Pallas kernels for 7% -> 8%
where the time goes in v5:
time: 176 us; the launch traced here: 175 us
  waiting for transfers between devices  89.2 us (51%)
  starting transfers between devices  39.8 us (23%)
  Pallas kernels  16.2 us (9%)
  local copies, waits for them, and re-layouts  10.4 us (6%)
  matrix products  10.3 us (6%)
  other arithmetic  7.89 us (4%)
    ppermute x12, waiting for transfers between devices, sent(): return lax.ppermute(value, ('ep', 'tp'), pairs)  65.4 us
    all_to_all x2, starting transfers between devices, exchange(): return lax.all_to_all(rows, 'ep', split_axis=0, concat_axis=0, tiled=True)  24.3 us
    all_to_all x2, waiting for transfers between devices, exchange(): return lax.all_to_all(rows, 'ep', split_axis=0, concat_axis=0, tiled=True)  19.3 us
    pallas_call x1, Pallas kernels, hidden_of(): pl.pallas_call(hidden_kernel, out_shape=jax.ShapeDtypeStruct((count, part...  7.94 us
    ppermute x12, starting transfers between devices, sent(): return lax.ppermute(value, ('ep', 'tp'), pairs)  7.69 us
    ppermute x3, starting transfers between devices, swapped(): lax.ppermute(value, 'tp', [(source, source ^ mask) for source in range(co...  4.7 us
    unnamed x26, local copies, waits for them, and re-layouts  3.93 us
    dot_general x1, matrix products, mixer_partial(): jnp.dot(mixed_rows, pool_out, preferred_element_type=jnp.float32)  3.91 us
  transfers between devices with their start and end apart: 19, of which 7 were waited for; matrix products, arithmetic and copies ran while one was open for 12% of the time, Pallas kernels for 8%

profile of v5, /device:TPU:8, one launch (start us, length us, event | category | flops | bytes accessed | tf_op | source)
XLA Modules:
  0.0 174.9 jit_solution(2344661304886667432)
XLA Ops:
  4.2 2.3 %dispatch.1 = (bf16[192,2048]{1,0:T(8,128)(2,1)S(1)}, bf16[2,192,384]{2,1,0:T(8,128)(2,1)S(1)}, bf16[64,3,2,2048]{3,2,1,0:T(2,128)(2,1)}) custom-call(bf16[192,2048]{1,0:T(8,128)(2,1)S(1)} %pad_maximum_fusion.x_ref, bf16[1,2048]{1,0:T(2,128)(2,1)S(1)} %reshape.268.gain_ref, s32[192,2]{1,0:T(8,128)S(1)} %fusion.40.targets_ref), custom_call_target="tpu_custom_call" | custom-call | tf_op jit(solution)/shard_map/dispatch/pallas_call | solution.py:139
  6.5 12.3 %all-to-all-start = ((bf16[64,3,2,2048]{3,2,1,0:T(2,128)(2,1)}), bf16[64,3,2,2048]{3,2,1,0:T(2,128)(2,1)}, u32[]{:S(2)}, u32[]{:S(2)}) async-start(bf16[64,3,2,2048]{3,2,1,0:T(2,128)(2,1)} %get-tuple-element.7), calls=%async_computation | async-start | bytes 3145728 | tf_op jit(solution)/shard_map/all_to_all | solution.py:323
  18.8 2.8 %collective-permute-start.10 = (bf16[2048,256]{1,0:T(8,128)(2,1)}, bf16[2048,256]{1,0:T(8,128)(2,1)S(1)}, u32[]{:S(2)}, u32[]{:S(2)}) collective-permute-start(bf16[2048,256]{1,0:T(8,128)(2,1)} %bitcast.23), channel_id=1, source_target_pairs={{0,6},{1,2},{2,4},{3,0},{4,7},{5,3},{6,5},{7,1},{8,14},{9,10},{10,... | collective-permute-start | bytes 3145736 | tf_op jit(solution)/shard_map/ppermute | solution.py:33
  22.3 1.6 collective-permute-start.8
  24.0 23.8 %collective-permute-done.10.refs_10_.refs_15_ = bf16[2048,256]{1,0:T(8,128)(2,1)S(1)} collective-permute-done((bf16[2048,256]{1,0:T(8,128)(2,1)}, bf16[2048,256]{1,0:T(8,128)(2,1)S(1)}, u32[]{:S(2)}, u32[]{:S(2)}) %collective-permute-start.10) | collective-permute-done | bytes 1048608 | tf_op jit(solution)/shard_map/ppermute | solution.py:33
  47.7 1.4 collective-permute-start.13
  49.2 21.2 %collective-permute-done.5.refs_3_.refs_6_ = bf16[2048,256]{1,0:T(8,128)(2,1)} collective-permute-done((bf16[2048,256]{1,0:T(8,128)(2,1)}, bf16[2048,256]{1,0:T(8,128)(2,1)}, u32[]{:S(2)}, u32[]{:S(2)}) %collective-permute-start.5) | collective-permute-done | bytes 1048608 | tf_op jit(solution)/shard_map/ppermute | solution.py:33
  70.9 20.3 %collective-permute-done.12.first_ref = bf16[256,2048]{1,0:T(8,128)(2,1)} collective-permute-done((bf16[256,2048]{1,0:T(8,128)(2,1)S(1)}, bf16[256,2048]{1,0:T(8,128)(2,1)}, u32[]{:S(2)}, u32[]{:S(2)}) %collective-permute-start.12) | collective-permute-done | bytes 1048608 | tf_op jit(solution)/shard_map/ppermute | solution.py:33
  93.9 1.6 fusion.41
  95.5 2.5 %collective-permute-start = (bf16[15,256]{1,0:T(8,128)(2,1)S(1)}, bf16[15,256]{1,0:T(8,128)(2,1)S(1)}, u32[]{:S(2)}, u32[]{:S(2)}) collective-permute-start(bf16[15,256]{1,0:T(8,128)(2,1)S(1)} %slice.254), channel_id=1, source_target_pairs={{0,4},{4,8},{8,12},{12,16},{16,20},{20,24},{24,28},{28,32},{32,36}... | collective-permute-start | bytes 23048 | tf_op jit(solution)/shard_map/ppermute | solution.py:16
  98.0 7.9 %hidden.1.hidden_ref = bf16[384,1024]{1,0:T(8,128)(2,1)} custom-call(s32[1]{0:T(128)} %bitcast.1.flag_ref, bf16[64,3,2,2048]{3,2,1,0:T(2,128)(2,1)} %all-to-all-done.rows_ref, bf16[2048,256]{1,0:T(8,128)(2,1)} %bitcast.22, bf16[2048,256]{1,0:T(8,128)(2,1)} %collective-permute-done.4.refs_1_.refs_4_, bf16[2048,256]{1,0:T(8,128)(2,1)} %bitcast.25, ...), custom_call_target="tpu_custom_call" | custom-call | flops 3221225472 | bytes 9437184 | tf_op jit(solution)/shard_map/hidden/pallas_call | solution.py:236
  107.0 2.5 %down.2.near_ref = f32[384,2048]{1,0:T(8,128)S(1)} custom-call(s32[1]{0:T(128)} %bitcast.1.flag_ref, bf16[384,1024]{1,0:T(8,128)(2,1)S(1)} %copy-done.1, bf16[256,2048]{1,0:T(8,128)(2,1)} %collective-permute-done.12.first_ref, bf16[256,2048]{1,0:T(8,128)(2,1)} %collective-permute-done.13.second_ref), custom_call_target="tpu_custom_call" | custom-call | flops 805306368 | bytes 4194304 | tf_op jit(solution)/shard_map/down/pallas_call | solution.py:302
  109.6 2.4 %down.3 = bf16[64,3,2,2048]{3,2,1,0:T(2,128)(2,1)S(1)} custom-call(s32[1]{0:T(128)} %bitcast.1.flag_ref, bf16[384,1024]{1,0:T(8,128)(2,1)S(1)} %copy-done.1, f32[384,2048]{1,0:T(8,128)S(1)} %down.2.near_ref, bf16[256,2048]{1,0:T(8,128)(2,1)} %collective-permute-done.14.second_ref, bf16[256,2048]{1,0:T(8,128)(2,1)S(1)} %bitcast.19, ...), custom_call_target="tpu_custom_call" | custom-call | flops 805306368 | bytes 4194304 | tf_op jit(solution)/shard_map/down/pallas_call | solution.py:310
  113.1 12.1 %all-to-all-start.1 = ((bf16[64,3,2,2048]{3,2,1,0:T(2,128)(2,1)}), bf16[64,3,2,2048]{3,2,1,0:T(2,128)(2,1)S(1)}, u32[]{:S(2)}, u32[]{:S(2)}) async-start(bf16[64,3,2,2048]{3,2,1,0:T(2,128)(2,1)} %copy-done.2), calls=%async_computation.1 | async-start | bytes 3145728 | tf_op jit(solution)/shard_map/all_to_all | solution.py:323
  125.2 2.1 %fusion = f32[512]{0:T(512)S(1)} fusion(bf16[512,2048]{1,0:T(8,128)(2,1)} %param.14), kind=kLoop, calls=%fused_computation.2 | loop fusion | flops 3145216 | bytes 2099200 | tf_op jit(solution)/shard_map/reduce_sum | solution.py:46
  127.6 1.3 convolution_exponential_fusion
  129.9 2.6 %fusion.7 = bf16[512,256]{1,0:T(8,128)(2,1)S(1)} fusion(bf16[2048,256]{1,0:T(8,128)(2,1)} %param.16, bf16[512,2048]{1,0:T(8,128)(2,1)} %param.14, f32[2048]{0:T(1024)S(1)} %convert_element_type.136, f32[512]{0:T(512)S(1)} %add_rsqrt_fusion), kind=kOutput, calls=%fused_computation.10 | convolution fusion | flops 541196288 | bytes 3418112 | tf_op jit(solution)/shard_map/dot_general | solution.py:52
  132.7 3.9 %convolution_convert_fusion = bf16[512,2048]{1,0:T(8,128)(2,1)} fusion(bf16[256,2048]{1,0:T(8,128)(2,1)S(1)} %copy-done, f32[256]{0:T(256)S(1)} %convert_element_type.161, f32[527,256]{1,0:T(8,128)S(1)} %maximum_convert_fusion, f32[512]{0:T(512)S(1)} %minimum_convert_fusion, f32[]{:T(128)S(6)} %convert_element_type.158, f32[]{:T(128)S(6)} %convert_element_type.157, ...), kind=kOutput, calls=%fused_computation.5 | convolution fusion | flops 609746944 | bytes 11668544 | tf_op jit(solution)/shard_map/dot_general | solution.py:76
  136.6 2.5 %constant_dynamic-slice_fusion.6 = (bf16[128,2048]{1,0:T(8,128)(2,1)}, bf16[128,2048]{1,0:T(8,128)(2,1)S(1)}, bf16[128,2048]{1,0:T(8,128)(2,1)}) fusion(bf16[512,2048]{1,0:T(8,128)(2,1)} %convolution_convert_fusion, s32[]{:T(128)S(6)} %select_n.68, s32[]{:T(128)S(6)} %select_n.70, s32[]{:T(128)S(6)} %select_n.69), kind=kLoop, calls=%fused_computation.88 | loop fusion | bytes 3145740 | tf_op jit(solution)/shard_map/dynamic_slice | solution.py:85
  139.7 1.8 %collective-permute-start.2 = (bf16[128,2048]{1,0:T(8,128)(2,1)}, bf16[128,2048]{1,0:T(8,128)(2,1)}, u32[]{:S(2)}, u32[]{:S(2)}) collective-permute-start(bf16[128,2048]{1,0:T(8,128)(2,1)} %get-tuple-element.16), channel_id=1, source_target_pairs={{0,2},{1,3},{2,0},{3,1},{4,6},{5,7},{6,4},{7,5},{8,10},{9,11},{10,... | collective-permute-start | bytes 1572872 | tf_op jit(solution)/shard_map/ppermute | solution.py:21
  141.5 2.4 %collective-permute-start.3 = (bf16[128,2048]{1,0:T(8,128)(2,1)S(1)}, bf16[128,2048]{1,0:T(8,128)(2,1)}, u32[]{:S(2)}, u32[]{:S(2)}) collective-permute-start(bf16[128,2048]{1,0:T(8,128)(2,1)S(1)} %get-tuple-element.15), channel_id=1, source_target_pairs={{0,3},{1,2},{2,1},{3,0},{4,7},{5,6},{6,5},{7,4},{8,11},{9,10},{10,... | collective-permute-start | bytes 1572872 | tf_op jit(solution)/shard_map/ppermute | solution.py:21
  145.9 19.3 %all-to-all-done.1.returned_ref = bf16[64,3,2,2048]{3,2,1,0:T(2,128)(2,1)S(1)} async-done(((bf16[64,3,2,2048]{3,2,1,0:T(2,128)(2,1)}), bf16[64,3,2,2048]{3,2,1,0:T(2,128)(2,1)S(1)}, u32[]{:S(2)}, u32[]{:S(2)}) %all-to-all-start.1) | async-done | bytes 1572896 | tf_op jit(solution)/shard_map/all_to_all | solution.py:323
  167.7 2.6 %add_convert_fusion = bf16[128,2048]{1,0:T(8,128)(2,1)} fusion(bf16[128,2048]{1,0:T(8,128)(2,1)} %collective-permute-done.3, bf16[128,2048]{1,0:T(8,128)(2,1)} %collective-permute-done.2, bf16[128,2048]{1,0:T(8,128)(2,1)} %collective-permute-done.1, bf16[512,2048]{1,0:T(8,128)(2,1)} %convolution_convert_fusion, s32[]{:T(128)S(6)} %select_n.67), kind=kLoop, calls=%fused_computation.17 | loop fusion | flops 2097152 | bytes 2621444 | tf_op jit(solution)/shard_map/convert_element_type | solution.py:91
  170.4 3.7 %collective-permute-done.16 = bf16[96,2048]{1,0:T(8,128)(2,1)S(1)} collective-permute-done((bf16[96,2048]{1,0:T(8,128)(2,1)S(1)}, bf16[96,2048]{1,0:T(8,128)(2,1)S(1)}, u32[]{:S(2)}, u32[]{:S(2)}) %collective-permute-start.16) | collective-permute-done | bytes 393248 | tf_op jit(solution)/shard_map/ppermute | solution.py:382
  (79 shorter events, 16.9 us)
Async XLA Ops:
  0.6 132.1 %copy-start = (bf16[256,2048]{1,0:T(8,128)(2,1)S(1)}, bf16[256,2048]{1,0:T(8,128)(2,1)}, u32[]{:S(2)}) copy-start(bf16[256,2048]{1,0:T(8,128)(2,1)} %param.19) | copy-start | bytes 3145732
  4.2 88.7 %copy-start.11 = (bf16[2048]{0:T(1024)(128)(2,1)S(1)}, bf16[2048]{0:T(1024)(128)(2,1)}, u32[]{:S(2)}) copy-start(bf16[2048]{0:T(1024)(128)(2,1)} %param.15) | copy-start | bytes 12292
  6.5 88.9 %copy-start.4 = (bf16[2,192,384]{2,1,0:T(8,128)(2,1)}, bf16[2,192,384]{2,1,0:T(8,128)(2,1)S(1)}, u32[]{:S(2)}) copy-start(bf16[2,192,384]{2,1,0:T(8,128)(2,1)S(1)} %get-tuple-element.8.pick_ref) | copy-start | bytes 884740
  6.5 91.4 %all-to-all-start = ((bf16[64,3,2,2048]{3,2,1,0:T(2,128)(2,1)}), bf16[64,3,2,2048]{3,2,1,0:T(2,128)(2,1)}, u32[]{:S(2)}, u32[]{:S(2)}) async-start(bf16[64,3,2,2048]{3,2,1,0:T(2,128)(2,1)} %get-tuple-element.7), calls=%async_computation | async-start | bytes 3145728 | tf_op jit(solution)/shard_map/all_to_all | solution.py:323
  18.8 29.0 %collective-permute-start.10 = (bf16[2048,256]{1,0:T(8,128)(2,1)}, bf16[2048,256]{1,0:T(8,128)(2,1)S(1)}, u32[]{:S(2)}, u32[]{:S(2)}) collective-permute-start(bf16[2048,256]{1,0:T(8,128)(2,1)} %bitcast.23), channel_id=1, source_target_pairs={{0,6},{1,2},{2,4},{3,0},{4,7},{5,3},{6,5},{7,1},{8,14},{9,10},{10,... | collective-permute-start | bytes 3145736 | tf_op jit(solution)/shard_map/ppermute | solution.py:33
  21.6 27.6 %collective-permute-start.4 = (bf16[2048,256]{1,0:T(8,128)(2,1)}, bf16[2048,256]{1,0:T(8,128)(2,1)}, u32[]{:S(2)}, u32[]{:S(2)}) collective-permute-start(bf16[2048,256]{1,0:T(8,128)(2,1)} %bitcast.20), channel_id=1, source_target_pairs={{0,4},{1,0},{2,6},{3,2},{4,5},{5,1},{6,7},{7,3},{8,12},{9,8},{10,1... | collective-permute-start | bytes 3145736 | tf_op jit(solution)/shard_map/ppermute | solution.py:33
  21.6 48.8 %collective-permute-start.5 = (bf16[2048,256]{1,0:T(8,128)(2,1)}, bf16[2048,256]{1,0:T(8,128)(2,1)}, u32[]{:S(2)}, u32[]{:S(2)}) collective-permute-start(bf16[2048,256]{1,0:T(8,128)(2,1)} %bitcast.24), channel_id=1, source_target_pairs={{0,4},{1,0},{2,6},{3,2},{4,5},{5,1},{6,7},{7,3},{8,12},{9,8},{10,1... | collective-permute-start | bytes 3145736 | tf_op jit(solution)/shard_map/ppermute | solution.py:33
  22.3 48.1 %collective-permute-start.8 = (bf16[2048,256]{1,0:T(8,128)(2,1)}, bf16[2048,256]{1,0:T(8,128)(2,1)}, u32[]{:S(2)}, u32[]{:S(2)}) collective-permute-start(bf16[2048,256]{1,0:T(8,128)(2,1)} %bitcast.21), channel_id=1, source_target_pairs={{0,6},{1,2},{2,4},{3,0},{4,7},{5,3},{6,5},{7,1},{8,14},{9,10},{10,... | collective-permute-start | bytes 3145736 | tf_op jit(solution)/shard_map/ppermute | solution.py:33
  24.0 67.3 %collective-permute-start.12 = (bf16[256,2048]{1,0:T(8,128)(2,1)S(1)}, bf16[256,2048]{1,0:T(8,128)(2,1)}, u32[]{:S(2)}, u32[]{:S(2)}) collective-permute-start(bf16[256,2048]{1,0:T(8,128)(2,1)S(1)} %bitcast.17), channel_id=1, source_target_pairs={{0,4},{1,0},{2,6},{3,2},{4,5},{5,1},{6,7},{7,3},{8,12},{9,8},{10,1... | collective-permute-start | bytes 3145736 | tf_op jit(solution)/shard_map/ppermute | solution.py:33
  47.7 43.6 %copy-start.6 = (bf16[2048,256]{1,0:T(8,128)(2,1)}, bf16[2048,256]{1,0:T(8,128)(2,1)S(1)}, u32[]{:S(2)}) copy-start(bf16[2048,256]{1,0:T(8,128)(2,1)S(1)} %collective-permute-done.10.refs_10_.refs_15_) | copy-start | bytes 3145732
  47.7 43.6 %collective-permute-start.13 = (bf16[256,2048]{1,0:T(8,128)(2,1)S(1)}, bf16[256,2048]{1,0:T(8,128)(2,1)}, u32[]{:S(2)}, u32[]{:S(2)}) collective-permute-start(bf16[256,2048]{1,0:T(8,128)(2,1)S(1)} %bitcast.18), channel_id=1, source_target_pairs={{0,6},{1,2},{2,4},{3,0},{4,7},{5,3},{6,5},{7,1},{8,14},{9,10},{10,... | collective-permute-start | bytes 3145736 | tf_op jit(solution)/shard_map/ppermute | solution.py:33
  49.2 42.6 %collective-permute-start.11 = (bf16[2048,256]{1,0:T(8,128)(2,1)S(1)}, bf16[2048,256]{1,0:T(8,128)(2,1)S(1)}, u32[]{:S(2)}, u32[]{:S(2)}) collective-permute-start(bf16[2048,256]{1,0:T(8,128)(2,1)S(1)} %collective-permute-done.10.refs_10_.refs_15_), channel_id=1, source_target_pairs={{0,4},{1,5},{2,6},{3,7},{4,0},{5,1},{6,2},{7,3},{8,12},{9,13},{10,... | collective-permute-start | bytes 3145736 | tf_op jit(solution)/shard_map/ppermute | solution.py:33
  70.4 25.0 %collective-permute-start.6 = (bf16[2048,256]{1,0:T(8,128)(2,1)}, bf16[2048,256]{1,0:T(8,128)(2,1)}, u32[]{:S(2)}, u32[]{:S(2)}) collective-permute-start(bf16[2048,256]{1,0:T(8,128)(2,1)} %collective-permute-done.4.refs_1_.refs_4_), channel_id=1, source_target_pairs={{0,4},{1,5},{2,6},{3,7},{4,0},{5,1},{6,2},{7,3},{8,12},{9,13},{10,... | collective-permute-start | bytes 3145736 | tf_op jit(solution)/shard_map/ppermute | solution.py:33
  70.4 27.5 %collective-permute-start.7 = (bf16[2048,256]{1,0:T(8,128)(2,1)}, bf16[2048,256]{1,0:T(8,128)(2,1)}, u32[]{:S(2)}, u32[]{:S(2)}) collective-permute-start(bf16[2048,256]{1,0:T(8,128)(2,1)} %collective-permute-done.5.refs_3_.refs_6_), channel_id=1, source_target_pairs={{0,4},{1,5},{2,6},{3,7},{4,0},{5,1},{6,2},{7,3},{8,12},{9,13},{10,... | collective-permute-start | bytes 3145736 | tf_op jit(solution)/shard_map/ppermute | solution.py:33
  91.2 6.7 %collective-permute-start.9 = (bf16[2048,256]{1,0:T(8,128)(2,1)}, bf16[2048,256]{1,0:T(8,128)(2,1)}, u32[]{:S(2)}, u32[]{:S(2)}) collective-permute-start(bf16[2048,256]{1,0:T(8,128)(2,1)} %collective-permute-done.8.refs_8_.refs_13_), channel_id=1, source_target_pairs={{0,4},{1,5},{2,6},{3,7},{4,0},{5,1},{6,2},{7,3},{8,12},{9,13},{10,... | collective-permute-start | bytes 3145736 | tf_op jit(solution)/shard_map/ppermute | solution.py:33
  91.4 18.2 %collective-permute-start.14 = (bf16[256,2048]{1,0:T(8,128)(2,1)}, bf16[256,2048]{1,0:T(8,128)(2,1)}, u32[]{:S(2)}, u32[]{:S(2)}) collective-permute-start(bf16[256,2048]{1,0:T(8,128)(2,1)} %collective-permute-done.13.second_ref), channel_id=1, source_target_pairs={{0,4},{1,5},{2,6},{3,7},{4,0},{5,1},{6,2},{7,3},{8,12},{9,13},{10,... | collective-permute-start | bytes 3145736 | tf_op jit(solution)/shard_map/ppermute | solution.py:33
  92.8 16.8 %collective-permute-start.15 = (bf16[256,2048]{1,0:T(8,128)(2,1)}, bf16[256,2048]{1,0:T(8,128)(2,1)}, u32[]{:S(2)}, u32[]{:S(2)}) collective-permute-start(bf16[256,2048]{1,0:T(8,128)(2,1)} %collective-permute-done.12.first_ref), channel_id=1, source_target_pairs={{0,4},{1,5},{2,6},{3,7},{4,0},{5,1},{6,2},{7,3},{8,12},{9,13},{10,... | collective-permute-start | bytes 3145736 | tf_op jit(solution)/shard_map/ppermute | solution.py:33
  95.5 37.2 %collective-permute-start = (bf16[15,256]{1,0:T(8,128)(2,1)S(1)}, bf16[15,256]{1,0:T(8,128)(2,1)S(1)}, u32[]{:S(2)}, u32[]{:S(2)}) collective-permute-start(bf16[15,256]{1,0:T(8,128)(2,1)S(1)} %slice.254), channel_id=1, source_target_pairs={{0,4},{4,8},{8,12},{12,16},{16,20},{20,24},{24,28},{28,32},{32,36}... | collective-permute-start | bytes 23048 | tf_op jit(solution)/shard_map/ppermute | solution.py:16
  113.1 52.1 %all-to-all-start.1 = ((bf16[64,3,2,2048]{3,2,1,0:T(2,128)(2,1)}), bf16[64,3,2,2048]{3,2,1,0:T(2,128)(2,1)S(1)}, u32[]{:S(2)}, u32[]{:S(2)}) async-start(bf16[64,3,2,2048]{3,2,1,0:T(2,128)(2,1)} %copy-done.2), calls=%async_computation.1 | async-start | bytes 3145728 | tf_op jit(solution)/shard_map/all_to_all | solution.py:323
  136.6 28.5 %copy-start.5 = (bf16[2,192,384]{2,1,0:T(8,128)(2,1)S(1)}, bf16[2,192,384]{2,1,0:T(8,128)(2,1)}, u32[]{:S(2)}) copy-start(bf16[2,192,384]{2,1,0:T(8,128)(2,1)} %copy-done.4) | copy-start | bytes 884740
  139.2 27.7 %collective-permute-start.1 = (bf16[128,2048]{1,0:T(8,128)(2,1)}, bf16[128,2048]{1,0:T(8,128)(2,1)}, u32[]{:S(2)}, u32[]{:S(2)}) collective-permute-start(bf16[128,2048]{1,0:T(8,128)(2,1)} %get-tuple-element.14), channel_id=1, source_target_pairs={{0,1},{1,0},{2,3},{3,2},{4,5},{5,4},{6,7},{7,6},{8,9},{9,8},{10,11... | collective-permute-start | bytes 1572872 | tf_op jit(solution)/shard_map/ppermute | solution.py:21
  139.7 27.1 %collective-permute-start.2 = (bf16[128,2048]{1,0:T(8,128)(2,1)}, bf16[128,2048]{1,0:T(8,128)(2,1)}, u32[]{:S(2)}, u32[]{:S(2)}) collective-permute-start(bf16[128,2048]{1,0:T(8,128)(2,1)} %get-tuple-element.16), channel_id=1, source_target_pairs={{0,2},{1,3},{2,0},{3,1},{4,6},{5,7},{6,4},{7,5},{8,10},{9,11},{10,... | collective-permute-start | bytes 1572872 | tf_op jit(solution)/shard_map/ppermute | solution.py:21
  141.5 26.2 %collective-permute-start.3 = (bf16[128,2048]{1,0:T(8,128)(2,1)S(1)}, bf16[128,2048]{1,0:T(8,128)(2,1)}, u32[]{:S(2)}, u32[]{:S(2)}) collective-permute-start(bf16[128,2048]{1,0:T(8,128)(2,1)S(1)} %get-tuple-element.15), channel_id=1, source_target_pairs={{0,3},{1,2},{2,1},{3,0},{4,7},{5,6},{6,5},{7,4},{8,11},{9,10},{10,... | collective-permute-start | bytes 1572872 | tf_op jit(solution)/shard_map/ppermute | solution.py:21
  166.2 7.9 %collective-permute-start.16 = (bf16[96,2048]{1,0:T(8,128)(2,1)S(1)}, bf16[96,2048]{1,0:T(8,128)(2,1)S(1)}, u32[]{:S(2)}, u32[]{:S(2)}) collective-permute-start(bf16[96,2048]{1,0:T(8,128)(2,1)S(1)} %get-tuple-element.11), channel_id=1, source_target_pairs={{0,1},{1,0},{2,3},{3,2},{4,7},{5,6},{6,5},{7,4},{8,9},{9,8},{10,11... | collective-permute-start | bytes 1179656 | tf_op jit(solution)/shard_map/ppermute | solution.py:382
  (8 other events, 47.9 us)

commit v6 on v5

--- a/solution.py
+++ b/solution.py
@@ -1,3 +1,5 @@
+import functools
+
 import jax
 import jax.numpy as jnp
 from jax import lax
@@ -169,24 +171,21 @@
     return picked / jnp.sum(picked, axis=1, keepdims=True)
 
 
-def combine_kernel(returned_ref, pick_ref, weight_ref, own_ref, other_ref):
+def combine_kernel(first_row, returned_ref, pick_ref, weight_ref, out_ref):
     returned = returned_ref[...].reshape(pick_ref.shape[2], returned_ref.shape[-1])
-    weight = weight_ref[...]
-    total = jnp.dot(pick_ref[0], returned, preferred_element_type=jnp.float32) * weight[:, 0:1]
-    total = total + jnp.dot(pick_ref[1], returned, preferred_element_type=jnp.float32) * weight[:, 1:2]
-    rows = own_ref.shape[0]
-    own_ref[...] = total[:rows]
-    other_ref[...] = total[rows:].astype(jnp.bfloat16)
-
-
-def combine(returned, pick, weight):
-    shape = (pick.shape[1] // 2, returned.shape[-1])
+    rows = slice(first_row, first_row + out_ref.shape[0])
+    weight = weight_ref[rows, :]
+    total = jnp.dot(pick_ref[0, rows, :], returned, preferred_element_type=jnp.float32)
+    total = total * weight[:, 0:1]
+    second = jnp.dot(pick_ref[1, rows, :], returned, preferred_element_type=jnp.float32)
+    out_ref[...] = (total + second * weight[:, 1:2]).astype(out_ref.dtype)
+
+
+def combine(returned, pick, weight, block, dtype):
+    rows = pick.shape[1] // 2
     return pl.pallas_call(
-        combine_kernel,
-        out_shape=[
-            jax.ShapeDtypeStruct(shape, jnp.float32),
-            jax.ShapeDtypeStruct(shape, jnp.bfloat16),
-        ],
+        functools.partial(combine_kernel, block * rows),
+        out_shape=jax.ShapeDtypeStruct((rows, returned.shape[-1]), dtype),
         compiler_params=pltpu.CompilerParams(vmem_limit_bytes=12 << 20),
         name="combine",
     )(returned, pick, weight)
@@ -373,7 +372,8 @@
         flag, hidden, downs, jax.ShapeDtypeStruct(payload.shape, jnp.bfloat16)
     )
     returned = exchange(result)
-    own, other = combine(returned, pick, weight)
+    other = combine(returned, pick, weight, 1, jnp.bfloat16)
+    own = combine(returned, pick, weight, 0, jnp.float32)
     pairs = [
         (device * tp_count + place, device * tp_count + (place ^ (1 + 2 * (device % 2))))
         for device in range(lax.axis_size("ep"))

time: 176 us -> 176 us (level)
  no operation moved by 1% of the time
where the time goes in v6:
time: 176 us; the launch traced here: 175 us
  waiting for transfers between devices  88.5 us (50%)
  starting transfers between devices  39.8 us (23%)
  Pallas kernels  16.6 us (9%)
  local copies, waits for them, and re-layouts  11.2 us (6%)
  matrix products  10.2 us (6%)
  other arithmetic  7.89 us (4%)
    ppermute x12, waiting for transfers between devices, sent(): return lax.ppermute(value, ('ep', 'tp'), pairs)  65.4 us
    all_to_all x2, starting transfers between devices, exchange(): return lax.all_to_all(rows, 'ep', split_axis=0, concat_axis=0, tiled=True)  24.3 us
    all_to_all x2, waiting for transfers between devices, exchange(): return lax.all_to_all(rows, 'ep', split_axis=0, concat_axis=0, tiled=True)  19.3 us
    pallas_call x1, Pallas kernels, hidden_of(): pl.pallas_call(hidden_kernel, out_shape=jax.ShapeDtypeStruct((count, part...  7.94 us
    ppermute x12, starting transfers between devices, sent(): return lax.ppermute(value, ('ep', 'tp'), pairs)  7.69 us
    ppermute x3, starting transfers between devices, swapped(): lax.ppermute(value, 'tp', [(source, source ^ mask) for source in range(co...  4.7 us
    unnamed x26, local copies, waits for them, and re-layouts  4.66 us
    dot_general x1, matrix products, mixer_partial(): jnp.dot(mixed_rows, pool_out, preferred_element_type=jnp.float32)  3.91 us
  transfers between devices with their start and end apart: 19, of which 7 were waited for; matrix products, arithmetic and copies ran while one was open for 12% of the time, Pallas kernels for 8%

profile of v6, /device:TPU:8, one launch (start us, length us, event | category | flops | bytes accessed | tf_op | source)
XLA Modules:
  0.0 175.3 jit_solution(7957887029164240926)
XLA Ops:
  4.2 2.3 %dispatch.1 = (bf16[192,2048]{1,0:T(8,128)(2,1)S(1)}, bf16[2,192,384]{2,1,0:T(8,128)(2,1)S(1)}, bf16[64,3,2,2048]{3,2,1,0:T(2,128)(2,1)}) custom-call(bf16[192,2048]{1,0:T(8,128)(2,1)S(1)} %pad_maximum_fusion.x_ref, bf16[1,2048]{1,0:T(2,128)(2,1)S(1)} %reshape.268.gain_ref, s32[192,2]{1,0:T(8,128)S(1)} %fusion.40.targets_ref), custom_call_target="tpu_custom_call" | custom-call | tf_op jit(solution)/shard_map/dispatch/pallas_call | solution.py:141
  7.2 12.3 %all-to-all-start = ((bf16[64,3,2,2048]{3,2,1,0:T(2,128)(2,1)}), bf16[64,3,2,2048]{3,2,1,0:T(2,128)(2,1)}, u32[]{:S(2)}, u32[]{:S(2)}) async-start(bf16[64,3,2,2048]{3,2,1,0:T(2,128)(2,1)} %get-tuple-element.5), calls=%async_computation | async-start | bytes 3145728 | tf_op jit(solution)/shard_map/all_to_all | solution.py:322
  19.5 2.8 %collective-permute-start.10 = (bf16[2048,256]{1,0:T(8,128)(2,1)}, bf16[2048,256]{1,0:T(8,128)(2,1)S(1)}, u32[]{:S(2)}, u32[]{:S(2)}) collective-permute-start(bf16[2048,256]{1,0:T(8,128)(2,1)} %bitcast.23), channel_id=1, source_target_pairs={{0,6},{1,2},{2,4},{3,0},{4,7},{5,3},{6,5},{7,1},{8,14},{9,10},{10,... | collective-permute-start | bytes 3145736 | tf_op jit(solution)/shard_map/ppermute | solution.py:35
  23.0 1.6 collective-permute-start.8
  24.7 23.8 %collective-permute-done.10.refs_10_.refs_15_ = bf16[2048,256]{1,0:T(8,128)(2,1)S(1)} collective-permute-done((bf16[2048,256]{1,0:T(8,128)(2,1)}, bf16[2048,256]{1,0:T(8,128)(2,1)S(1)}, u32[]{:S(2)}, u32[]{:S(2)}) %collective-permute-start.10) | collective-permute-done | bytes 1048608 | tf_op jit(solution)/shard_map/ppermute | solution.py:35
  48.4 1.4 collective-permute-start.13
  49.9 21.2 %collective-permute-done.5.refs_3_.refs_6_ = bf16[2048,256]{1,0:T(8,128)(2,1)} collective-permute-done((bf16[2048,256]{1,0:T(8,128)(2,1)}, bf16[2048,256]{1,0:T(8,128)(2,1)}, u32[]{:S(2)}, u32[]{:S(2)}) %collective-permute-start.5) | collective-permute-done | bytes 1048608 | tf_op jit(solution)/shard_map/ppermute | solution.py:35
  71.6 20.3 %collective-permute-done.12.first_ref = bf16[256,2048]{1,0:T(8,128)(2,1)} collective-permute-done((bf16[256,2048]{1,0:T(8,128)(2,1)S(1)}, bf16[256,2048]{1,0:T(8,128)(2,1)}, u32[]{:S(2)}, u32[]{:S(2)}) %collective-permute-start.12) | collective-permute-done | bytes 1048608 | tf_op jit(solution)/shard_map/ppermute | solution.py:35
  94.6 1.6 fusion.41
  96.2 2.5 %collective-permute-start = (bf16[15,256]{1,0:T(8,128)(2,1)S(1)}, bf16[15,256]{1,0:T(8,128)(2,1)S(1)}, u32[]{:S(2)}, u32[]{:S(2)}) collective-permute-start(bf16[15,256]{1,0:T(8,128)(2,1)S(1)} %slice.254), channel_id=1, source_target_pairs={{0,4},{4,8},{8,12},{12,16},{16,20},{20,24},{24,28},{28,32},{32,36}... | collective-permute-start | bytes 23048 | tf_op jit(solution)/shard_map/ppermute | solution.py:18
  98.7 7.9 %hidden.1.hidden_ref = bf16[384,1024]{1,0:T(8,128)(2,1)} custom-call(s32[1]{0:T(128)} %bitcast.1.flag_ref, bf16[64,3,2,2048]{3,2,1,0:T(2,128)(2,1)} %all-to-all-done.rows_ref, bf16[2048,256]{1,0:T(8,128)(2,1)} %bitcast.22, bf16[2048,256]{1,0:T(8,128)(2,1)} %collective-permute-done.4.refs_1_.refs_4_, bf16[2048,256]{1,0:T(8,128)(2,1)} %bitcast.25, ...), custom_call_target="tpu_custom_call" | custom-call | flops 3221225472 | bytes 9437184 | tf_op jit(solution)/shard_map/hidden/pallas_call | solution.py:235
  107.7 2.5 %down.2.near_ref = f32[384,2048]{1,0:T(8,128)S(1)} custom-call(s32[1]{0:T(128)} %bitcast.1.flag_ref, bf16[384,1024]{1,0:T(8,128)(2,1)S(1)} %copy-done.1, bf16[256,2048]{1,0:T(8,128)(2,1)} %collective-permute-done.12.first_ref, bf16[256,2048]{1,0:T(8,128)(2,1)} %collective-permute-done.13.second_ref), custom_call_target="tpu_custom_call" | custom-call | flops 805306368 | bytes 4194304 | tf_op jit(solution)/shard_map/down/pallas_call | solution.py:301
  110.3 2.4 %down.3 = bf16[64,3,2,2048]{3,2,1,0:T(2,128)(2,1)S(1)} custom-call(s32[1]{0:T(128)} %bitcast.1.flag_ref, bf16[384,1024]{1,0:T(8,128)(2,1)S(1)} %copy-done.1, f32[384,2048]{1,0:T(8,128)S(1)} %down.2.near_ref, bf16[256,2048]{1,0:T(8,128)(2,1)} %collective-permute-done.14.second_ref, bf16[256,2048]{1,0:T(8,128)(2,1)S(1)} %bitcast.19, ...), custom_call_target="tpu_custom_call" | custom-call | flops 805306368 | bytes 4194304 | tf_op jit(solution)/shard_map/down/pallas_call | solution.py:309
  113.8 12.1 %all-to-all-start.1 = ((bf16[64,3,2,2048]{3,2,1,0:T(2,128)(2,1)}), bf16[64,3,2,2048]{3,2,1,0:T(2,128)(2,1)S(1)}, u32[]{:S(2)}, u32[]{:S(2)}) async-start(bf16[64,3,2,2048]{3,2,1,0:T(2,128)(2,1)} %copy-done.2), calls=%async_computation.1 | async-start | bytes 3145728 | tf_op jit(solution)/shard_map/all_to_all | solution.py:322
  125.9 2.1 %fusion = f32[512]{0:T(512)S(1)} fusion(bf16[512,2048]{1,0:T(8,128)(2,1)} %param.14), kind=kLoop, calls=%fused_computation.2 | loop fusion | flops 3145216 | bytes 2099200 | tf_op jit(solution)/shard_map/reduce_sum | solution.py:48
  128.3 1.3 convolution_exponential_fusion
  130.6 2.6 %fusion.7 = bf16[512,256]{1,0:T(8,128)(2,1)S(1)} fusion(bf16[2048,256]{1,0:T(8,128)(2,1)} %param.16, bf16[512,2048]{1,0:T(8,128)(2,1)} %param.14, f32[2048]{0:T(1024)S(1)} %convert_element_type.136, f32[512]{0:T(512)S(1)} %add_rsqrt_fusion), kind=kOutput, calls=%fused_computation.10 | convolution fusion | flops 541196288 | bytes 3418112 | tf_op jit(solution)/shard_map/dot_general | solution.py:54
  133.4 3.9 %convolution_convert_fusion = bf16[512,2048]{1,0:T(8,128)(2,1)} fusion(bf16[256,2048]{1,0:T(8,128)(2,1)S(1)} %copy-done, f32[256]{0:T(256)S(1)} %convert_element_type.161, f32[527,256]{1,0:T(8,128)S(1)} %maximum_convert_fusion, f32[512]{0:T(512)S(1)} %minimum_convert_fusion, f32[]{:T(128)S(6)} %convert_element_type.158, f32[]{:T(128)S(6)} %convert_element_type.157, ...), kind=kOutput, calls=%fused_computation.5 | convolution fusion | flops 609746944 | bytes 11668544 | tf_op jit(solution)/shard_map/dot_general | solution.py:78
  137.3 2.5 %constant_dynamic-slice_fusion.6 = (bf16[128,2048]{1,0:T(8,128)(2,1)}, bf16[128,2048]{1,0:T(8,128)(2,1)S(1)}, bf16[128,2048]{1,0:T(8,128)(2,1)}) fusion(bf16[512,2048]{1,0:T(8,128)(2,1)} %convolution_convert_fusion, s32[]{:T(128)S(6)} %select_n.68, s32[]{:T(128)S(6)} %select_n.70, s32[]{:T(128)S(6)} %select_n.69), kind=kLoop, calls=%fused_computation.88 | loop fusion | bytes 3145740 | tf_op jit(solution)/shard_map/dynamic_slice | solution.py:87
  140.4 1.8 %collective-permute-start.2 = (bf16[128,2048]{1,0:T(8,128)(2,1)}, bf16[128,2048]{1,0:T(8,128)(2,1)}, u32[]{:S(2)}, u32[]{:S(2)}) collective-permute-start(bf16[128,2048]{1,0:T(8,128)(2,1)} %get-tuple-element.12), channel_id=1, source_target_pairs={{0,2},{1,3},{2,0},{3,1},{4,6},{5,7},{6,4},{7,5},{8,10},{9,11},{10,... | collective-permute-start | bytes 1572872 | tf_op jit(solution)/shard_map/ppermute | solution.py:23
  142.2 2.3 %collective-permute-start.3 = (bf16[128,2048]{1,0:T(8,128)(2,1)S(1)}, bf16[128,2048]{1,0:T(8,128)(2,1)}, u32[]{:S(2)}, u32[]{:S(2)}) collective-permute-start(bf16[128,2048]{1,0:T(8,128)(2,1)S(1)} %get-tuple-element.11), channel_id=1, source_target_pairs={{0,3},{1,2},{2,1},{3,0},{4,7},{5,6},{6,5},{7,4},{8,11},{9,10},{10,... | collective-permute-start | bytes 1572872 | tf_op jit(solution)/shard_map/ppermute | solution.py:23
  146.6 19.3 %all-to-all-done.1.returned_ref = bf16[64,3,2,2048]{3,2,1,0:T(2,128)(2,1)S(1)} async-done(((bf16[64,3,2,2048]{3,2,1,0:T(2,128)(2,1)}), bf16[64,3,2,2048]{3,2,1,0:T(2,128)(2,1)S(1)}, u32[]{:S(2)}, u32[]{:S(2)}) %all-to-all-start.1) | async-done | bytes 1572896 | tf_op jit(solution)/shard_map/all_to_all | solution.py:322
  168.5 2.6 %add_convert_fusion = bf16[128,2048]{1,0:T(8,128)(2,1)} fusion(bf16[128,2048]{1,0:T(8,128)(2,1)} %collective-permute-done.3, bf16[128,2048]{1,0:T(8,128)(2,1)} %collective-permute-done.2, bf16[128,2048]{1,0:T(8,128)(2,1)} %collective-permute-done.1, bf16[512,2048]{1,0:T(8,128)(2,1)} %convolution_convert_fusion, s32[]{:T(128)S(6)} %select_n.67), kind=kLoop, calls=%fused_computation.17 | loop fusion | flops 2097152 | bytes 2621444 | tf_op jit(solution)/shard_map/convert_element_type | solution.py:93
  171.9 2.6 %collective-permute-done.16 = bf16[96,2048]{1,0:T(8,128)(2,1)S(1)} collective-permute-done((bf16[96,2048]{1,0:T(8,128)(2,1)S(1)}, bf16[96,2048]{1,0:T(8,128)(2,1)S(1)}, u32[]{:S(2)}, u32[]{:S(2)}) %collective-permute-start.16) | collective-permute-done | bytes 393248 | tf_op jit(solution)/shard_map/ppermute | solution.py:382
  (80 shorter events, 18.5 us)
Async XLA Ops:
  0.6 132.8 %copy-start = (bf16[256,2048]{1,0:T(8,128)(2,1)S(1)}, bf16[256,2048]{1,0:T(8,128)(2,1)}, u32[]{:S(2)}) copy-start(bf16[256,2048]{1,0:T(8,128)(2,1)} %param.19) | copy-start | bytes 3145732
  4.2 20.5 %copy-start.5 = (bf16[1,256,2048]{2,1,0:T(8,128)(2,1)S(1)}, bf16[1,256,2048]{2,1,0:T(8,128)(2,1)}, u32[]{:S(2)}) copy-start(bf16[1,256,2048]{2,1,0:T(8,128)(2,1)} %param.27) | copy-start | bytes 3145732
  4.2 89.4 %copy-start.11 = (bf16[2048]{0:T(1024)(128)(2,1)S(1)}, bf16[2048]{0:T(1024)(128)(2,1)}, u32[]{:S(2)}) copy-start(bf16[2048]{0:T(1024)(128)(2,1)} %param.15) | copy-start | bytes 12292
  7.2 91.4 %all-to-all-start = ((bf16[64,3,2,2048]{3,2,1,0:T(2,128)(2,1)}), bf16[64,3,2,2048]{3,2,1,0:T(2,128)(2,1)}, u32[]{:S(2)}, u32[]{:S(2)}) async-start(bf16[64,3,2,2048]{3,2,1,0:T(2,128)(2,1)} %get-tuple-element.5), calls=%async_computation | async-start | bytes 3145728 | tf_op jit(solution)/shard_map/all_to_all | solution.py:322
  19.5 29.0 %collective-permute-start.10 = (bf16[2048,256]{1,0:T(8,128)(2,1)}, bf16[2048,256]{1,0:T(8,128)(2,1)S(1)}, u32[]{:S(2)}, u32[]{:S(2)}) collective-permute-start(bf16[2048,256]{1,0:T(8,128)(2,1)} %bitcast.23), channel_id=1, source_target_pairs={{0,6},{1,2},{2,4},{3,0},{4,7},{5,3},{6,5},{7,1},{8,14},{9,10},{10,... | collective-permute-start | bytes 3145736 | tf_op jit(solution)/shard_map/ppermute | solution.py:35
  22.3 27.6 %collective-permute-start.4 = (bf16[2048,256]{1,0:T(8,128)(2,1)}, bf16[2048,256]{1,0:T(8,128)(2,1)}, u32[]{:S(2)}, u32[]{:S(2)}) collective-permute-start(bf16[2048,256]{1,0:T(8,128)(2,1)} %bitcast.20), channel_id=1, source_target_pairs={{0,4},{1,0},{2,6},{3,2},{4,5},{5,1},{6,7},{7,3},{8,12},{9,8},{10,1... | collective-permute-start | bytes 3145736 | tf_op jit(solution)/shard_map/ppermute | solution.py:35
  22.3 48.8 %collective-permute-start.5 = (bf16[2048,256]{1,0:T(8,128)(2,1)}, bf16[2048,256]{1,0:T(8,128)(2,1)}, u32[]{:S(2)}, u32[]{:S(2)}) collective-permute-start(bf16[2048,256]{1,0:T(8,128)(2,1)} %bitcast.24), channel_id=1, source_target_pairs={{0,4},{1,0},{2,6},{3,2},{4,5},{5,1},{6,7},{7,3},{8,12},{9,8},{10,1... | collective-permute-start | bytes 3145736 | tf_op jit(solution)/shard_map/ppermute | solution.py:35
  23.0 48.1 %collective-permute-start.8 = (bf16[2048,256]{1,0:T(8,128)(2,1)}, bf16[2048,256]{1,0:T(8,128)(2,1)}, u32[]{:S(2)}, u32[]{:S(2)}) collective-permute-start(bf16[2048,256]{1,0:T(8,128)(2,1)} %bitcast.21), channel_id=1, source_target_pairs={{0,6},{1,2},{2,4},{3,0},{4,7},{5,3},{6,5},{7,1},{8,14},{9,10},{10,... | collective-permute-start | bytes 3145736 | tf_op jit(solution)/shard_map/ppermute | solution.py:35
  24.7 67.3 %collective-permute-start.12 = (bf16[256,2048]{1,0:T(8,128)(2,1)S(1)}, bf16[256,2048]{1,0:T(8,128)(2,1)}, u32[]{:S(2)}, u32[]{:S(2)}) collective-permute-start(bf16[256,2048]{1,0:T(8,128)(2,1)S(1)} %bitcast.17), channel_id=1, source_target_pairs={{0,4},{1,0},{2,6},{3,2},{4,5},{5,1},{6,7},{7,3},{8,12},{9,8},{10,1... | collective-permute-start | bytes 3145736 | tf_op jit(solution)/shard_map/ppermute | solution.py:35
  48.4 43.6 %copy-start.6 = (bf16[2048,256]{1,0:T(8,128)(2,1)}, bf16[2048,256]{1,0:T(8,128)(2,1)S(1)}, u32[]{:S(2)}) copy-start(bf16[2048,256]{1,0:T(8,128)(2,1)S(1)} %collective-permute-done.10.refs_10_.refs_15_) | copy-start | bytes 3145732
  48.4 43.6 %collective-permute-start.13 = (bf16[256,2048]{1,0:T(8,128)(2,1)S(1)}, bf16[256,2048]{1,0:T(8,128)(2,1)}, u32[]{:S(2)}, u32[]{:S(2)}) collective-permute-start(bf16[256,2048]{1,0:T(8,128)(2,1)S(1)} %bitcast.18), channel_id=1, source_target_pairs={{0,6},{1,2},{2,4},{3,0},{4,7},{5,3},{6,5},{7,1},{8,14},{9,10},{10,... | collective-permute-start | bytes 3145736 | tf_op jit(solution)/shard_map/ppermute | solution.py:35
  49.9 42.6 %collective-permute-start.11 = (bf16[2048,256]{1,0:T(8,128)(2,1)S(1)}, bf16[2048,256]{1,0:T(8,128)(2,1)S(1)}, u32[]{:S(2)}, u32[]{:S(2)}) collective-permute-start(bf16[2048,256]{1,0:T(8,128)(2,1)S(1)} %collective-permute-done.10.refs_10_.refs_15_), channel_id=1, source_target_pairs={{0,4},{1,5},{2,6},{3,7},{4,0},{5,1},{6,2},{7,3},{8,12},{9,13},{10,... | collective-permute-start | bytes 3145736 | tf_op jit(solution)/shard_map/ppermute | solution.py:35
  71.1 25.0 %collective-permute-start.6 = (bf16[2048,256]{1,0:T(8,128)(2,1)}, bf16[2048,256]{1,0:T(8,128)(2,1)}, u32[]{:S(2)}, u32[]{:S(2)}) collective-permute-start(bf16[2048,256]{1,0:T(8,128)(2,1)} %collective-permute-done.4.refs_1_.refs_4_), channel_id=1, source_target_pairs={{0,4},{1,5},{2,6},{3,7},{4,0},{5,1},{6,2},{7,3},{8,12},{9,13},{10,... | collective-permute-start | bytes 3145736 | tf_op jit(solution)/shard_map/ppermute | solution.py:35
  71.1 27.5 %collective-permute-start.7 = (bf16[2048,256]{1,0:T(8,128)(2,1)}, bf16[2048,256]{1,0:T(8,128)(2,1)}, u32[]{:S(2)}, u32[]{:S(2)}) collective-permute-start(bf16[2048,256]{1,0:T(8,128)(2,1)} %collective-permute-done.5.refs_3_.refs_6_), channel_id=1, source_target_pairs={{0,4},{1,5},{2,6},{3,7},{4,0},{5,1},{6,2},{7,3},{8,12},{9,13},{10,... | collective-permute-start | bytes 3145736 | tf_op jit(solution)/shard_map/ppermute | solution.py:35
  91.9 6.7 %collective-permute-start.9 = (bf16[2048,256]{1,0:T(8,128)(2,1)}, bf16[2048,256]{1,0:T(8,128)(2,1)}, u32[]{:S(2)}, u32[]{:S(2)}) collective-permute-start(bf16[2048,256]{1,0:T(8,128)(2,1)} %collective-permute-done.8.refs_8_.refs_13_), channel_id=1, source_target_pairs={{0,4},{1,5},{2,6},{3,7},{4,0},{5,1},{6,2},{7,3},{8,12},{9,13},{10,... | collective-permute-start | bytes 3145736 | tf_op jit(solution)/shard_map/ppermute | solution.py:35
  92.1 18.2 %collective-permute-start.14 = (bf16[256,2048]{1,0:T(8,128)(2,1)}, bf16[256,2048]{1,0:T(8,128)(2,1)}, u32[]{:S(2)}, u32[]{:S(2)}) collective-permute-start(bf16[256,2048]{1,0:T(8,128)(2,1)} %collective-permute-done.13.second_ref), channel_id=1, source_target_pairs={{0,4},{1,5},{2,6},{3,7},{4,0},{5,1},{6,2},{7,3},{8,12},{9,13},{10,... | collective-permute-start | bytes 3145736 | tf_op jit(solution)/shard_map/ppermute | solution.py:35
  93.5 16.8 %collective-permute-start.15 = (bf16[256,2048]{1,0:T(8,128)(2,1)}, bf16[256,2048]{1,0:T(8,128)(2,1)}, u32[]{:S(2)}, u32[]{:S(2)}) collective-permute-start(bf16[256,2048]{1,0:T(8,128)(2,1)} %collective-permute-done.12.first_ref), channel_id=1, source_target_pairs={{0,4},{1,5},{2,6},{3,7},{4,0},{5,1},{6,2},{7,3},{8,12},{9,13},{10,... | collective-permute-start | bytes 3145736 | tf_op jit(solution)/shard_map/ppermute | solution.py:35
  96.2 37.2 %collective-permute-start = (bf16[15,256]{1,0:T(8,128)(2,1)S(1)}, bf16[15,256]{1,0:T(8,128)(2,1)S(1)}, u32[]{:S(2)}, u32[]{:S(2)}) collective-permute-start(bf16[15,256]{1,0:T(8,128)(2,1)S(1)} %slice.254), channel_id=1, source_target_pairs={{0,4},{4,8},{8,12},{12,16},{16,20},{20,24},{24,28},{28,32},{32,36}... | collective-permute-start | bytes 23048 | tf_op jit(solution)/shard_map/ppermute | solution.py:18
  113.8 52.1 %all-to-all-start.1 = ((bf16[64,3,2,2048]{3,2,1,0:T(2,128)(2,1)}), bf16[64,3,2,2048]{3,2,1,0:T(2,128)(2,1)S(1)}, u32[]{:S(2)}, u32[]{:S(2)}) async-start(bf16[64,3,2,2048]{3,2,1,0:T(2,128)(2,1)} %copy-done.2), calls=%async_computation.1 | async-start | bytes 3145728 | tf_op jit(solution)/shard_map/all_to_all | solution.py:322
  137.3 28.5 %copy-start.4 = (bf16[2,192,384]{2,1,0:T(8,128)(2,1)S(1)}, bf16[2,192,384]{2,1,0:T(8,128)(2,1)}, u32[]{:S(2)}) copy-start(bf16[2,192,384]{2,1,0:T(8,128)(2,1)} %copy-done.3) | copy-start | bytes 884740
  139.9 27.4 %collective-permute-start.1 = (bf16[128,2048]{1,0:T(8,128)(2,1)}, bf16[128,2048]{1,0:T(8,128)(2,1)}, u32[]{:S(2)}, u32[]{:S(2)}) collective-permute-start(bf16[128,2048]{1,0:T(8,128)(2,1)} %get-tuple-element.10), channel_id=1, source_target_pairs={{0,1},{1,0},{2,3},{3,2},{4,5},{5,4},{6,7},{7,6},{8,9},{9,8},{10,11... | collective-permute-start | bytes 1572872 | tf_op jit(solution)/shard_map/ppermute | solution.py:23
  140.4 26.8 %collective-permute-start.2 = (bf16[128,2048]{1,0:T(8,128)(2,1)}, bf16[128,2048]{1,0:T(8,128)(2,1)}, u32[]{:S(2)}, u32[]{:S(2)}) collective-permute-start(bf16[128,2048]{1,0:T(8,128)(2,1)} %get-tuple-element.12), channel_id=1, source_target_pairs={{0,2},{1,3},{2,0},{3,1},{4,6},{5,7},{6,4},{7,5},{8,10},{9,11},{10,... | collective-permute-start | bytes 1572872 | tf_op jit(solution)/shard_map/ppermute | solution.py:23
  142.2 26.2 %collective-permute-start.3 = (bf16[128,2048]{1,0:T(8,128)(2,1)S(1)}, bf16[128,2048]{1,0:T(8,128)(2,1)}, u32[]{:S(2)}, u32[]{:S(2)}) collective-permute-start(bf16[128,2048]{1,0:T(8,128)(2,1)S(1)} %get-tuple-element.11), channel_id=1, source_target_pairs={{0,3},{1,2},{2,1},{3,0},{4,7},{5,6},{6,5},{7,4},{8,11},{9,10},{10,... | collective-permute-start | bytes 1572872 | tf_op jit(solution)/shard_map/ppermute | solution.py:23
  166.6 7.9 %collective-permute-start.16 = (bf16[96,2048]{1,0:T(8,128)(2,1)S(1)}, bf16[96,2048]{1,0:T(8,128)(2,1)S(1)}, u32[]{:S(2)}, u32[]{:S(2)}) collective-permute-start(bf16[96,2048]{1,0:T(8,128)(2,1)S(1)} %combine.3), channel_id=1, source_target_pairs={{0,1},{1,0},{2,3},{3,2},{4,7},{5,6},{6,5},{7,4},{8,9},{9,8},{10,11... | collective-permute-start | bytes 1179656 | tf_op jit(solution)/shard_map/ppermute | solution.py:382
  (8 other events, 28.8 us)
